TPU v7x, 512 devices: a whole 4x4x16 slice. The times are simulated.
512 devices in a mesh: sp: 64 (over z, y), tp: 8 (over x, core).
Axes of the slice: x: 4, y: 4, z: 16, core: 2. Of those that a mesh axis runs over, the one named last changes fastest.
Arguments:
- latent: bfloat16 [49152, 2048], P(('sp', 'tp')), may hold values from -6 to 6
- condition: float32 [2048], P('sp'), may hold values from -6 to 6
- context_condition: float32 [2048], P('sp'), may hold values from -6 to 6
- context: bfloat16 [1024, 2048], P('sp'), may hold values from -6 to 6
- norm_gain: float32 [2048], replicated, may hold values from 0.1 to 1.9
- shift_weight: bfloat16 [2048, 2048], P('sp', 'tp'), may hold values from -0.375 to 0.375
- scale_weight: bfloat16 [2048, 2048], P('sp', 'tp'), may hold values from -0.375 to 0.375
- gate_weight: bfloat16 [2048, 2048], P('sp', 'tp'), may hold values from -0.375 to 0.375
- query_weight: bfloat16 [2048, 2048], P(None, 'tp'), may hold values from -2 to 2
- key_matrix: bfloat16 [2048, 1024], P(None, 'tp'), may hold values from -2 to 2
- value_matrix: bfloat16 [2048, 1024], P(None, 'tp'), may hold values from -0.125 to 0.125
- sink_logit_head: float32 [16], P('tp'), may hold values from 6 to 10
- out_weight: bfloat16 [2048, 2048], P('tp'), may hold values from -0.125 to 0.125
Outputs:
- updated: bfloat16 [49152, 2048], P(('sp', 'tp'))
All inputs are finite; a program needn't handle non-finite values.
Results may differ from a plain program's by a relative error of at most 0.012.
The roundings to bfloat16 on the way count: a program that leaves them out, or rounds other values in their place, can miss the bound.
Values may be sent and summed in bfloat16 or wider, within the bound.
No kernel may reach another device: no remote copies, remote signals or barrier semaphores. Data moves between devices by JAX's collectives and lax.ppermute only.
A program may use at most 64 MiB of HBM per device.

v0:
```python
import functools

import jax
import jax.numpy as jnp
from jax import lax
from jax.sharding import Mesh
from jax.sharding import PartitionSpec as P

QUERY_HEADS = 16
KEY_VALUE_HEADS = 8
HEAD_DIM = 128
WINDOW_REACH = 128
GRID_W = 64
SP = ("sp_0", "sp_1")
SP_TP = ("sp_0", "sp_1", "tp")


NORM_EPS = 1e-05
MASKED_SCORE = -1e30


def one_axis_at_a_time(x, axes):
    return functools.reduce(lax.psum, axes, x)


def side_by_side(arrays, axis, dim, along):
    both = jnp.concatenate(arrays, axis=along)
    out, at, outs = (lax.all_gather(both, axis, axis=dim, tiled=True), 0, [])
    for a in arrays:
        outs.append(lax.slice_in_dim(out, at, at + a.shape[along], axis=along))
        at += a.shape[along]
    return tuple(outs)


def padded_2(block, sides, width):
    for axis, dim in sides:
        count = lax.axis_size(axis)
        forward = [(i, i + 1) for i in range(count - 1)]
        backward = [(target, source) for source, target in forward]
        low = lax.ppermute(
            lax.slice_in_dim(block, block.shape[dim] - width, None, axis=dim), axis, forward
        )
        high = lax.ppermute(lax.slice_in_dim(block, 0, width, axis=dim), axis, backward)
        block = jnp.concatenate([low, block, high], axis=dim)
    return block


def sent_to_all(x, axis):
    peers = lax.axis_size(axis)
    return lax.all_to_all(jnp.broadcast_to(x[None], (peers, *x.shape)), axis, 0, 0, tiled=True)


def laid_out(blocks, dim):
    blocks = jnp.moveaxis(blocks, 0, dim)
    shape = blocks.shape
    return blocks.reshape(*shape[:dim], shape[dim] * shape[dim + 1], *shape[dim + 2 :])


def gathered_copies(x, axis, dim):
    blocks = sent_to_all(x, axis)
    return laid_out(blocks, dim)


def in_blocks(x, dim, peers):
    before, after = (x.shape[:dim], x.shape[dim + 1 :])
    return jnp.moveaxis(x.reshape(*before, peers, -1, *after), dim, 0)


def summed_on_arrival(x, axis, dim):
    peers = lax.axis_size(axis)
    blocks = lax.all_to_all(in_blocks(x, dim, peers), axis, 0, 0, tiled=True)
    return jnp.sum(blocks.astype(jnp.float32), axis=0)


def rotate(vectors, position):
    quarter = HEAD_DIM // 4
    grid_row = (position // GRID_W).astype(jnp.float32)
    grid_col = (position % GRID_W).astype(jnp.float32)
    inv_freq = 10000.0 ** (-jnp.arange(0, HEAD_DIM // 2, 2, dtype=jnp.float32) / (HEAD_DIM // 2))
    angles = jnp.concatenate([grid_row[:, None] * inv_freq, grid_col[:, None] * inv_freq], axis=-1)
    cosine_table = jnp.cos(angles).reshape(-1, 1, 2, quarter)
    sine_table = jnp.sin(angles).reshape(-1, 1, 2, quarter)
    pieces = vectors.reshape(vectors.shape[0], vectors.shape[1], 2, 2, quarter)
    first_half = pieces[..., 0, :]
    second_half = pieces[..., 1, :]
    turned = jnp.stack(
        [
            first_half * cosine_table - second_half * sine_table,
            first_half * sine_table + second_half * cosine_table,
        ],
        axis=-2,
    )
    return turned.reshape(vectors.shape)


def modulated_norm(rows_in, norm_gain, shift, scale):
    floats = rows_in.astype(jnp.float32)
    normed = (
        floats * lax.rsqrt(jnp.mean(floats * floats, axis=-1, keepdims=True) + NORM_EPS) * norm_gain
    )
    return (normed * (1.0 + scale) + shift).astype(jnp.bfloat16)


def shards(
    latent,
    condition,
    context_condition,
    context,
    norm_gain,
    shift_weight,
    scale_weight,
    gate_weight,
    query_weight,
    key_matrix,
    value_matrix,
    sink_logit_head,
    out_weight,
):
    tp_count = lax.axis_size("tp")
    group_rows = latent.shape[0] * tp_count
    offset = lax.axis_index(SP) * group_rows
    total_rows = group_rows * lax.axis_size(SP)
    active = jax.nn.silu(jnp.stack([condition, context_condition])).astype(jnp.bfloat16)
    shift_part = jnp.dot(active, shift_weight, preferred_element_type=jnp.float32)
    scale_part = jnp.dot(active, scale_weight, preferred_element_type=jnp.float32)
    gate_part = jnp.dot(active[:1], gate_weight, preferred_element_type=jnp.float32)
    shift_sum, scale_sum, gate_sum = (
        one_axis_at_a_time(shift_part, SP),
        one_axis_at_a_time(scale_part, SP),
        one_axis_at_a_time(gate_part, SP),
    )
    shift_all, scale_all, gate_all = side_by_side((shift_sum, scale_sum, gate_sum), "tp", 1, 0)
    hidden_state = modulated_norm(latent, norm_gain, shift_all[0], scale_all[0])
    query_width = query_weight.shape[1]
    pair_width = key_matrix.shape[1]
    block_rows = lax.all_gather(hidden_state, "tp", axis=0, tiled=True)
    row_count = block_rows.shape[0]
    position = offset + jnp.arange(row_count, dtype=jnp.int32)
    query_row_block = jnp.dot(block_rows, query_weight, preferred_element_type=jnp.float32)
    query_row_block = rotate(query_row_block.reshape(row_count, -1, HEAD_DIM), position)
    key_rows = jnp.dot(block_rows, key_matrix, preferred_element_type=jnp.float32)
    key_rows = rotate(key_rows.reshape(row_count, -1, HEAD_DIM), position)
    value_rows = jnp.dot(block_rows, value_matrix, preferred_element_type=jnp.float32)
    projected = jnp.concatenate(
        [
            query_row_block.reshape(row_count, query_width),
            key_rows.reshape(row_count, pair_width),
            value_rows,
        ],
        axis=1,
    ).astype(jnp.bfloat16)
    padded = padded_2(projected[:, query_width:], ((SP, 0),), WINDOW_REACH)
    ctx_hidden = modulated_norm(context, norm_gain, shift_all[1], scale_all[1])
    ctx_pairs = gathered_copies(
        jnp.concatenate(
            [
                jnp.dot(ctx_hidden, key_matrix, preferred_element_type=jnp.float32),
                jnp.dot(ctx_hidden, value_matrix, preferred_element_type=jnp.float32),
            ],
            axis=1,
        ).astype(jnp.bfloat16),
        SP,
        0,
    )
    blocks = group_rows // WINDOW_REACH
    kv_local = pair_width // HEAD_DIM
    queries_per_group = QUERY_HEADS // KEY_VALUE_HEADS
    query_blocks = projected[:, :query_width].reshape(
        blocks, WINDOW_REACH, kv_local, queries_per_group, HEAD_DIM
    )
    key_pad = padded[:, :pair_width].reshape(blocks + 2, WINDOW_REACH, kv_local, HEAD_DIM)
    value_pad = padded[:, pair_width:].reshape(blocks + 2, WINDOW_REACH, kv_local, HEAD_DIM)
    band_keys = jnp.concatenate([key_pad[:-2], key_pad[1:-1], key_pad[2:]], axis=1)
    band_values = jnp.concatenate([value_pad[:-2], value_pad[1:-1], value_pad[2:]], axis=1)
    context_key_rows = ctx_pairs[:, :pair_width].reshape(-1, kv_local, HEAD_DIM)
    context_value_rows = ctx_pairs[:, pair_width:].reshape(-1, kv_local, HEAD_DIM)
    factor = HEAD_DIM ** (-0.5)
    band_scores = (
        jnp.einsum("nqhgd,nkhd->nhgqk", query_blocks, band_keys, preferred_element_type=jnp.float32)
        * factor
    )
    block_ids = jnp.arange(blocks, dtype=jnp.int32)[:, None, None]
    query_pos = (
        offset + block_ids * WINDOW_REACH + jnp.arange(WINDOW_REACH, dtype=jnp.int32)[None, :, None]
    )
    key_pos = (
        offset
        + (block_ids - 1) * WINDOW_REACH
        + jnp.arange(3 * WINDOW_REACH, dtype=jnp.int32)[None, None, :]
    )
    allowed = (
        (jnp.abs(key_pos - query_pos) <= WINDOW_REACH) & (key_pos >= 0) & (key_pos < total_rows)
    )
    band_scores = jnp.where(allowed[:, None, None], band_scores, MASKED_SCORE)
    ctx_scores = (
        jnp.einsum(
            "nqhgd,chd->nhgqc", query_blocks, context_key_rows, preferred_element_type=jnp.float32
        )
        * factor
    )
    sink_logit_rows = sink_logit_head.reshape(1, kv_local, queries_per_group, 1, 1)
    maxima = jnp.maximum(
        jnp.maximum(
            jnp.max(band_scores, axis=-1, keepdims=True),
            jnp.max(ctx_scores, axis=-1, keepdims=True),
        ),
        sink_logit_rows,
    )
    band_exp = jnp.exp(band_scores - maxima)
    ctx_exp = jnp.exp(ctx_scores - maxima)
    denominator = (
        jnp.sum(band_exp, axis=-1, keepdims=True)
        + jnp.sum(ctx_exp, axis=-1, keepdims=True)
        + jnp.exp(sink_logit_rows - maxima)
    )
    band_weights = (band_exp / denominator).astype(jnp.bfloat16)
    ctx_weights = (ctx_exp / denominator).astype(jnp.bfloat16)
    attended = jnp.einsum(
        "nhgqk,nkhd->nqhgd", band_weights, band_values, preferred_element_type=jnp.float32
    ) + jnp.einsum(
        "nhgqc,chd->nqhgd", ctx_weights, context_value_rows, preferred_element_type=jnp.float32
    )
    attended = attended.astype(jnp.bfloat16).reshape(group_rows, query_width)
    mixed_sum = summed_on_arrival(
        jnp.dot(attended, out_weight, preferred_element_type=jnp.float32).astype(jnp.bfloat16),
        "tp",
        0,
    )
    return (latent.astype(jnp.float32) + gate_all[0] * mixed_sum).astype(jnp.bfloat16)


def solution(mesh):
    torus = Mesh(mesh.devices.reshape(16, 4, mesh.shape["tp"]), ("sp_0", "sp_1", "tp"))
    return jax.shard_map(
        shards,
        mesh=torus,
        in_specs=(
            P(SP_TP, None),
            P(SP),
            P(SP),
            P(SP, None),
            P(),
            P(SP, "tp"),
            P(SP, "tp"),
            P(SP, "tp"),
            P(None, "tp"),
            P(None, "tp"),
            P(None, "tp"),
            P("tp"),
            P("tp", None),
        ),
        out_specs=P(SP_TP, None),
        check_vma=False,
    )
```

profile of v0, /device:TPU:128, one launch (start us, length us, event | category | flops | bytes accessed | tf_op | source)
XLA Modules:
  0.0 187.9 jit_solution(3284651303342493575)
XLA Ops:
  6.6 1.3 fusion.20
  11.1 30.9 %all-reduce = (f32[1,256]{1,0:T(1,128)S(1)}, f32[2,256]{1,0:T(2,128)S(1)}, f32[2,256]{1,0:T(2,128)S(1)}) all-reduce(f32[1,256]{1,0:T(1,128)S(1)} %fusion.59, f32[2,256]{1,0:T(2,128)S(1)} %fusion.71, f32[2,256]{1,0:T(2,128)S(1)} %fusion.70), channel_id=1, replica_groups=mesh['sp_0'=16,'sp_1'=4,'tp'=8] {'sp_0'}, use_global_device_ids=true, to_apply=%region_4.5 | all-reduce | flops 1280 | bytes 10240 | tf_op jit(solution)/shard_map/psum | solution.py:23
  42.0 10.8 %all-reduce.1 = (f32[1,256]{1,0:T(1,128)S(1)}, f32[2,256]{1,0:T(2,128)S(1)}, f32[2,256]{1,0:T(2,128)S(1)}) all-reduce(f32[1,256]{1,0:T(1,128)S(1)} %get-tuple-element.5, f32[2,256]{1,0:T(2,128)S(1)} %get-tuple-element.6, f32[2,256]{1,0:T(2,128)S(1)} %get-tuple-element.7), channel_id=1, replica_groups=mesh['sp_0'=16,'sp_1'=4,'tp'=8] {'sp_1'}, use_global_device_ids=true, to_apply=%region_5.6 | all-reduce | flops 1280 | bytes 10240 | tf_op jit(solution)/shard_map/psum | solution.py:23
  52.9 13.1 %all_gather.6 = f32[5,2048]{1,0:T(8,128)S(1)} all-gather(f32[5,256]{1,0:T(8,128)S(1)} %pad_maximum_fusion.12), channel_id=1, replica_groups=mesh['sp_0'=16,'sp_1'=4,'tp'=8] {'tp'}, dimensions={1}, use_global_device_ids=true | all-gather | bytes 46080 | tf_op jit(solution)/shard_map/all_gather | solution.py:28
  66.0 2.0 %fusion.24 = bf16[96,2048]{1,0:T(8,128)(2,1)} fusion(bf16[96,2048]{1,0:T(8,128)(2,1)} %param.13, f32[2048]{0:T(1024)S(1)} %bitcast.156, f32[2048]{0:T(1024)S(1)} %bitcast.157, f32[2048]{0:T(1024)} %param.17, f32[96]{0:T(128)S(1)} %add_rsqrt_fusion.1), kind=kLoop, calls=%fused_computation.34 | loop fusion | flops 1179648 | bytes 811392 | tf_op jit(solution)/shard_map/convert_element_type | solution.py:101
  68.0 1.0 fusion.42
  69.0 1.3 convolution_convert_fusion.2
  70.6 0.8 broadcast_in_dim.12
  71.5 12.3 %all-to-all-start = ((bf16[64,16,256]{2,1,0:T(8,128)(2,1)}), bf16[64,16,256]{2,1,0:T(8,128)(2,1)S(1)}, u32[]{:S(2)}, u32[]{:S(2)}) async-start(bf16[64,16,256]{2,1,0:T(8,128)(2,1)} %broadcast_in_dim.12), calls=%async_computation | async-start | bytes 1048576 | tf_op jit(solution)/shard_map/all_to_all | solution.py:50
  84.8 1.4 fusion.18
  86.2 14.9 %all-gather.2.cloned.1.call-done = bf16[768,2048]{1,0:T(8,128)(2,1)} async-done(((bf16[96,2048]{1,0:T(8,128)(2,1)}), bf16[768,2048]{1,0:T(8,128)(2,1)}) %all-gather.2.cloned.1.call-update) | async-done | bytes 3145744 | tf_op jit(solution)/shard_map/all_gather | solution.py:136
  101.2 3.0 %fusion.72 = f32[768,128]{0,1:T(8,128)S(1)} fusion(bf16[768,2048]{1,0:T(8,128)(2,1)} %all-gather.2.cloned.1.call-done, bf16[2048,128]{1,0:T(8,128)(2,1)S(1)} %copy-done.3), kind=kOutput, calls=%fused_computation.126 | convolution fusion | flops 402653184 | bytes 4063232 | tf_op jit(solution)/shard_map/dot_general | solution.py:141
  105.2 3.0 %convolution_convert_fusion.1 = bf16[768,128]{1,0:T(8,128)(2,1)S(1)} fusion(bf16[768,2048]{1,0:T(8,128)(2,1)} %all-gather.2.cloned.1.call-done, bf16[2048,128]{1,0:T(8,128)(2,1)S(1)} %copy-done.5), kind=kOutput, calls=%fused_computation.27 | convolution fusion | flops 402751488 | bytes 3866624 | tf_op jit(solution)/shard_map/dot_general | solution.py:143
  108.9 3.4 %collective-permute-start = (bf16[128,256]{1,0:T(8,128)(2,1)}, bf16[128,256]{1,0:T(8,128)(2,1)S(1)}, u32[]{:S(2)}, u32[]{:S(2)}) collective-permute-start(bf16[128,256]{1,0:T(8,128)(2,1)} %get-tuple-element.21), channel_id=1, source_target_pairs={{0,8},{8,16},{16,24},{24,32},{32,40},{40,48},{48,56},{56,64},{64,7... | collective-permute-start | bytes 196616 | tf_op jit(solution)/shard_map/ppermute | solution.py:40
  112.3 5.9 %collective-permute-start.1 = (bf16[128,256]{1,0:T(8,128)(2,1)}, bf16[128,256]{1,0:T(8,128)(2,1)S(1)}, u32[]{:S(2)}, u32[]{:S(2)}) collective-permute-start(bf16[128,256]{1,0:T(8,128)(2,1)} %get-tuple-element.22), channel_id=1, source_target_pairs={{8,0},{16,8},{24,16},{32,24},{40,32},{48,40},{56,48},{64,56},{72,6... | collective-permute-start | bytes 196616 | tf_op jit(solution)/shard_map/ppermute | solution.py:43
  118.3 1.1 fusion.73
  120.3 3.7 %bitcast_reduce_fusion = (f32[6,2,128]{2,1,0:T(2,128)S(1)}, f32[1024,6,128,2]{2,0,3,1:T(8,128)}) fusion(bf16[6,128,2,128]{3,1,2,0:T(8,128)(2,1)S(1)} %copy.27, bf16[1024,256]{1,0:T(8,128)(2,1)S(1)} %bitcast.144), kind=kOutput, calls=%fused_computation.1 | convolution fusion | flops 405797376 | bytes 6952960 | tf_op jit(solution)/shard_map/nqhgd,chd->nhgqc/dot_general | solution.py:196
  126.5 1.5 fusion.6
  128.1 3.8 %fusion.1 = f32[6,2,128]{2,1,0:T(2,128)S(1)} fusion(f32[1024,6,128,2]{2,0,3,1:T(8,128)} %get-tuple-element.41, f32[6,2,128]{2,1,0:T(2,128)S(1)} %maximum_maximum_fusion), kind=kLoop, calls=%fused_computation.5 | loop fusion | flops 4717056 | bytes 6303744 | tf_op jit(solution)/shard_map/reduce_sum | solution.py:213
  134.2 0.9 slice-done.1
  135.1 1.5 fusion.13
  137.0 1.0 convolution_convert_fusion
  138.0 41.2 %all_to_all.10 = bf16[8,96,2048]{2,1,0:T(8,128)(2,1)S(1)} all-to-all(bf16[8,96,2048]{2,1,0:T(8,128)(2,1)S(1)} %bitcast.139), channel_id=1, replica_groups=mesh['sp_0'=16,'sp_1'=4,'tp'=8] {'tp'}, dimensions={0} | all-to-all | bytes 6291456 | tf_op jit(solution)/shard_map/all_to_all | solution.py:71
  180.2 0.8 fusion.25
  (67 shorter events, 13.3 us)
Async XLA Ops:
  6.5 130.5 %copy-start = (bf16[256,2048]{1,0:T(8,128)(2,1)S(1)}, bf16[256,2048]{1,0:T(8,128)(2,1)}, u32[]{:S(2)}) copy-start(bf16[256,2048]{1,0:T(8,128)(2,1)} %param.25) | copy-start | bytes 3145732
  6.5 63.8 %copy-start.7 = (f32[2048]{0:T(1024)S(1)}, f32[2048]{0:T(1024)}, u32[]{:S(2)}) copy-start(f32[2048]{0:T(1024)} %param.17) | copy-start | bytes 24580
  6.5 63.8 %copy-start.4 = (bf16[16,2048]{1,0:T(8,128)(2,1)S(1)}, bf16[16,2048]{1,0:T(8,128)(2,1)}, u32[]{:S(2)}) copy-start(bf16[16,2048]{1,0:T(8,128)(2,1)} %param.16) | copy-start | bytes 196612
  6.5 63.8 %copy-start.3 = (bf16[2048,128]{1,0:T(8,128)(2,1)S(1)}, bf16[2048,128]{1,0:T(8,128)(2,1)}, u32[]{:S(2)}) copy-start(bf16[2048,128]{1,0:T(8,128)(2,1)} %param.22) | copy-start | bytes 1572868
  6.5 94.6 %all-gather.2.cloned.1.call-start = ((), (), s32[]{:S(2)}) async-start(), calls=%async_computation.2 | async-start | bytes 3538944 | tf_op jit(solution)/shard_map/all_gather | solution.py:136
  71.5 48.8 %all-to-all-start = ((bf16[64,16,256]{2,1,0:T(8,128)(2,1)}), bf16[64,16,256]{2,1,0:T(8,128)(2,1)S(1)}, u32[]{:S(2)}, u32[]{:S(2)}) async-start(bf16[64,16,256]{2,1,0:T(8,128)(2,1)} %broadcast_in_dim.12), calls=%async_computation | async-start | bytes 1048576 | tf_op jit(solution)/shard_map/all_to_all | solution.py:50
  86.2 18.9 %copy-start.5 = (bf16[2048,128]{1,0:T(8,128)(2,1)S(1)}, bf16[2048,128]{1,0:T(8,128)(2,1)}, u32[]{:S(2)}) copy-start(bf16[2048,128]{1,0:T(8,128)(2,1)} %param.23) | copy-start | bytes 1572868
  105.2 13.1 %copy-start.2 = (bf16[768,2048]{1,0:T(8,128)(2,1)S(1)}, bf16[768,2048]{1,0:T(8,128)(2,1)}, u32[]{:S(2)}) copy-start(bf16[768,2048]{1,0:T(8,128)(2,1)} %all-gather.2.cloned.1.call-done) | copy-start | bytes 9437188
  105.2 13.1 %copy-start.9 = (bf16[2048,256]{1,0:T(8,128)(2,1)S(1)}, bf16[2048,256]{1,0:T(8,128)(2,1)}, u32[]{:S(2)}) copy-start(bf16[2048,256]{1,0:T(8,128)(2,1)} %param.21) | copy-start | bytes 3145732
  108.9 16.4 %collective-permute-start = (bf16[128,256]{1,0:T(8,128)(2,1)}, bf16[128,256]{1,0:T(8,128)(2,1)S(1)}, u32[]{:S(2)}, u32[]{:S(2)}) collective-permute-start(bf16[128,256]{1,0:T(8,128)(2,1)} %get-tuple-element.21), channel_id=1, source_target_pairs={{0,8},{8,16},{16,24},{24,32},{32,40},{40,48},{48,56},{56,64},{64,7... | collective-permute-start | bytes 196616 | tf_op jit(solution)/shard_map/ppermute | solution.py:40
  112.3 13.0 %collective-permute-start.1 = (bf16[128,256]{1,0:T(8,128)(2,1)}, bf16[128,256]{1,0:T(8,128)(2,1)S(1)}, u32[]{:S(2)}, u32[]{:S(2)}) collective-permute-start(bf16[128,256]{1,0:T(8,128)(2,1)} %get-tuple-element.22), channel_id=1, source_target_pairs={{8,0},{16,8},{24,16},{32,24},{40,32},{48,40},{56,48},{64,56},{72,6... | collective-permute-start | bytes 196616 | tf_op jit(solution)/shard_map/ppermute | solution.py:43
  126.5 1.5 copy-start.8
  131.9 0.9 copy-start.6
  131.9 2.3 %slice-start = ((s8[6291456]{0:T(1024)(128)(4,1)}), s8[4194304]{0:T(1024)(128)(4,1)S(1)}, s32[]{:S(2)}) async-start(s8[6291456]{0:T(1024)(128)(4,1)} %bitcast.137), calls=%async_computation.3 | async-start | bytes 8388608
  132.8 2.2 %slice-start.1 = ((s8[6291456]{0:T(1024)(128)(4,1)}), s8[2097152]{0:T(1024)(128)(4,1)S(1)}, s32[]{:S(2)}) async-start(s8[6291456]{0:T(1024)(128)(4,1)} %bitcast.137), calls=%async_computation.4 | async-start | bytes 4194304
  179.2 1.0 copy-start.1
Sparse Core Ops, SparseCore 0:
  68.2 32.9 all-gather.1
where the time goes:
time: 189 us; the launch traced here: 188 us
  blocking collectives  96.1 us (51%)
  starting transfers between devices  21.6 us (11%)
  matrix products  19.7 us (10%)
  other arithmetic  15.8 us (8%)
  waiting for transfers between devices  15 us (8%)
  between operations  13.8 us (7%)
  local copies, waits for them, and re-layouts  5.96 us (3%)
    psum x2, blocking collectives, one_axis_at_a_time(): return functools.reduce(lax.psum, axes, x)  41.8 us
    all_to_all x1, blocking collectives, summed_on_arrival(): blocks = lax.all_to_all(in_blocks(x, dim, peers), axis, 0, 0, tiled=True)  41.2 us
    all_gather x1, waiting for transfers between devices, shards(): block_rows = lax.all_gather(hidden_state, 'tp', axis=0, tiled=True)  14.9 us
    all_gather x1, blocking collectives, side_by_side(): out, at, outs = (lax.all_gather(both, axis, axis=dim, tiled=True), 0, [])  13.1 us
    all_to_all x1, starting transfers between devices, sent_to_all(): lax.all_to_all(jnp.broadcast_to(x[None], (peers, *x.shape)), axis, 0, 0,...  12.3 us
    ppermute x1, starting transfers between devices, padded_2(): lax.ppermute(lax.slice_in_dim(block, 0, width, axis=dim), axis, backward)  5.93 us
    reduce_sum x1, other arithmetic, shards(): jnp.sum(ctx_exp, axis=-1, keepdims=True)  3.82 us
  transfers between devices with their start and end apart: 4, of which 1 were waited for; matrix products, arithmetic and copies ran while one was open for 11% of the time, Pallas kernels for 0%

commit v1 on v0

v1 whole, which is shorter than its diff:
```python
import jax
import jax.numpy as jnp
from jax import lax
from jax.sharding import Mesh
from jax.sharding import PartitionSpec as P

QUERY_HEADS = 16
KEY_VALUE_HEADS = 8
HEAD_DIM = 128
WINDOW_REACH = 128
GRID_W = 64
SP = ("z", "y")
TP = ("x", "c")
PLANE = ("y", "x", "c")
ALL = ("z", "y", "x", "c")

NORM_EPS = 1e-05
MASKED_SCORE = -1e30


def sent_to_all(x, axis):
    peers = lax.axis_size(axis)
    return lax.all_to_all(jnp.broadcast_to(x[None], (peers, *x.shape)), axis, 0, 0, tiled=True)


def padded_2(block, axis, width):
    count = lax.axis_size(axis)
    forward = [(i, i + 1) for i in range(count - 1)]
    backward = [(target, source) for source, target in forward]
    low = lax.ppermute(block[block.shape[0] - width :], axis, forward)
    high = lax.ppermute(block[:width], axis, backward)
    return jnp.concatenate([low, block, high], axis=0)


def rotate(vectors, position):
    quarter = HEAD_DIM // 4
    grid_row = (position // GRID_W).astype(jnp.float32)
    grid_col = (position % GRID_W).astype(jnp.float32)
    inv_freq = 10000.0 ** (-jnp.arange(0, HEAD_DIM // 2, 2, dtype=jnp.float32) / (HEAD_DIM // 2))
    angles = jnp.concatenate([grid_row[:, None] * inv_freq, grid_col[:, None] * inv_freq], axis=-1)
    cosine_table = jnp.cos(angles).reshape(-1, 1, 2, quarter)
    sine_table = jnp.sin(angles).reshape(-1, 1, 2, quarter)
    pieces = vectors.reshape(vectors.shape[0], vectors.shape[1], 2, 2, quarter)
    first_half = pieces[..., 0, :]
    second_half = pieces[..., 1, :]
    turned = jnp.stack(
        [
            first_half * cosine_table - second_half * sine_table,
            first_half * sine_table + second_half * cosine_table,
        ],
        axis=-2,
    )
    return turned.reshape(vectors.shape)


def modulated_norm(rows_in, norm_gain, shift, scale):
    floats = rows_in.astype(jnp.float32)
    normed = (
        floats * lax.rsqrt(jnp.mean(floats * floats, axis=-1, keepdims=True) + NORM_EPS) * norm_gain
    )
    return (normed * (1.0 + scale) + shift).astype(jnp.bfloat16)


def shards(
    latent,
    condition,
    context_condition,
    context,
    norm_gain,
    shift_weight,
    scale_weight,
    gate_weight,
    query_weight,
    key_matrix,
    value_matrix,
    sink_logit_head,
    out_weight,
):
    nz, ny, nx, nc = (lax.axis_size(a) for a in ALL)
    rows, width = latent.shape
    group_rows = rows * nx * nc
    offset = lax.axis_index(SP) * group_rows
    total_rows = group_rows * nz * ny
    latent_x = sent_to_all(latent, "x")
    active = jax.nn.silu(jnp.stack([condition, context_condition])).astype(jnp.bfloat16)
    shift_part = jnp.dot(active, shift_weight, preferred_element_type=jnp.float32)
    scale_part = jnp.dot(active, scale_weight, preferred_element_type=jnp.float32)
    gate_part = jnp.dot(active[:1], gate_weight, preferred_element_type=jnp.float32)
    parts = jnp.concatenate([shift_part, scale_part, gate_part], axis=0)
    columns = parts.shape[1]
    coarse = parts.astype(jnp.bfloat16)
    fine = (parts - coarse.astype(jnp.float32)).astype(jnp.bfloat16)
    share = context.shape[0] // (nx * nc)
    mine = lax.dynamic_slice_in_dim(context, lax.axis_index(TP) * share, share, 0)
    mine = mine.reshape(-1, columns)
    sent = jnp.concatenate([mine, coarse, fine], axis=0)
    got = sent_to_all(sent, "z")
    ctx_z = got[:, : mine.shape[0]].reshape(nz * share, width)
    halves = got[:, mine.shape[0] :].astype(jnp.float32)
    z_sum = jnp.sum(halves[:, :5] + halves[:, 5:], axis=0)
    planes = sent_to_all(z_sum.reshape(1, -1), PLANE)
    ctx_x = sent_to_all(ctx_z, "x")
    latent_all = sent_to_all(latent_x, "c").reshape(nc, nx, rows, width)
    ctx_all = sent_to_all(ctx_x.reshape(-1, width), "c").reshape(-1, width)
    mods = jnp.sum(planes.reshape(ny, nx * nc, 5, columns), axis=0)
    mods = jnp.moveaxis(mods, 0, 1).reshape(5, width)
    shift, ctx_shift, scale, ctx_scale, gate = (mods[i] for i in range(5))
    ctx_hidden = modulated_norm(ctx_all, norm_gain, ctx_shift, ctx_scale)
    ctx_pairs = sent_to_all(
        jnp.concatenate(
            [
                jnp.dot(ctx_hidden, key_matrix, preferred_element_type=jnp.float32),
                jnp.dot(ctx_hidden, value_matrix, preferred_element_type=jnp.float32),
            ],
            axis=1,
        ).astype(jnp.bfloat16),
        "y",
    )
    ctx_pairs = ctx_pairs.reshape(-1, ctx_pairs.shape[-1])
    query_width = query_weight.shape[1]
    pair_width = key_matrix.shape[1]
    block_rows = modulated_norm(latent_all, norm_gain, shift, scale).reshape(group_rows, width)
    position = (
        offset
        + jnp.arange(nc, dtype=jnp.int32)[:, None, None] * rows
        + jnp.arange(nx, dtype=jnp.int32)[None, :, None] * (rows * nc)
        + jnp.arange(rows, dtype=jnp.int32)[None, None, :]
    ).reshape(-1)
    query_rows = jnp.dot(block_rows, query_weight, preferred_element_type=jnp.float32)
    query_rows = rotate(query_rows.reshape(group_rows, -1, HEAD_DIM), position)
    key_rows = jnp.dot(block_rows, key_matrix, preferred_element_type=jnp.float32)
    key_rows = rotate(key_rows.reshape(group_rows, -1, HEAD_DIM), position)
    value_rows = jnp.dot(block_rows, value_matrix, preferred_element_type=jnp.float32)
    projected = jnp.concatenate(
        [
            query_rows.reshape(group_rows, query_width),
            key_rows.reshape(group_rows, pair_width),
            value_rows,
        ],
        axis=1,
    ).astype(jnp.bfloat16)
    projected = jnp.swapaxes(projected.reshape(nc, nx, rows, -1), 0, 1).reshape(group_rows, -1)
    padded = padded_2(projected[:, query_width:], SP, WINDOW_REACH)
    blocks = group_rows // WINDOW_REACH
    kv_local = pair_width // HEAD_DIM
    queries_per_group = QUERY_HEADS // KEY_VALUE_HEADS
    query_blocks = projected[:, :query_width].reshape(
        blocks, WINDOW_REACH, kv_local, queries_per_group, HEAD_DIM
    )
    key_pad = padded[:, :pair_width].reshape(blocks + 2, WINDOW_REACH, kv_local, HEAD_DIM)
    value_pad = padded[:, pair_width:].reshape(blocks + 2, WINDOW_REACH, kv_local, HEAD_DIM)
    band_keys = jnp.concatenate([key_pad[:-2], key_pad[1:-1], key_pad[2:]], axis=1)
    band_values = jnp.concatenate([value_pad[:-2], value_pad[1:-1], value_pad[2:]], axis=1)
    context_key_rows = ctx_pairs[:, :pair_width].reshape(-1, kv_local, HEAD_DIM)
    context_value_rows = ctx_pairs[:, pair_width:].reshape(-1, kv_local, HEAD_DIM)
    factor = HEAD_DIM ** (-0.5)
    band_scores = (
        jnp.einsum("nqhgd,nkhd->nhgqk", query_blocks, band_keys, preferred_element_type=jnp.float32)
        * factor
    )
    block_ids = jnp.arange(blocks, dtype=jnp.int32)[:, None, None]
    query_pos = (
        offset + block_ids * WINDOW_REACH + jnp.arange(WINDOW_REACH, dtype=jnp.int32)[None, :, None]
    )
    key_pos = (
        offset
        + (block_ids - 1) * WINDOW_REACH
        + jnp.arange(3 * WINDOW_REACH, dtype=jnp.int32)[None, None, :]
    )
    allowed = (
        (jnp.abs(key_pos - query_pos) <= WINDOW_REACH) & (key_pos >= 0) & (key_pos < total_rows)
    )
    band_scores = jnp.where(allowed[:, None, None], band_scores, MASKED_SCORE)
    ctx_scores = (
        jnp.einsum(
            "nqhgd,chd->nhgqc", query_blocks, context_key_rows, preferred_element_type=jnp.float32
        )
        * factor
    )
    sink_logit_rows = sink_logit_head.reshape(1, kv_local, queries_per_group, 1, 1)
    maxima = jnp.maximum(
        jnp.maximum(
            jnp.max(band_scores, axis=-1, keepdims=True),
            jnp.max(ctx_scores, axis=-1, keepdims=True),
        ),
        sink_logit_rows,
    )
    band_exp = jnp.exp(band_scores - maxima)
    ctx_exp = jnp.exp(ctx_scores - maxima)
    denominator = (
        jnp.sum(band_exp, axis=-1, keepdims=True)
        + jnp.sum(ctx_exp, axis=-1, keepdims=True)
        + jnp.exp(sink_logit_rows - maxima)
    )
    band_weights = (band_exp / denominator).astype(jnp.bfloat16)
    ctx_weights = (ctx_exp / denominator).astype(jnp.bfloat16)
    attended = jnp.einsum(
        "nhgqk,nkhd->nqhgd", band_weights, band_values, preferred_element_type=jnp.float32
    ) + jnp.einsum(
        "nhgqc,chd->nqhgd", ctx_weights, context_value_rows, preferred_element_type=jnp.float32
    )
    attended = attended.astype(jnp.bfloat16).reshape(nx, nc, rows, query_width)
    attended = jnp.swapaxes(attended, 0, 1).reshape(group_rows, query_width)
    partial = jnp.dot(attended, out_weight, preferred_element_type=jnp.float32)
    partial = partial.astype(jnp.bfloat16).reshape(nc, nx * rows, width)
    pair = lax.all_to_all(partial, "c", 0, 0, tiled=True)
    pair = jnp.sum(pair.astype(jnp.float32), axis=0).astype(jnp.bfloat16)
    mixed = lax.all_to_all(pair.reshape(nx, rows, width), "x", 0, 0, tiled=True)
    mixed = jnp.sum(mixed.astype(jnp.float32), axis=0)
    return (latent.astype(jnp.float32) + gate * mixed).astype(jnp.bfloat16)


def solution(mesh):
    torus = Mesh(mesh.devices.reshape(16, 4, 4, 2), ALL)
    return jax.shard_map(
        shards,
        mesh=torus,
        in_specs=(
            P(ALL, None),
            P(SP),
            P(SP),
            P(SP, None),
            P(),
            P(SP, TP),
            P(SP, TP),
            P(SP, TP),
            P(None, TP),
            P(None, TP),
            P(None, TP),
            P(TP),
            P(TP, None),
        ),
        out_specs=P(ALL, None),
        check_vma=False,
    )
```

time: 189 us -> 193 us (1.021)
  the two profiles are of different devices: /device:TPU:128 before, /device:TPU:32 now
where the time goes in v1:
time: 193 us; the launch traced here: 192 us
  waiting for transfers between devices  61.4 us (32%)
  starting transfers between devices  47.2 us (24%)
  local copies, waits for them, and re-layouts  22.6 us (12%)
  other arithmetic  22.3 us (12%)
  blocking collectives  19.4 us (10%)
  matrix products  18.9 us (10%)
    all_to_all x5, waiting for transfers between devices, sent_to_all(): lax.all_to_all(jnp.broadcast_to(x[None], (peers, *x.shape)), axis, 0, 0,...  40.4 us
    all_to_all x5, starting transfers between devices, sent_to_all(): lax.all_to_all(jnp.broadcast_to(x[None], (peers, *x.shape)), axis, 0, 0,...  34.4 us
    all_to_all x1, waiting for transfers between devices, shards(): mixed = lax.all_to_all(pair.reshape(nx, rows, width), 'x', 0, 0, tiled=True)  21 us
    all_to_all x2, blocking collectives, sent_to_all(): lax.all_to_all(jnp.broadcast_to(x[None], (peers, *x.shape)), axis, 0, 0,...  12.1 us
    all_to_all x1, blocking collectives, shards(): pair = lax.all_to_all(partial, 'c', 0, 0, tiled=True)  7.24 us
    broadcast_in_dim x9, local copies, waits for them, and re-layouts, sent_to_all(): jnp.broadcast_to(x[None], (peers, *x.shape))  7.04 us
    ppermute x1, starting transfers between devices, padded_2(): high = lax.ppermute(block[:width], axis, backward)  5.43 us
    all_to_all x1, starting transfers between devices, shards(): mixed = lax.all_to_all(pair.reshape(nx, rows, width), 'x', 0, 0, tiled=True)  4.87 us
  transfers between devices with their start and end apart: 8, of which 5 were waited for; matrix products, arithmetic and copies ran while one was open for 21% of the time, Pallas kernels for 0%

profile of v1, /device:TPU:32, one launch (start us, length us, event | category | flops | bytes accessed | tf_op | source)
XLA Modules:
  0.0 192.3 jit_solution(1076376398341799624)
XLA Ops:
  4.9 15.2 %all-to-all-start = ((bf16[16,26,256]{2,1,0:T(8,128)(2,1)}), bf16[16,26,256]{2,1,0:T(8,128)(2,1)S(1)}, u32[]{:S(2)}, u32[]{:S(2)}) async-start(bf16[16,26,256]{2,1,0:T(8,128)(2,1)} %broadcast_in_dim.28), calls=%async_computation | async-start | bytes 524288 | tf_op jit(solution)/shard_map/all_to_all | solution.py:23
  20.4 17.6 %all-to-all-done = bf16[16,26,256]{2,1,0:T(8,128)(2,1)S(1)} async-done(((bf16[16,26,256]{2,1,0:T(8,128)(2,1)}), bf16[16,26,256]{2,1,0:T(8,128)(2,1)S(1)}, u32[]{:S(2)}, u32[]{:S(2)}) %all-to-all-start) | async-done | bytes 213024 | tf_op jit(solution)/shard_map/all_to_all | solution.py:23
  38.8 7.3 %all-to-all-start.1 = ((f32[32,1,1280]{2,1,0:T(1,128)}), f32[32,1,1280]{2,1,0:T(1,128)S(1)}, u32[]{:S(2)}, u32[]{:S(2)}) async-start(f32[32,1,1280]{2,1,0:T(1,128)} %broadcast_in_dim.30), calls=%async_computation.1 | async-start | bytes 327680 | tf_op jit(solution)/shard_map/all_to_all | solution.py:23
  48.4 5.8 %all-to-all-done.1 = f32[32,1,1280]{2,1,0:T(1,128)S(1)} async-done(((f32[32,1,1280]{2,1,0:T(1,128)}), f32[32,1,1280]{2,1,0:T(1,128)S(1)}, u32[]{:S(2)}, u32[]{:S(2)}) %all-to-all-start.1) | async-done | bytes 163872 | tf_op jit(solution)/shard_map/all_to_all | solution.py:23
  55.5 3.6 %all-to-all-start.2 = ((bf16[4,96,2048]{2,1,0:T(8,128)(2,1)}), bf16[4,96,2048]{2,1,0:T(8,128)(2,1)S(1)}, u32[]{:S(2)}, u32[]{:S(2)}) async-start(bf16[4,96,2048]{2,1,0:T(8,128)(2,1)} %broadcast_in_dim.31), calls=%async_computation.2 | async-start | bytes 3145728 | tf_op jit(solution)/shard_map/all_to_all | solution.py:23
  60.1 2.3 %copy.70 = bf16[2048,256]{0,1:T(8,128)(2,1)} copy(bf16[2048,256]{1,0:T(8,128)(2,1)} %param.21) | data formatting | bytes 2097152 | tf_op args[8]
  62.6 2.8 %fusion.27 = pred[6,128,384]{1,2,0:T(8,128)(4,1)} fusion(s32[6,128]{1,0:T(8,128)S(1)} %iota_add_fusion.1, s32[6,384]{1,0:T(8,128)S(1)} %iota_add_fusion, pred[6,384]{1,0:T(8,128)(4,1)S(1)} %get-tuple-element.35, pred[6,384]{1,0:T(8,128)(4,1)S(1)} %get-tuple-element.34), kind=kLoop, calls=%fused_computation.36 | loop fusion | flops 1474560 | bytes 311808 | tf_op jit(solution)/shard_map/and | solution.py:171
  69.2 11.3 %all-to-all-done.2 = bf16[4,96,2048]{2,1,0:T(8,128)(2,1)S(1)} async-done(((bf16[4,96,2048]{2,1,0:T(8,128)(2,1)}), bf16[4,96,2048]{2,1,0:T(8,128)(2,1)S(1)}, u32[]{:S(2)}, u32[]{:S(2)}) %all-to-all-start.2) | async-done | bytes 1572896 | tf_op jit(solution)/shard_map/all_to_all | solution.py:23
  80.8 7.2 %all_to_all.45 = bf16[2,4,96,2048]{3,2,1,0:T(8,128)(2,1)} all-to-all(bf16[2,4,96,2048]{3,2,1,0:T(8,128)(2,1)S(1)} %broadcast_in_dim.32), channel_id=1, replica_groups=mesh['z'=16,'y'=4,'x'=4,'c'=2] {'c'}, dimensions={0} | all-to-all | bytes 6291456 | tf_op jit(solution)/shard_map/all_to_all | solution.py:23
  88.9 4.1 %all-to-all-start.4 = ((bf16[4,32,2048]{2,1,0:T(8,128)(2,1)}), bf16[4,32,2048]{2,1,0:T(8,128)(2,1)}, u32[]{:S(2)}, u32[]{:S(2)}) async-start(bf16[4,32,2048]{2,1,0:T(8,128)(2,1)} %broadcast_in_dim.36), calls=%async_computation.4 | async-start | bytes 1048576 | tf_op jit(solution)/shard_map/all_to_all | solution.py:23
  93.1 2.7 %fusion = f32[2,4,96]{2,1,0:T(4,128)S(1)} fusion(bf16[2,4,96,2048]{3,2,1,0:T(8,128)(2,1)} %all_to_all.45), kind=kLoop, calls=%fused_computation.2 | loop fusion | flops 4717824 | bytes 3148800 | tf_op jit(solution)/shard_map/reduce_sum | solution.py:59
  100.6 3.0 %fusion.72 = f32[768,2,2,2,32]{0,4,3,2,1:T(8,128)S(1)} fusion(bf16[768,2048,1,1,1]{1,0,4,3,2:T(8,128)(2,1)} %bitcast.190, bf16[2,2,2,32,2048]{4,3,2,1,0:T(8,128)(2,1)S(1)} %bitcast.193), kind=kOutput, calls=%fused_computation.137 | convolution fusion | flops 805306368 | bytes 4980736 | tf_op jit(solution)/shard_map/dot_general | solution.py:129
  104.3 3.0 %convolution_convert_fusion.1 = bf16[2,4,96,128]{3,2,1,0:T(8,128)(2,1)S(1)} fusion(bf16[2,4,96,2048]{3,2,1,0:T(8,128)(2,1)} %copy-done.2, bf16[2048,128]{1,0:T(8,128)(2,1)} %param.23), kind=kOutput, calls=%fused_computation.38 | convolution fusion | flops 402751488 | bytes 3866624 | tf_op jit(solution)/shard_map/dot_general | solution.py:133
  111.0 2.5 %collective-permute-start = (bf16[128,256]{1,0:T(8,128)(2,1)S(1)}, bf16[128,256]{1,0:T(8,128)(2,1)S(1)}, u32[]{:S(2)}, u32[]{:S(2)}) collective-permute-start(bf16[128,256]{1,0:T(8,128)(2,1)S(1)} %get-tuple-element.11), channel_id=1, source_target_pairs={{0,8},{8,16},{16,24},{24,32},{32,40},{40,48},{48,56},{56,64},{64,7... | collective-permute-start | bytes 196616 | tf_op jit(solution)/shard_map/ppermute | solution.py:30
  113.5 5.4 %collective-permute-start.1 = (bf16[128,256]{1,0:T(8,128)(2,1)S(1)}, bf16[128,256]{1,0:T(8,128)(2,1)S(1)}, u32[]{:S(2)}, u32[]{:S(2)}) collective-permute-start(bf16[128,256]{1,0:T(8,128)(2,1)S(1)} %get-tuple-element.12), channel_id=1, source_target_pairs={{8,0},{16,8},{24,16},{32,24},{40,32},{48,40},{56,48},{64,56},{72,6... | collective-permute-start | bytes 196616 | tf_op jit(solution)/shard_map/ppermute | solution.py:31
  122.6 4.9 %all_to_all.46 = bf16[2,128,2048]{2,1,0:T(8,128)(2,1)S(1)} all-to-all(bf16[2,128,2048]{2,1,0:T(8,128)(2,1)S(1)} %broadcast_in_dim.38), channel_id=1, replica_groups=mesh['z'=16,'y'=4,'x'=4,'c'=2] {'c'}, dimensions={0} | all-to-all | bytes 2097152 | tf_op jit(solution)/shard_map/all_to_all | solution.py:23
  130.2 4.1 %all-to-all-start.6 = ((bf16[4,256,256]{2,1,0:T(8,128)(2,1)}), bf16[4,256,256]{2,1,0:T(8,128)(2,1)}, u32[]{:S(2)}, u32[]{:S(2)}) async-start(bf16[4,256,256]{2,1,0:T(8,128)(2,1)} %broadcast_in_dim.39), calls=%async_computation.6 | async-start | bytes 1048576 | tf_op jit(solution)/shard_map/all_to_all | solution.py:23
  138.8 5.7 %all-to-all-done.6 = bf16[4,256,256]{2,1,0:T(8,128)(2,1)} async-done(((bf16[4,256,256]{2,1,0:T(8,128)(2,1)}), bf16[4,256,256]{2,1,0:T(8,128)(2,1)}, u32[]{:S(2)}, u32[]{:S(2)}) %all-to-all-start.6) | async-done | bytes 524320 | tf_op jit(solution)/shard_map/all_to_all | solution.py:23
  144.5 2.1 %bitcast_reduce_fusion = (f32[6,2,128]{2,1,0:T(2,128)S(1)}, f32[1024,6,128,2]{2,0,3,1:T(8,128)S(1)}) fusion(bf16[6,128,2,128]{3,2,1,0:T(2,128)(2,1)} %reshape.699, bf16[1024,256]{1,0:T(8,128)(2,1)} %bitcast.40), kind=kOutput, calls=%fused_computation.8 | convolution fusion | flops 405797376 | bytes 6952960 | tf_op jit(solution)/shard_map/nqhgd,chd->nhgqc/dot_general | solution.py:175
  149.6 2.4 %fusion.22 = bf16[6,128,1,2,128]{1,4,3,0,2:T(8,128)(2,1)S(1)} fusion(f32[6,128,1,2,128]{1,4,3,0,2:T(8,128)S(1)} %convolution_bitcast_fusion, f32[6,2,128]{2,1,0:T(2,128)S(1)} %exponential_add_fusion, f32[6,2,128]{2,1,0:T(2,128)S(1)} %maximum_maximum_fusion, f32[1024,6,128,2]{2,0,3,1:T(8,128)S(1)} %get-tuple-element.41, bf16[1024,256]{1,0:T(8,128)(2,1)} %bitcast.40), kind=kOutput, calls=%fused_computation.31 | convolution fusion | flops 409337856 | bytes 7745536 | tf_op jit(solution)/shard_map/nhgqc,chd->nqhgd/dot_general | solution.py:199
  153.8 7.2 %all_to_all.47 = bf16[2,384,2048]{2,1,0:T(8,128)(2,1)} all-to-all(bf16[2,384,2048]{2,1,0:T(8,128)(2,1)S(1)} %bitcast.184), channel_id=1, replica_groups=mesh['z'=16,'y'=4,'x'=4,'c'=2] {'c'}, dimensions={0} | all-to-all | bytes 6291456 | tf_op jit(solution)/shard_map/all_to_all | solution.py:206
  161.0 4.2 %reduce_sum.81 = bf16[384,2048]{1,0:T(8,128)(2,1)} reduce(bf16[2,384,2048]{2,1,0:T(8,128)(2,1)} %all_to_all.47, bf16[]{:T(256)} %constant.100.clone.1), dimensions={0}, to_apply=%region_8.9 | reduce | flops 786432 | bytes 4718594 | tf_op jit(solution)/shard_map/reduce_sum | solution.py:207
  165.3 4.9 %all-to-all-start.8 = ((bf16[4,96,2048]{2,1,0:T(8,128)(2,1)}), bf16[4,96,2048]{2,1,0:T(8,128)(2,1)S(1)}, u32[]{:S(2)}, u32[]{:S(2)}) async-start(bf16[4,96,2048]{2,1,0:T(8,128)(2,1)} %bitcast.185), calls=%async_computation.8 | async-start | bytes 3145728 | tf_op jit(solution)/shard_map/all_to_all | solution.py:208
  170.1 21.0 %all-to-all-done.8 = bf16[4,96,2048]{2,1,0:T(8,128)(2,1)S(1)} async-done(((bf16[4,96,2048]{2,1,0:T(8,128)(2,1)}), bf16[4,96,2048]{2,1,0:T(8,128)(2,1)S(1)}, u32[]{:S(2)}, u32[]{:S(2)}) %all-to-all-start.8) | async-done | bytes 1572896 | tf_op jit(solution)/shard_map/all_to_all | solution.py:208
  (131 shorter events, 41.4 us)
Async XLA Ops:
  0.0 152.8 %copy-start = (bf16[256,2048]{1,0:T(8,128)(2,1)S(1)}, bf16[256,2048]{1,0:T(8,128)(2,1)}, u32[]{:S(2)}) copy-start(bf16[256,2048]{1,0:T(8,128)(2,1)} %param.25) | copy-start | bytes 3145732
  0.0 54.2 %copy-start.4 = (bf16[96,2048]{1,0:T(8,128)(2,1)S(1)}, bf16[96,2048]{1,0:T(8,128)(2,1)}, u32[]{:S(2)}) copy-start(bf16[96,2048]{1,0:T(8,128)(2,1)} %param.13) | copy-start | bytes 1179652
  4.9 33.1 %all-to-all-start = ((bf16[16,26,256]{2,1,0:T(8,128)(2,1)}), bf16[16,26,256]{2,1,0:T(8,128)(2,1)S(1)}, u32[]{:S(2)}, u32[]{:S(2)}) async-start(bf16[16,26,256]{2,1,0:T(8,128)(2,1)} %broadcast_in_dim.28), calls=%async_computation | async-start | bytes 524288 | tf_op jit(solution)/shard_map/all_to_all | solution.py:23
  38.8 15.3 %all-to-all-start.1 = ((f32[32,1,1280]{2,1,0:T(1,128)}), f32[32,1,1280]{2,1,0:T(1,128)S(1)}, u32[]{:S(2)}, u32[]{:S(2)}) async-start(f32[32,1,1280]{2,1,0:T(1,128)} %broadcast_in_dim.30), calls=%async_computation.1 | async-start | bytes 327680 | tf_op jit(solution)/shard_map/all_to_all | solution.py:23
  48.4 10.8 %copy-start.3 = (bf16[2048,128]{1,0:T(8,128)(2,1)S(1)}, bf16[2048,128]{1,0:T(8,128)(2,1)}, u32[]{:S(2)}) copy-start(bf16[2048,128]{1,0:T(8,128)(2,1)} %param.22) | copy-start | bytes 1572868
  55.5 24.9 %all-to-all-start.2 = ((bf16[4,96,2048]{2,1,0:T(8,128)(2,1)}), bf16[4,96,2048]{2,1,0:T(8,128)(2,1)S(1)}, u32[]{:S(2)}, u32[]{:S(2)}) async-start(bf16[4,96,2048]{2,1,0:T(8,128)(2,1)} %broadcast_in_dim.31), calls=%async_computation.2 | async-start | bytes 3145728 | tf_op jit(solution)/shard_map/all_to_all | solution.py:23
  88.0 7.8 %copy-start.19 = (f32[2048]{0:T(1024)S(1)}, f32[2048]{0:T(1024)}, u32[]{:S(2)}) copy-start(f32[2048]{0:T(1024)} %param.17) | copy-start | bytes 24580
  88.9 32.5 %all-to-all-start.4 = ((bf16[4,32,2048]{2,1,0:T(8,128)(2,1)}), bf16[4,32,2048]{2,1,0:T(8,128)(2,1)}, u32[]{:S(2)}, u32[]{:S(2)}) async-start(bf16[4,32,2048]{2,1,0:T(8,128)(2,1)} %broadcast_in_dim.36), calls=%async_computation.4 | async-start | bytes 1048576 | tf_op jit(solution)/shard_map/all_to_all | solution.py:23
  93.1 2.8 %copy-start.1 = (bf16[2,4,96,2048]{3,2,1,0:T(8,128)(2,1)S(1)}, bf16[2,4,96,2048]{3,2,1,0:T(8,128)(2,1)}, u32[]{:S(2)}) copy-start(bf16[2,4,96,2048]{3,2,1,0:T(8,128)(2,1)} %all_to_all.45) | copy-start | bytes 9437188
  97.1 1.7 copy-start.2
  97.2 1.6 copy-start.14
  97.2 3.4 %copy-start.7 = (bf16[2048,256]{0,1:T(8,128)(2,1)S(1)}, bf16[2048,256]{0,1:T(8,128)(2,1)}, u32[]{:S(2)}) copy-start(bf16[2048,256]{0,1:T(8,128)(2,1)} %copy.70) | copy-start | bytes 3145732
  100.6 3.0 %copy-start.9 = (f32[768,2,32]{0,2,1:T(8,128)S(1)}, f32[768,2,32]{0,2,1:T(8,128)}, u32[]{:S(2)}) copy-start(f32[768,2,32]{0,2,1:T(8,128)} %get-tuple-element.21) | copy-start | bytes 589828
  100.6 3.0 %copy-start.10 = (f32[768,2,32]{0,2,1:T(8,128)S(1)}, f32[768,2,32]{0,2,1:T(8,128)}, u32[]{:S(2)}) copy-start(f32[768,2,32]{0,2,1:T(8,128)} %get-tuple-element.22) | copy-start | bytes 589828
  104.3 3.9 %copy-start.8 = (bf16[2,4,96,128]{2,1,0,3:T(4,128)(2,1)S(1)}, bf16[2,4,96,128]{2,1,0,3:T(4,128)(2,1)}, u32[]{:S(2)}) copy-start(bf16[2,4,96,128]{2,1,0,3:T(4,128)(2,1)} %concatenate.85) | copy-start | bytes 589828
  111.0 23.3 %collective-permute-start = (bf16[128,256]{1,0:T(8,128)(2,1)S(1)}, bf16[128,256]{1,0:T(8,128)(2,1)S(1)}, u32[]{:S(2)}, u32[]{:S(2)}) collective-permute-start(bf16[128,256]{1,0:T(8,128)(2,1)S(1)} %get-tuple-element.11), channel_id=1, source_target_pairs={{0,8},{8,16},{16,24},{24,32},{32,40},{40,48},{48,56},{56,64},{64,7... | collective-permute-start | bytes 196616 | tf_op jit(solution)/shard_map/ppermute | solution.py:30
  113.5 20.8 %collective-permute-start.1 = (bf16[128,256]{1,0:T(8,128)(2,1)S(1)}, bf16[128,256]{1,0:T(8,128)(2,1)S(1)}, u32[]{:S(2)}, u32[]{:S(2)}) collective-permute-start(bf16[128,256]{1,0:T(8,128)(2,1)S(1)} %get-tuple-element.12), channel_id=1, source_target_pairs={{8,0},{16,8},{24,16},{32,24},{40,32},{48,40},{56,48},{64,56},{72,6... | collective-permute-start | bytes 196616 | tf_op jit(solution)/shard_map/ppermute | solution.py:31
  121.4 6.4 %copy-start.20 = (f32[1,2,8,128]{3,1,2,0:T(2,128)S(1)}, f32[1,2,8,128]{3,1,2,0:T(2,128)}, u32[]{:S(2)}) copy-start(f32[1,2,8,128]{3,1,2,0:T(2,128)} %copy.99) | copy-start | bytes 24580
  122.6 5.7 %copy-start.12 = (bf16[2048,128]{1,0:T(8,128)(2,1)S(1)}, bf16[2048,128]{1,0:T(8,128)(2,1)}, u32[]{:S(2)}) copy-start(bf16[2048,128]{1,0:T(8,128)(2,1)} %param.23) | copy-start | bytes 1572868
  130.2 14.3 %all-to-all-start.6 = ((bf16[4,256,256]{2,1,0:T(8,128)(2,1)}), bf16[4,256,256]{2,1,0:T(8,128)(2,1)}, u32[]{:S(2)}, u32[]{:S(2)}) async-start(bf16[4,256,256]{2,1,0:T(8,128)(2,1)} %broadcast_in_dim.39), calls=%async_computation.6 | async-start | bytes 1048576 | tf_op jit(solution)/shard_map/all_to_all | solution.py:23
  144.5 2.1 %copy-start.22 = (f32[2]{0:T(128)S(1)}, f32[2]{0:T(128)}, u32[]{:S(2)}) copy-start(f32[2]{0:T(128)} %param.24) | copy-start | bytes 28
  165.3 4.9 %copy-start.21 = (f32[1,2,8,128]{3,2,1,0:T(8,128)S(1)}, f32[1,2,8,128]{3,2,1,0:T(8,128)}, u32[]{:S(2)}) copy-start(f32[1,2,8,128]{3,2,1,0:T(8,128)} %get-tuple-element.23) | copy-start | bytes 24580
  165.3 26.2 %copy-start.5 = (bf16[96,2048]{1,0:T(8,128)(2,1)S(1)}, bf16[96,2048]{1,0:T(8,128)(2,1)}, u32[]{:S(2)}) copy-start(bf16[96,2048]{1,0:T(8,128)(2,1)} %param.13) | copy-start | bytes 1179652
  165.3 25.9 %all-to-all-start.8 = ((bf16[4,96,2048]{2,1,0:T(8,128)(2,1)}), bf16[4,96,2048]{2,1,0:T(8,128)(2,1)S(1)}, u32[]{:S(2)}, u32[]{:S(2)}) async-start(bf16[4,96,2048]{2,1,0:T(8,128)(2,1)} %bitcast.185), calls=%async_computation.8 | async-start | bytes 3145728 | tf_op jit(solution)/shard_map/all_to_all | solution.py:208
  (7 other events, 8.4 us)

commit v2 on v1

v2 whole, which is shorter than its diff:
```python
import jax
import jax.numpy as jnp
from jax import lax
from jax.experimental import pallas as pl
from jax.experimental.pallas import tpu as pltpu
from jax.sharding import Mesh
from jax.sharding import PartitionSpec as P

HEAD_DIM = 128
WINDOW_REACH = 128
GRID_W = 64
SP = ("z", "y")
TP = ("x", "c")
PLANE = ("y", "x", "c")
ALL = ("z", "y", "x", "c")
NORM_EPS = 1e-05
MASKED_SCORE = -1e30
LOG2_E = 1.4426950408889634
CHUNK = 16


VMEM = pl.BlockSpec(memory_space=pltpu.VMEM)
SMEM = pl.BlockSpec(memory_space=pltpu.SMEM)
F32 = jnp.float32
BF16 = jnp.bfloat16


def shape_of(shape, dtype):
    return jax.ShapeDtypeStruct(shape, dtype)


def copies(x, axis):
    return jnp.broadcast_to(x[None], (lax.axis_size(axis), *x.shape))


def exchanged(blocks, axis):
    return lax.all_to_all(blocks, axis, 0, 0, tiled=True)


def dot(a, b):
    return jnp.dot(a, b, preferred_element_type=F32)


def row_vector(planes_ref, index, columns):
    count = planes_ref.shape[0] // 4
    cut = pl.ds(index * columns, columns)
    pieces = []
    for t in range(count):
        piece = planes_ref[t, :, cut]
        for y in range(1, 4):
            piece = piece + planes_ref[y * count + t, :, cut]
        pieces.append(piece)
    return jnp.concatenate(pieces, axis=1)


def parts_kernel(
    member_ref, cond_ref, ctx_cond_ref, shift_ref, scale_ref, gate_ref, ctx_ref, out_ref
):
    def active(ref):
        v = ref[...]
        return (v / (1.0 + jnp.exp(-v))).astype(BF16)

    both = jnp.concatenate([active(cond_ref), active(ctx_cond_ref)], axis=0)
    both = jnp.concatenate([both, jnp.zeros((14, both.shape[1]), BF16)], axis=0)
    shift = dot(both, shift_ref[...])
    scale = dot(both, scale_ref[...])
    gate = dot(both, gate_ref[...])
    width = ctx_ref.shape[1]
    blank = jnp.zeros((1, width - 5 * shift.shape[1]), F32)
    row = jnp.concatenate(
        [shift[0:1], shift[1:2], scale[0:1], scale[1:2], gate[0:1], blank], axis=1
    )
    coarse = row.astype(BF16).astype(F32)
    ctx = ctx_ref[...].astype(F32)
    at = lax.broadcasted_iota(jnp.int32, (ctx.shape[0], 1), 0)
    picked = [
        jnp.sum(jnp.where(at == 2 * member_ref[0] + i, ctx, 0.0), axis=0, keepdims=True)
        for i in range(2)
    ]
    rows = jnp.concatenate(picked + [coarse, row - coarse], axis=0).astype(BF16)
    for i in range(out_ref.shape[0]):
        out_ref[i] = rows


def normed_rows(ref, x, start, multiplier, shift):
    rows = ref[x, pl.ds(start, CHUNK), :].astype(F32)
    mean = jnp.mean(rows * rows, axis=-1, keepdims=True)
    return (rows * lax.rsqrt(mean + NORM_EPS) * multiplier + shift).astype(BF16)


def turned(u, cosine, sine):
    lane = lax.broadcasted_iota(jnp.int32, u.shape, 1)
    first = (lane % 64) < 32
    swapped = jnp.where(first, pltpu.roll(u, 96, 1), pltpu.roll(u, 32, 1))
    return u * cosine + swapped * sine


def qkv_kernel(
    base_ref, own_ref, other_ref, planes_ref, gain_ref, wq_ref, wkv_ref, cos_ref, sin_ref,
    q_ref, kv_ref, hidden_ref,
):
    columns = wq_ref.shape[1]
    shift = row_vector(planes_ref, 0, columns)
    multiplier = gain_ref[...] * (1.0 + row_vector(planes_ref, 2, columns))
    count, rows, _ = own_ref.shape
    steps = rows // CHUNK

    def step(i, carry):
        x = i // steps
        start = pl.multiple_of((i % steps) * CHUNK, CHUNK)
        at = pl.multiple_of(base_ref[x] + start, CHUNK)
        hidden_ref[pl.ds(at, CHUNK), :] = normed_rows(own_ref, x, start, multiplier, shift)
        at = pl.multiple_of(base_ref[count + x] + start, CHUNK)
        hidden_ref[pl.ds(at, CHUNK), :] = normed_rows(other_ref, x, start, multiplier, shift)
        return carry

    lax.fori_loop(0, count * steps, step, 0)
    block = 384
    for at in range(0, hidden_ref.shape[0], block):
        cut = slice(at, at + block)
        hidden = hidden_ref[cut, :]
        cosine, sine = cos_ref[cut, :], sin_ref[cut, :]
        queries = dot(hidden, wq_ref[...])
        q_ref[cut, :HEAD_DIM] = turned(queries[:, :HEAD_DIM], cosine, sine).astype(BF16)
        q_ref[cut, HEAD_DIM:] = turned(queries[:, HEAD_DIM:], cosine, sine).astype(BF16)
        pairs = dot(hidden, wkv_ref[...])
        kv_ref[cut, :HEAD_DIM] = turned(pairs[:, :HEAD_DIM], cosine, sine).astype(BF16)
        kv_ref[cut, HEAD_DIM:] = pairs[:, HEAD_DIM:].astype(BF16)


def context_kernel(own_ref, other_ref, planes_ref, gain_ref, wkv_ref, out_ref, hidden_ref):
    columns = wkv_ref.shape[1]
    shift = row_vector(planes_ref, 1, columns)
    multiplier = gain_ref[...] * (1.0 + row_vector(planes_ref, 3, columns))
    count, rows, _ = own_ref.shape
    steps = rows // CHUNK
    half = count * rows

    def step(i, carry):
        x = i // steps
        start = pl.multiple_of((i % steps) * CHUNK, CHUNK)
        at = pl.multiple_of(x * rows + start, CHUNK)
        hidden_ref[pl.ds(at, CHUNK), :] = normed_rows(own_ref, x, start, multiplier, shift)
        at = pl.multiple_of(half + x * rows + start, CHUNK)
        hidden_ref[pl.ds(at, CHUNK), :] = normed_rows(other_ref, x, start, multiplier, shift)
        return carry

    lax.fori_loop(0, count * steps, step, 0)
    pairs = dot(hidden_ref[...], wkv_ref[...]).astype(BF16)
    for y in range(out_ref.shape[0]):
        out_ref[y] = pairs


def attention_kernel(
    place_ref, sink_ref, q_ref, low_ref, kv_ref, high_ref, ctx_ref, weight_ref,
    keep_ref, send_ref, padded_ref, attended_ref, gathered_ref,
):
    reach = WINDOW_REACH
    total = kv_ref.shape[0]
    core, first, last = place_ref[0], place_ref[1], place_ref[2]
    padded_ref[:reach, :] = low_ref[...]
    padded_ref[reach : reach + total, :] = kv_ref[...]
    padded_ref[reach + total :, :] = high_ref[...]
    ctx = ctx_ref[...].reshape(-1, 2 * HEAD_DIM)
    ctx_keys, ctx_values = ctx[:, :HEAD_DIM], ctx[:, HEAD_DIM:]
    factor = HEAD_DIM ** (-0.5) * LOG2_E
    row = lax.broadcasted_iota(jnp.int32, (2 * reach, 1), 0)
    sink = jnp.where(row < reach, sink_ref[0], sink_ref[1]) * LOG2_E
    position = lax.broadcasted_iota(jnp.int32, (2 * reach, 3 * reach), 0) % reach
    column = lax.broadcasted_iota(jnp.int32, (2 * reach, 3 * reach), 1)
    band = (column >= position) & (column <= position + 2 * reach)
    blocks = total // reach
    contract = (((1,), (1,)), ((), ()))

    def step(b, carry):
        at = pl.multiple_of(b * reach, reach)
        both = q_ref[pl.ds(at, reach), :]
        queries = jnp.concatenate([both[:, :HEAD_DIM], both[:, HEAD_DIM:]], axis=0)
        keys = padded_ref[pl.ds(at, 3 * reach), :HEAD_DIM]
        values = padded_ref[pl.ds(at, 3 * reach), HEAD_DIM:]
        lowest = jnp.where(b == 0, first * reach, 0)
        highest = jnp.where(b == blocks - 1, (3 - last) * reach, 3 * reach)
        allowed = band & (column >= lowest) & (column < highest)
        near = lax.dot_general(queries, keys, contract, preferred_element_type=F32) * factor
        near = jnp.where(allowed, near, MASKED_SCORE)
        far = lax.dot_general(queries, ctx_keys, contract, preferred_element_type=F32) * factor
        top = jnp.maximum(
            jnp.max(near, axis=-1, keepdims=True), jnp.max(far, axis=-1, keepdims=True)
        )
        top = jnp.maximum(top, sink)
        near = jnp.exp2(near - top)
        far = jnp.exp2(far - top)
        share = (
            jnp.sum(near, axis=-1, keepdims=True)
            + jnp.sum(far, axis=-1, keepdims=True)
            + jnp.exp2(sink - top)
        )
        mixed = dot(near.astype(BF16), values) + dot(far.astype(BF16), ctx_values)
        mixed = (mixed / share).astype(BF16)
        attended_ref[pl.ds(at, reach), :HEAD_DIM] = mixed[:reach]
        attended_ref[pl.ds(at, reach), HEAD_DIM:] = mixed[reach:]
        return carry

    lax.fori_loop(0, blocks, step, 0)
    rows = keep_ref.shape[0] // 4
    for x in range(4):
        mine = pl.multiple_of((2 * x + core) * rows, CHUNK)
        theirs = pl.multiple_of((2 * x + 1 - core) * rows, CHUNK)
        keep_ref[x * rows : (x + 1) * rows, :] = attended_ref[pl.ds(mine, rows), :]
        gathered_ref[x * rows : (x + 1) * rows, :] = attended_ref[pl.ds(theirs, rows), :]
    width = 512
    for n in range(0, send_ref.shape[1], width):
        send_ref[:, n : n + width] = dot(
            gathered_ref[...], weight_ref[:, n : n + width]
        ).astype(BF16)


def pair_kernel(keep_ref, weight_ref, got_ref, out_ref):
    width = 512
    count, rows, _ = out_ref.shape
    for n in range(0, got_ref.shape[1], width):
        cut = slice(n, n + width)
        both = dot(keep_ref[...], weight_ref[:, cut]) + got_ref[:, cut].astype(F32)
        out_ref[:, :, cut] = both.astype(BF16).reshape(count, rows, width)


def final_kernel(latent_ref, mixed_ref, planes_ref, out_ref):
    count = mixed_ref.shape[0]
    columns = planes_ref.shape[2] // 5
    gate = row_vector(planes_ref, 4, columns)

    def step(i, carry):
        cut = pl.ds(pl.multiple_of(i * CHUNK, CHUNK), CHUNK)
        mixed = mixed_ref[0, cut, :].astype(F32)
        for x in range(1, count):
            mixed = mixed + mixed_ref[x, cut, :].astype(F32)
        out_ref[cut, :] = (latent_ref[cut, :].astype(F32) + gate * mixed).astype(BF16)
        return carry

    lax.fori_loop(0, latent_ref.shape[0] // CHUNK, step, 0)


SHIFTS = (0, 1, 3, 2)


def from_all_x(block):
    got = [block]
    for shift in SHIFTS[1:]:
        got.append(lax.ppermute(block, "x", [(i, (i + shift) % 4) for i in range(4)]))
    return jnp.stack(got)


def swapped(x):
    return lax.ppermute(x, "c", [(0, 1), (1, 0)])


def tables(position):
    inv_freq = 10000.0 ** (-jnp.arange(0, HEAD_DIM // 2, 2, dtype=F32) / (HEAD_DIM // 2))
    by_row = (position // GRID_W).astype(F32)[:, None] * inv_freq
    by_col = (position % GRID_W).astype(F32)[:, None] * inv_freq
    angles = jnp.concatenate([by_row, by_row, by_col, by_col], axis=1)
    sign = jnp.where((jnp.arange(HEAD_DIM) % 64) < 32, -1.0, 1.0).astype(F32)
    return jnp.cos(angles), jnp.sin(angles) * sign


def shards(
    latent,
    condition,
    context_condition,
    context,
    norm_gain,
    shift_weight,
    scale_weight,
    gate_weight,
    query_weight,
    key_matrix,
    value_matrix,
    sink_logit_head,
    out_weight,
):
    nz, ny, nx, nc = (lax.axis_size(a) for a in ALL)
    rows, width = latent.shape
    group_rows = rows * nx * nc
    columns = shift_weight.shape[1]
    place = lax.axis_index(SP)
    core = lax.axis_index("c").astype(jnp.int32)
    gain = norm_gain.reshape(1, width)
    member = lax.axis_index(TP).astype(jnp.int32)
    share = context.shape[0] // (nx * nc)
    parts = pl.pallas_call(
        parts_kernel,
        out_shape=shape_of((nz, share + 2, width), BF16),
        in_specs=[SMEM] + [VMEM] * 6,
        out_specs=VMEM,
        name="parts",
    )(
        member[None],
        condition.reshape(1, -1),
        context_condition.reshape(1, -1),
        shift_weight,
        scale_weight,
        gate_weight,
        context,
    )
    parts = exchanged(parts, "z")
    latent_x = from_all_x(latent)
    sums = jnp.sum(parts[:, share:, : 5 * columns].astype(F32), axis=(0, 1)).reshape(1, -1)
    planes = exchanged(copies(sums, PLANE), PLANE)
    ctx_x = from_all_x(parts[:, :share].reshape(nz * share, width))
    latent_c = swapped(latent_x)
    ctx_c = swapped(ctx_x)
    pair_weight = jnp.concatenate([key_matrix, value_matrix], axis=1)
    cosine, sine = tables(place * group_rows + jnp.arange(group_rows, dtype=jnp.int32))
    ctx_pairs = pl.pallas_call(
        context_kernel,
        out_shape=shape_of((ny, nx * nc * nz * share, 2 * HEAD_DIM), BF16),
        in_specs=[VMEM] * 5,
        out_specs=VMEM,
        scratch_shapes=[pltpu.VMEM((nx * nc * nz * share, width), BF16)],
        name="context_pairs",
    )(ctx_x, ctx_c, planes, gain, pair_weight)
    ctx_pairs = exchanged(ctx_pairs, "y")
    sources = (lax.axis_index("x").astype(jnp.int32) - jnp.array(SHIFTS, jnp.int32)) % nx
    bases = jnp.concatenate([2 * sources + core, 2 * sources + 1 - core]) * rows
    queries, pairs = pl.pallas_call(
        qkv_kernel,
        out_shape=(
            shape_of((group_rows, 2 * HEAD_DIM), BF16),
            shape_of((group_rows, 2 * HEAD_DIM), BF16),
        ),
        in_specs=[SMEM] + [VMEM] * 8,
        out_specs=(VMEM, VMEM),
        scratch_shapes=[pltpu.VMEM((group_rows, width), BF16)],
        name="qkv",
    )(bases, latent_x, latent_c, planes, gain, query_weight, pair_weight, cosine, sine)
    count = nz * ny
    forward = [(i, i + 1) for i in range(count - 1)]
    backward = [(i + 1, i) for i in range(count - 1)]
    low = lax.ppermute(pairs[group_rows - WINDOW_REACH :], SP, forward)
    high = lax.ppermute(pairs[:WINDOW_REACH], SP, backward)
    where = jnp.stack(
        [core, (place == 0).astype(jnp.int32), (place == count - 1).astype(jnp.int32)]
    )
    half = group_rows // nc
    keep, send = pl.pallas_call(
        attention_kernel,
        out_shape=(
            shape_of((half, 2 * HEAD_DIM), BF16),
            shape_of((half, width), BF16),
        ),
        in_specs=[SMEM] * 2 + [VMEM] * 6,
        out_specs=(VMEM, VMEM),
        scratch_shapes=[
            pltpu.VMEM((group_rows + 2 * WINDOW_REACH, 2 * HEAD_DIM), BF16),
            pltpu.VMEM((group_rows, 2 * HEAD_DIM), BF16),
            pltpu.VMEM((half, 2 * HEAD_DIM), BF16),
        ],
        name="attention",
    )(where, sink_logit_head, queries, low, pairs, high, ctx_pairs, out_weight)
    got = swapped(send)
    paired = pl.pallas_call(
        pair_kernel,
        out_shape=shape_of((nx, rows, width), BF16),
        in_specs=[VMEM] * 3,
        out_specs=VMEM,
        name="pair",
    )(keep, out_weight, got)
    mixed = exchanged(paired, "x")
    return pl.pallas_call(
        final_kernel,
        out_shape=shape_of((rows, width), BF16),
        in_specs=[VMEM] * 3,
        out_specs=VMEM,
        name="final",
    )(latent, mixed, planes)


def solution(mesh):
    torus = Mesh(mesh.devices.reshape(16, 4, 4, 2), ALL)

    return jax.shard_map(
        shards,
        mesh=torus,
        in_specs=(
            P(ALL, None),
            P(SP),
            P(SP),
            P(SP, None),
            P(),
            P(SP, TP),
            P(SP, TP),
            P(SP, TP),
            P(None, TP),
            P(None, TP),
            P(None, TP),
            P(TP),
            P(TP, None),
        ),
        out_specs=P(ALL, None),
        check_vma=False,
    )
```

time: 193 us -> 158 us (0.82)
  the two profiles are of different devices: /device:TPU:32 before, /device:TPU:24 now
where the time goes in v2:
time: 158 us; the launch traced here: 157 us
  starting transfers between devices  57.5 us (36%)
  waiting for transfers between devices  30.4 us (19%)
  Pallas kernels  30 us (19%)
  blocking collectives  25.7 us (16%)
  other arithmetic  7.36 us (5%)
  local copies, waits for them, and re-layouts  6.27 us (4%)
    all_to_all x3, starting transfers between devices, exchanged(): return lax.all_to_all(blocks, axis, 0, 0, tiled=True)  26 us
    all_to_all x1, blocking collectives, exchanged(): return lax.all_to_all(blocks, axis, 0, 0, tiled=True)  25.7 us
    ppermute x6, starting transfers between devices, from_all_x(): lax.ppermute(block, 'x', [(i, (i + shift) % 4) for i in range(4)])  19.9 us
    all_to_all x3, waiting for transfers between devices, exchanged(): return lax.all_to_all(blocks, axis, 0, 0, tiled=True)  17.1 us
    pallas_call x1, Pallas kernels, shards(): pl.pallas_call(qkv_kernel, out_shape=(shape_of((group_rows, 2 * HEAD_DIM)...  9.22 us
    pallas_call x1, Pallas kernels, shards(): pl.pallas_call(attention_kernel, out_shape=(shape_of((half, 2 * HEAD_DIM)...  8.83 us
    ppermute x3, starting transfers between devices, swapped(): return lax.ppermute(x, 'c', [(0, 1), (1, 0)])  5.75 us
    ppermute x6, waiting for transfers between devices, from_all_x(): lax.ppermute(block, 'x', [(i, (i + shift) % 4) for i in range(4)])  4.98 us
  transfers between devices with their start and end apart: 14, of which 5 were waited for; matrix products, arithmetic and copies ran while one was open for 7% of the time, Pallas kernels for 10%

profile of v2, /device:TPU:24, one launch (start us, length us, event | category | flops | bytes accessed | tf_op | source)
XLA Modules:
  0.0 157.4 jit_solution(10982645224669421290)
XLA Ops:
  0.0 5.1 %collective-permute-start.2 = (bf16[96,2048]{1,0:T(8,128)(2,1)}, bf16[96,2048]{1,0:T(8,128)(2,1)S(1)}, u32[]{:S(2)}, u32[]{:S(2)}) collective-permute-start(bf16[96,2048]{1,0:T(8,128)(2,1)} %latent_ref.1), channel_id=1, source_target_pairs={{0,4},{2,6},{4,0},{6,2},{1,5},{3,7},{5,1},{7,3},{8,12},{10,14},{12... | collective-permute-start | bytes 1179656 | tf_op jit(solution)/shard_map/ppermute | solution.py:249
  5.1 3.1 %collective-permute-start.1 = (bf16[96,2048]{1,0:T(8,128)(2,1)}, bf16[96,2048]{1,0:T(8,128)(2,1)S(1)}, u32[]{:S(2)}, u32[]{:S(2)}) collective-permute-start(bf16[96,2048]{1,0:T(8,128)(2,1)} %latent_ref.1), channel_id=1, source_target_pairs={{0,6},{2,0},{4,2},{6,4},{1,7},{3,1},{5,3},{7,5},{8,14},{10,8},{12,... | collective-permute-start | bytes 1179656 | tf_op jit(solution)/shard_map/ppermute | solution.py:249
  8.1 2.8 %collective-permute-start = (bf16[96,2048]{1,0:T(8,128)(2,1)}, bf16[96,2048]{1,0:T(8,128)(2,1)S(1)}, u32[]{:S(2)}, u32[]{:S(2)}) collective-permute-start(bf16[96,2048]{1,0:T(8,128)(2,1)} %latent_ref.1), channel_id=1, source_target_pairs={{0,2},{2,4},{4,6},{6,0},{1,3},{3,5},{5,7},{7,1},{8,10},{10,12},{12... | collective-permute-start | bytes 1179656 | tf_op jit(solution)/shard_map/ppermute | solution.py:249
  12.7 15.2 %all-to-all-start = ((bf16[16,4,2048]{2,1,0:T(4,128)(2,1)}), bf16[16,4,2048]{2,1,0:T(4,128)(2,1)S(1)}, u32[]{:S(2)}, u32[]{:S(2)}) async-start(bf16[16,4,2048]{2,1,0:T(4,128)(2,1)} %parts.1), calls=%async_computation | async-start | bytes 524288 | tf_op jit(solution)/shard_map/all_to_all | solution.py:37
  30.3 1.9 %collective-permute-start.3 = (bf16[4,96,2048]{2,1,0:T(8,128)(2,1)S(1)}, bf16[4,96,2048]{2,1,0:T(8,128)(2,1)}, u32[]{:S(2)}, u32[]{:S(2)}) collective-permute-start(bf16[4,96,2048]{2,1,0:T(8,128)(2,1)S(1)} %pad_maximum_fusion.own_ref), channel_id=1, source_target_pairs={{0,1},{1,0},{2,3},{3,2},{4,5},{5,4},{6,7},{7,6},{8,9},{9,8},{10,11... | collective-permute-start | bytes 4718600 | tf_op jit(solution)/shard_map/ppermute | solution.py:254
  32.3 2.4 %sine_multiply_fusion = (f32[768,128]{1,0:T(8,128)}, f32[768,128]{1,0:T(8,128)}) fusion(f32[128]{0:T(128)S(1)} %compare_select_fusion.2, f32[768,32]{1,0:T(8,128)S(1)} %get-tuple-element.20, f32[768,32]{1,0:T(8,128)S(1)} %get-tuple-element.19), kind=kLoop, calls=%fused_computation.3 | loop fusion | flops 393216 | bytes 983552 | tf_op jit(solution)/shard_map/mul | solution.py:263
  34.8 11.0 %all-to-all-done = bf16[16,4,2048]{2,1,0:T(4,128)(2,1)S(1)} async-done(((bf16[16,4,2048]{2,1,0:T(4,128)(2,1)}), bf16[16,4,2048]{2,1,0:T(4,128)(2,1)S(1)}, u32[]{:S(2)}, u32[]{:S(2)}) %all-to-all-start) | async-done | bytes 262176 | tf_op jit(solution)/shard_map/all_to_all | solution.py:37
  45.9 3.0 %collective-permute-start.8 = (bf16[32,2048]{1,0:T(8,128)(2,1)S(1)}, bf16[32,2048]{1,0:T(8,128)(2,1)S(1)}, u32[]{:S(2)}, u32[]{:S(2)}) collective-permute-start(bf16[32,2048]{1,0:T(8,128)(2,1)S(1)} %reshape.70), channel_id=1, source_target_pairs={{0,4},{2,6},{4,0},{6,2},{1,5},{3,7},{5,1},{7,3},{8,12},{10,14},{12... | collective-permute-start | bytes 393224 | tf_op jit(solution)/shard_map/ppermute | solution.py:249
  49.0 4.1 %collective-permute-start.7 = (bf16[32,2048]{1,0:T(8,128)(2,1)S(1)}, bf16[32,2048]{1,0:T(8,128)(2,1)S(1)}, u32[]{:S(2)}, u32[]{:S(2)}) collective-permute-start(bf16[32,2048]{1,0:T(8,128)(2,1)S(1)} %reshape.70), channel_id=1, source_target_pairs={{0,6},{2,0},{4,2},{6,4},{1,7},{3,1},{5,3},{7,5},{8,14},{10,8},{12,... | collective-permute-start | bytes 393224 | tf_op jit(solution)/shard_map/ppermute | solution.py:249
  53.0 1.9 %collective-permute-start.6 = (bf16[32,2048]{1,0:T(8,128)(2,1)S(1)}, bf16[32,2048]{1,0:T(8,128)(2,1)}, u32[]{:S(2)}, u32[]{:S(2)}) collective-permute-start(bf16[32,2048]{1,0:T(8,128)(2,1)S(1)} %reshape.70), channel_id=1, source_target_pairs={{0,2},{2,4},{4,6},{6,0},{1,3},{3,5},{5,7},{7,1},{8,10},{10,12},{12... | collective-permute-start | bytes 393224 | tf_op jit(solution)/shard_map/ppermute | solution.py:249
  56.2 5.0 %collective-permute-done.6 = bf16[32,2048]{1,0:T(8,128)(2,1)} collective-permute-done((bf16[32,2048]{1,0:T(8,128)(2,1)S(1)}, bf16[32,2048]{1,0:T(8,128)(2,1)}, u32[]{:S(2)}, u32[]{:S(2)}) %collective-permute-start.6) | collective-permute-done | bytes 131104 | tf_op jit(solution)/shard_map/ppermute | solution.py:249
  66.1 5.2 %all-to-all-start.1 = ((f32[32,1,1280]{2,1,0:T(1,128)}), f32[32,1,1280]{2,1,0:T(1,128)S(1)}, u32[]{:S(2)}, u32[]{:S(2)}) async-start(f32[32,1,1280]{2,1,0:T(1,128)} %broadcast_in_dim.22), calls=%async_computation.1 | async-start | bytes 327680 | tf_op jit(solution)/shard_map/all_to_all | solution.py:37
  71.3 6.1 %all-to-all-done.1.planes_ref = f32[32,1,1280]{2,1,0:T(1,128)S(1)} async-done(((f32[32,1,1280]{2,1,0:T(1,128)}), f32[32,1,1280]{2,1,0:T(1,128)S(1)}, u32[]{:S(2)}, u32[]{:S(2)}) %all-to-all-start.1) | async-done | bytes 163872 | tf_op jit(solution)/shard_map/all_to_all | solution.py:37
  78.1 4.0 %context_pairs.1 = bf16[4,256,256]{2,1,0:T(8,128)(2,1)} custom-call(bf16[4,32,2048]{2,1,0:T(8,128)(2,1)} %copy-done.4, bf16[4,32,2048]{2,1,0:T(8,128)(2,1)} %collective-permute-done.9.other_ref, f32[32,1,1280]{2,1,0:T(1,128)} %copy-done.2, f32[1,2048]{1,0:T(1,128)} %bitcast.20, bf16[2048,256]{1,0:T(8,128)(2,1)} %copy-done), custom_call_target="tpu_custom_call" | custom-call | tf_op jit(solution)/shard_map/context_pairs/pallas_call | solution.py:314
  82.1 5.5 %all-to-all-start.2 = ((bf16[4,256,256]{2,1,0:T(8,128)(2,1)}), bf16[4,256,256]{2,1,0:T(8,128)(2,1)S(1)}, u32[]{:S(2)}, u32[]{:S(2)}) async-start(bf16[4,256,256]{2,1,0:T(8,128)(2,1)} %context_pairs.1), calls=%async_computation.2 | async-start | bytes 1048576 | tf_op jit(solution)/shard_map/all_to_all | solution.py:37
  88.2 9.2 %qkv.1 = (bf16[768,256]{1,0:T(8,128)(2,1)}, bf16[768,256]{1,0:T(8,128)(2,1)}) custom-call(s32[8]{0:T(128)} %add_multiply_fusion.base_ref, bf16[4,96,2048]{2,1,0:T(8,128)(2,1)} %copy-done.1, bf16[4,96,2048]{2,1,0:T(8,128)(2,1)} %collective-permute-done.3.other_ref, f32[32,1,1280]{2,1,0:T(1,128)} %copy-done.2, f32[1,2048]{1,0:T(1,128)} %bitcast.21, ...), custom_call_target="tpu_custom_call" | custom-call | tf_op jit(solution)/shard_map/qkv/pallas_call | solution.py:325
  98.3 2.9 %collective-permute-start.4 = (bf16[128,256]{1,0:T(8,128)(2,1)S(1)}, bf16[128,256]{1,0:T(8,128)(2,1)S(1)}, u32[]{:S(2)}, u32[]{:S(2)}) collective-permute-start(bf16[128,256]{1,0:T(8,128)(2,1)S(1)} %get-tuple-element.18), channel_id=1, source_target_pairs={{0,8},{8,16},{16,24},{24,32},{32,40},{40,48},{48,56},{56,64},{64,7... | collective-permute-start | bytes 196616 | tf_op jit(solution)/shard_map/ppermute | solution.py:339
  101.3 2.9 %collective-permute-start.5 = (bf16[128,256]{1,0:T(8,128)(2,1)S(1)}, bf16[128,256]{1,0:T(8,128)(2,1)S(1)}, u32[]{:S(2)}, u32[]{:S(2)}) collective-permute-start(bf16[128,256]{1,0:T(8,128)(2,1)S(1)} %get-tuple-element.17), channel_id=1, source_target_pairs={{8,0},{16,8},{24,16},{32,24},{40,32},{48,40},{56,48},{64,56},{72,6... | collective-permute-start | bytes 196616 | tf_op jit(solution)/shard_map/ppermute | solution.py:340
  104.8 4.7 %collective-permute-done.5.high_ref = bf16[128,256]{1,0:T(8,128)(2,1)S(1)} collective-permute-done((bf16[128,256]{1,0:T(8,128)(2,1)S(1)}, bf16[128,256]{1,0:T(8,128)(2,1)S(1)}, u32[]{:S(2)}, u32[]{:S(2)}) %collective-permute-start.5) | collective-permute-done | bytes 65568 | tf_op jit(solution)/shard_map/ppermute | solution.py:340
  110.2 8.8 %attention.1 = (bf16[384,256]{1,0:T(8,128)(2,1)}, bf16[384,2048]{1,0:T(8,128)(2,1)}) custom-call(s32[3]{0:T(128)} %pad_add_fusion.place_ref, f32[2]{0:T(128)} %sink_ref.1, bf16[768,256]{1,0:T(8,128)(2,1)} %get-tuple-element.9.q_ref, bf16[128,256]{1,0:T(8,128)(2,1)} %copy-done.12, bf16[768,256]{1,0:T(8,128)(2,1)} %get-tuple-element.10.kv_ref, ...), custom_call_target="tpu_custom_call" | custom-call | tf_op jit(solution)/shard_map/attention/pallas_call | solution.py:345
  120.9 3.6 %collective-permute-done.10.got_ref = bf16[384,2048]{1,0:T(8,128)(2,1)S(1)} collective-permute-done((bf16[384,2048]{1,0:T(8,128)(2,1)}, bf16[384,2048]{1,0:T(8,128)(2,1)S(1)}, u32[]{:S(2)}, u32[]{:S(2)}) %collective-permute-start.10) | collective-permute-done | bytes 1572896 | tf_op jit(solution)/shard_map/ppermute | solution.py:254
  125.6 3.5 %pair.1 = bf16[4,96,2048]{2,1,0:T(8,128)(2,1)} custom-call(bf16[384,256]{1,0:T(8,128)(2,1)} %get-tuple-element.11.keep_ref, bf16[256,2048]{1,0:T(8,128)(2,1)} %weight_ref.3, bf16[384,2048]{1,0:T(8,128)(2,1)} %copy-done.6), custom_call_target="tpu_custom_call" | custom-call | tf_op jit(solution)/shard_map/pair/pallas_call | solution.py:361
  129.2 25.7 %all_to_all.20.mixed_ref = bf16[4,96,2048]{2,1,0:T(8,128)(2,1)} all-to-all(bf16[4,96,2048]{2,1,0:T(8,128)(2,1)} %pair.1), channel_id=1, replica_groups=mesh['z'=16,'y'=4,'x'=4,'c'=2] {'x'}, dimensions={0} | all-to-all | bytes 3145728 | tf_op jit(solution)/shard_map/all_to_all | solution.py:37
  154.9 2.6 %final.1 = bf16[96,2048]{1,0:T(8,128)(2,1)} custom-call(bf16[96,2048]{1,0:T(8,128)(2,1)} %latent_ref.1, bf16[4,96,2048]{2,1,0:T(8,128)(2,1)} %all_to_all.20.mixed_ref, f32[32,1,1280]{2,1,0:T(1,128)} %copy-done.2), custom_call_target="tpu_custom_call" | custom-call | tf_op jit(solution)/shard_map/final/pallas_call | solution.py:369
  (60 shorter events, 16.9 us)
Async XLA Ops:
  0.0 29.0 %copy-start.5 = (bf16[96,2048]{1,0:T(8,128)(2,1)S(1)}, bf16[96,2048]{1,0:T(8,128)(2,1)}, u32[]{:S(2)}) copy-start(bf16[96,2048]{1,0:T(8,128)(2,1)} %latent_ref.1) | copy-start | bytes 1179652
  0.0 28.2 %collective-permute-start.2 = (bf16[96,2048]{1,0:T(8,128)(2,1)}, bf16[96,2048]{1,0:T(8,128)(2,1)S(1)}, u32[]{:S(2)}, u32[]{:S(2)}) collective-permute-start(bf16[96,2048]{1,0:T(8,128)(2,1)} %latent_ref.1), channel_id=1, source_target_pairs={{0,4},{2,6},{4,0},{6,2},{1,5},{3,7},{5,1},{7,3},{8,12},{10,14},{12... | collective-permute-start | bytes 1179656 | tf_op jit(solution)/shard_map/ppermute | solution.py:249
  5.1 23.2 %collective-permute-start.1 = (bf16[96,2048]{1,0:T(8,128)(2,1)}, bf16[96,2048]{1,0:T(8,128)(2,1)S(1)}, u32[]{:S(2)}, u32[]{:S(2)}) collective-permute-start(bf16[96,2048]{1,0:T(8,128)(2,1)} %latent_ref.1), channel_id=1, source_target_pairs={{0,6},{2,0},{4,2},{6,4},{1,7},{3,1},{5,3},{7,5},{8,14},{10,8},{12,... | collective-permute-start | bytes 1179656 | tf_op jit(solution)/shard_map/ppermute | solution.py:249
  8.1 20.1 %collective-permute-start = (bf16[96,2048]{1,0:T(8,128)(2,1)}, bf16[96,2048]{1,0:T(8,128)(2,1)S(1)}, u32[]{:S(2)}, u32[]{:S(2)}) collective-permute-start(bf16[96,2048]{1,0:T(8,128)(2,1)} %latent_ref.1), channel_id=1, source_target_pairs={{0,2},{2,4},{4,6},{6,0},{1,3},{3,5},{5,7},{7,1},{8,10},{10,12},{12... | collective-permute-start | bytes 1179656 | tf_op jit(solution)/shard_map/ppermute | solution.py:249
  12.7 33.0 %all-to-all-start = ((bf16[16,4,2048]{2,1,0:T(4,128)(2,1)}), bf16[16,4,2048]{2,1,0:T(4,128)(2,1)S(1)}, u32[]{:S(2)}, u32[]{:S(2)}) async-start(bf16[16,4,2048]{2,1,0:T(4,128)(2,1)} %parts.1), calls=%async_computation | async-start | bytes 524288 | tf_op jit(solution)/shard_map/all_to_all | solution.py:37
  30.3 15.6 %copy-start.1 = (bf16[4,96,2048]{2,1,0:T(8,128)(2,1)}, bf16[4,96,2048]{2,1,0:T(8,128)(2,1)S(1)}, u32[]{:S(2)}) copy-start(bf16[4,96,2048]{2,1,0:T(8,128)(2,1)S(1)} %pad_maximum_fusion.own_ref) | copy-start | bytes 4718596
  30.3 57.9 %collective-permute-start.3 = (bf16[4,96,2048]{2,1,0:T(8,128)(2,1)S(1)}, bf16[4,96,2048]{2,1,0:T(8,128)(2,1)}, u32[]{:S(2)}, u32[]{:S(2)}) collective-permute-start(bf16[4,96,2048]{2,1,0:T(8,128)(2,1)S(1)} %pad_maximum_fusion.own_ref), channel_id=1, source_target_pairs={{0,1},{1,0},{2,3},{3,2},{4,5},{5,4},{6,7},{7,6},{8,9},{9,8},{10,11... | collective-permute-start | bytes 4718600 | tf_op jit(solution)/shard_map/ppermute | solution.py:254
  34.7 29.5 %copy-start.14 = (s32[4]{0:T(128)S(1)}, s32[4]{0:T(128)}, u32[]{:S(2)}) copy-start(s32[4]{0:T(128)} %constant.104) | copy-start | bytes 52
  45.8 15.4 %copy-start.7 = (bf16[16,4,2048]{2,1,0:T(4,128)(2,1)}, bf16[16,4,2048]{2,1,0:T(4,128)(2,1)S(1)}, u32[]{:S(2)}) copy-start(bf16[16,4,2048]{2,1,0:T(4,128)(2,1)S(1)} %all-to-all-done) | copy-start | bytes 786436
  45.9 10.3 %collective-permute-start.8 = (bf16[32,2048]{1,0:T(8,128)(2,1)S(1)}, bf16[32,2048]{1,0:T(8,128)(2,1)S(1)}, u32[]{:S(2)}, u32[]{:S(2)}) collective-permute-start(bf16[32,2048]{1,0:T(8,128)(2,1)S(1)} %reshape.70), channel_id=1, source_target_pairs={{0,4},{2,6},{4,0},{6,2},{1,5},{3,7},{5,1},{7,3},{8,12},{10,14},{12... | collective-permute-start | bytes 393224 | tf_op jit(solution)/shard_map/ppermute | solution.py:249
  49.0 7.3 %collective-permute-start.7 = (bf16[32,2048]{1,0:T(8,128)(2,1)S(1)}, bf16[32,2048]{1,0:T(8,128)(2,1)S(1)}, u32[]{:S(2)}, u32[]{:S(2)}) collective-permute-start(bf16[32,2048]{1,0:T(8,128)(2,1)S(1)} %reshape.70), channel_id=1, source_target_pairs={{0,6},{2,0},{4,2},{6,4},{1,7},{3,1},{5,3},{7,5},{8,14},{10,8},{12,... | collective-permute-start | bytes 393224 | tf_op jit(solution)/shard_map/ppermute | solution.py:249
  53.0 8.2 %collective-permute-start.6 = (bf16[32,2048]{1,0:T(8,128)(2,1)S(1)}, bf16[32,2048]{1,0:T(8,128)(2,1)}, u32[]{:S(2)}, u32[]{:S(2)}) collective-permute-start(bf16[32,2048]{1,0:T(8,128)(2,1)S(1)} %reshape.70), channel_id=1, source_target_pairs={{0,2},{2,4},{4,6},{6,0},{1,3},{3,5},{5,7},{7,1},{8,10},{10,12},{12... | collective-permute-start | bytes 393224 | tf_op jit(solution)/shard_map/ppermute | solution.py:249
  56.1 21.3 %copy-start = (bf16[2048,256]{1,0:T(8,128)(2,1)}, bf16[2048,256]{1,0:T(8,128)(2,1)S(1)}, u32[]{:S(2)}) copy-start(bf16[2048,256]{1,0:T(8,128)(2,1)S(1)} %constant_dynamic-update-slice_fusion.wkv_ref) | copy-start | bytes 3145732
  56.2 5.0 %copy-start.10 = (bf16[32,2048]{1,0:T(8,128)(2,1)}, bf16[32,2048]{1,0:T(8,128)(2,1)S(1)}, u32[]{:S(2)}) copy-start(bf16[32,2048]{1,0:T(8,128)(2,1)S(1)} %collective-permute-done.8) | copy-start | bytes 393220
  56.2 5.0 %copy-start.11 = (bf16[32,2048]{1,0:T(8,128)(2,1)}, bf16[32,2048]{1,0:T(8,128)(2,1)S(1)}, u32[]{:S(2)}) copy-start(bf16[32,2048]{1,0:T(8,128)(2,1)S(1)} %collective-permute-done.7) | copy-start | bytes 393220
  62.3 15.1 %copy-start.4 = (bf16[4,32,2048]{2,1,0:T(8,128)(2,1)}, bf16[4,32,2048]{2,1,0:T(8,128)(2,1)S(1)}, u32[]{:S(2)}) copy-start(bf16[4,32,2048]{2,1,0:T(8,128)(2,1)S(1)} %pad_maximum_fusion.1.own_ref) | copy-start | bytes 1572868
  62.3 15.1 %collective-permute-start.9 = (bf16[4,32,2048]{2,1,0:T(8,128)(2,1)S(1)}, bf16[4,32,2048]{2,1,0:T(8,128)(2,1)}, u32[]{:S(2)}, u32[]{:S(2)}) collective-permute-start(bf16[4,32,2048]{2,1,0:T(8,128)(2,1)S(1)} %pad_maximum_fusion.1.own_ref), channel_id=1, source_target_pairs={{0,1},{1,0},{2,3},{3,2},{4,5},{5,4},{6,7},{7,6},{8,9},{9,8},{10,11... | collective-permute-start | bytes 1572872 | tf_op jit(solution)/shard_map/ppermute | solution.py:254
  66.1 11.3 %all-to-all-start.1 = ((f32[32,1,1280]{2,1,0:T(1,128)}), f32[32,1,1280]{2,1,0:T(1,128)S(1)}, u32[]{:S(2)}, u32[]{:S(2)}) async-start(f32[32,1,1280]{2,1,0:T(1,128)} %broadcast_in_dim.22), calls=%async_computation.1 | async-start | bytes 327680 | tf_op jit(solution)/shard_map/all_to_all | solution.py:37
  82.1 22.8 %all-to-all-start.2 = ((bf16[4,256,256]{2,1,0:T(8,128)(2,1)}), bf16[4,256,256]{2,1,0:T(8,128)(2,1)S(1)}, u32[]{:S(2)}, u32[]{:S(2)}) async-start(bf16[4,256,256]{2,1,0:T(8,128)(2,1)} %context_pairs.1), calls=%async_computation.2 | async-start | bytes 1048576 | tf_op jit(solution)/shard_map/all_to_all | solution.py:37
  98.3 6.5 %collective-permute-start.4 = (bf16[128,256]{1,0:T(8,128)(2,1)S(1)}, bf16[128,256]{1,0:T(8,128)(2,1)S(1)}, u32[]{:S(2)}, u32[]{:S(2)}) collective-permute-start(bf16[128,256]{1,0:T(8,128)(2,1)S(1)} %get-tuple-element.18), channel_id=1, source_target_pairs={{0,8},{8,16},{16,24},{24,32},{32,40},{40,48},{48,56},{56,64},{64,7... | collective-permute-start | bytes 196616 | tf_op jit(solution)/shard_map/ppermute | solution.py:339
  101.3 8.3 %collective-permute-start.5 = (bf16[128,256]{1,0:T(8,128)(2,1)S(1)}, bf16[128,256]{1,0:T(8,128)(2,1)S(1)}, u32[]{:S(2)}, u32[]{:S(2)}) collective-permute-start(bf16[128,256]{1,0:T(8,128)(2,1)S(1)} %get-tuple-element.17), channel_id=1, source_target_pairs={{8,0},{16,8},{24,16},{32,24},{40,32},{48,40},{56,48},{64,56},{72,6... | collective-permute-start | bytes 196616 | tf_op jit(solution)/shard_map/ppermute | solution.py:340
  104.8 4.7 %copy-start.3 = (bf16[4,256,256]{2,1,0:T(8,128)(2,1)}, bf16[4,256,256]{2,1,0:T(8,128)(2,1)S(1)}, u32[]{:S(2)}) copy-start(bf16[4,256,256]{2,1,0:T(8,128)(2,1)S(1)} %all-to-all-done.2.ctx_ref) | copy-start | bytes 1572868
  104.8 4.7 %copy-start.12 = (bf16[128,256]{1,0:T(8,128)(2,1)}, bf16[128,256]{1,0:T(8,128)(2,1)S(1)}, u32[]{:S(2)}) copy-start(bf16[128,256]{1,0:T(8,128)(2,1)S(1)} %collective-permute-done.4.low_ref) | copy-start | bytes 196612
  119.0 5.5 %collective-permute-start.10 = (bf16[384,2048]{1,0:T(8,128)(2,1)}, bf16[384,2048]{1,0:T(8,128)(2,1)S(1)}, u32[]{:S(2)}, u32[]{:S(2)}) collective-permute-start(bf16[384,2048]{1,0:T(8,128)(2,1)} %get-tuple-element.12), channel_id=1, source_target_pairs={{0,1},{1,0},{2,3},{3,2},{4,5},{5,4},{6,7},{7,6},{8,9},{9,8},{10,11... | collective-permute-start | bytes 4718600 | tf_op jit(solution)/shard_map/ppermute | solution.py:254
  (5 other events, 6.4 us)

commit v3 on v2

--- a/solution.py
+++ b/solution.py
@@ -53,9 +53,7 @@
     return jnp.concatenate(pieces, axis=1)
 
 
-def parts_kernel(
-    member_ref, cond_ref, ctx_cond_ref, shift_ref, scale_ref, gate_ref, ctx_ref, out_ref
-):
+def parts_kernel(cond_ref, ctx_cond_ref, shift_ref, scale_ref, gate_ref, out_ref):
     def active(ref):
         v = ref[...]
         return (v / (1.0 + jnp.exp(-v))).astype(BF16)
@@ -65,21 +63,9 @@
     shift = dot(both, shift_ref[...])
     scale = dot(both, scale_ref[...])
     gate = dot(both, gate_ref[...])
-    width = ctx_ref.shape[1]
-    blank = jnp.zeros((1, width - 5 * shift.shape[1]), F32)
-    row = jnp.concatenate(
-        [shift[0:1], shift[1:2], scale[0:1], scale[1:2], gate[0:1], blank], axis=1
-    )
-    coarse = row.astype(BF16).astype(F32)
-    ctx = ctx_ref[...].astype(F32)
-    at = lax.broadcasted_iota(jnp.int32, (ctx.shape[0], 1), 0)
-    picked = [
-        jnp.sum(jnp.where(at == 2 * member_ref[0] + i, ctx, 0.0), axis=0, keepdims=True)
-        for i in range(2)
-    ]
-    rows = jnp.concatenate(picked + [coarse, row - coarse], axis=0).astype(BF16)
+    row = jnp.concatenate([shift[0:1], shift[1:2], scale[0:1], scale[1:2], gate[0:1]], axis=1)
     for i in range(out_ref.shape[0]):
-        out_ref[i] = rows
+        out_ref[i] = row
 
 
 def normed_rows(ref, x, start, multiplier, shift):
@@ -128,41 +114,28 @@
         kv_ref[cut, HEAD_DIM:] = pairs[:, HEAD_DIM:].astype(BF16)
 
 
-def context_kernel(own_ref, other_ref, planes_ref, gain_ref, wkv_ref, out_ref, hidden_ref):
+def context_kernel(ctx_ref, planes_ref, gain_ref, wkv_ref, out_ref):
     columns = wkv_ref.shape[1]
     shift = row_vector(planes_ref, 1, columns)
     multiplier = gain_ref[...] * (1.0 + row_vector(planes_ref, 3, columns))
-    count, rows, _ = own_ref.shape
-    steps = rows // CHUNK
-    half = count * rows
-
-    def step(i, carry):
-        x = i // steps
-        start = pl.multiple_of((i % steps) * CHUNK, CHUNK)
-        at = pl.multiple_of(x * rows + start, CHUNK)
-        hidden_ref[pl.ds(at, CHUNK), :] = normed_rows(own_ref, x, start, multiplier, shift)
-        at = pl.multiple_of(half + x * rows + start, CHUNK)
-        hidden_ref[pl.ds(at, CHUNK), :] = normed_rows(other_ref, x, start, multiplier, shift)
-        return carry
-
-    lax.fori_loop(0, count * steps, step, 0)
-    pairs = dot(hidden_ref[...], wkv_ref[...]).astype(BF16)
-    for y in range(out_ref.shape[0]):
-        out_ref[y] = pairs
+    rows = ctx_ref[...].astype(F32)
+    mean = jnp.mean(rows * rows, axis=-1, keepdims=True)
+    hidden = (rows * lax.rsqrt(mean + NORM_EPS) * multiplier + shift).astype(BF16)
+    pairs = dot(hidden, wkv_ref[...]).astype(BF16)
+    for z in range(out_ref.shape[0]):
+        out_ref[z] = pairs
 
 
 def attention_kernel(
-    place_ref, sink_ref, q_ref, low_ref, kv_ref, high_ref, ctx_ref, weight_ref,
-    keep_ref, send_ref, padded_ref, attended_ref, gathered_ref,
+    place_ref, sink_ref, q_ref, low_ref, kv_ref, high_ref, ctx_ref, attended_ref, padded_ref,
 ):
     reach = WINDOW_REACH
     total = kv_ref.shape[0]
-    core, first, last = place_ref[0], place_ref[1], place_ref[2]
+    first, last = place_ref[0], place_ref[1]
     padded_ref[:reach, :] = low_ref[...]
     padded_ref[reach : reach + total, :] = kv_ref[...]
     padded_ref[reach + total :, :] = high_ref[...]
-    ctx = ctx_ref[...].reshape(-1, 2 * HEAD_DIM)
-    ctx_keys, ctx_values = ctx[:, :HEAD_DIM], ctx[:, HEAD_DIM:]
+    ctx_keys, ctx_values = ctx_ref[:, :HEAD_DIM], ctx_ref[:, HEAD_DIM:]
     factor = HEAD_DIM ** (-0.5) * LOG2_E
     row = lax.broadcasted_iota(jnp.int32, (2 * reach, 1), 0)
     sink = jnp.where(row < reach, sink_ref[0], sink_ref[1]) * LOG2_E
@@ -202,38 +175,37 @@
         return carry
 
     lax.fori_loop(0, blocks, step, 0)
-    rows = keep_ref.shape[0] // 4
-    for x in range(4):
-        mine = pl.multiple_of((2 * x + core) * rows, CHUNK)
-        theirs = pl.multiple_of((2 * x + 1 - core) * rows, CHUNK)
-        keep_ref[x * rows : (x + 1) * rows, :] = attended_ref[pl.ds(mine, rows), :]
-        gathered_ref[x * rows : (x + 1) * rows, :] = attended_ref[pl.ds(theirs, rows), :]
+
+
+def project_kernel(
+    source_ref, attended_ref, w0_ref, w1_ref, w2_ref, w3_ref, send_ref, keep_ref, rows_ref
+):
+    weights = (w0_ref, w1_ref, w2_ref, w3_ref)
+    core = source_ref[4]
+    rows = send_ref.shape[0]
+    deep = attended_ref.shape[2]
+    mine = pl.multiple_of(core * rows, CHUNK)
+    theirs = pl.multiple_of((1 - core) * rows, CHUNK)
+    for j in range(4):
+        cut = slice(j * deep, (j + 1) * deep)
+        rows_ref[:rows, cut] = attended_ref[source_ref[j], pl.ds(theirs, rows), :]
+        rows_ref[rows:, cut] = attended_ref[source_ref[j], pl.ds(mine, rows), :]
     width = 512
     for n in range(0, send_ref.shape[1], width):
-        send_ref[:, n : n + width] = dot(
-            gathered_ref[...], weight_ref[:, n : n + width]
-        ).astype(BF16)
-
-
-def pair_kernel(keep_ref, weight_ref, got_ref, out_ref):
-    width = 512
-    count, rows, _ = out_ref.shape
-    for n in range(0, got_ref.shape[1], width):
         cut = slice(n, n + width)
-        both = dot(keep_ref[...], weight_ref[:, cut]) + got_ref[:, cut].astype(F32)
-        out_ref[:, :, cut] = both.astype(BF16).reshape(count, rows, width)
-
-
-def final_kernel(latent_ref, mixed_ref, planes_ref, out_ref):
-    count = mixed_ref.shape[0]
-    columns = planes_ref.shape[2] // 5
-    gate = row_vector(planes_ref, 4, columns)
+        total = dot(rows_ref[:, :deep], w0_ref[:, cut])
+        for j in range(1, 4):
+            total = total + dot(rows_ref[:, j * deep : (j + 1) * deep], weights[j][:, cut])
+        send_ref[:, cut] = total[:rows].astype(BF16)
+        keep_ref[:, cut] = total[rows:]
+
+
+def final_kernel(latent_ref, keep_ref, got_ref, planes_ref, out_ref):
+    gate = row_vector(planes_ref, 4, planes_ref.shape[2] // 5)
 
     def step(i, carry):
         cut = pl.ds(pl.multiple_of(i * CHUNK, CHUNK), CHUNK)
-        mixed = mixed_ref[0, cut, :].astype(F32)
-        for x in range(1, count):
-            mixed = mixed + mixed_ref[x, cut, :].astype(F32)
+        mixed = keep_ref[cut, :] + got_ref[cut, :].astype(F32)
         out_ref[cut, :] = (latent_ref[cut, :].astype(F32) + gate * mixed).astype(BF16)
         return carry
 
@@ -243,11 +215,11 @@
 SHIFTS = (0, 1, 3, 2)
 
 
-def from_all_x(block):
-    got = [block]
+def from_other_x(block):
+    got = []
     for shift in SHIFTS[1:]:
         got.append(lax.ppermute(block, "x", [(i, (i + shift) % 4) for i in range(4)]))
-    return jnp.stack(got)
+    return got
 
 
 def swapped(x):
@@ -285,42 +257,40 @@
     place = lax.axis_index(SP)
     core = lax.axis_index("c").astype(jnp.int32)
     gain = norm_gain.reshape(1, width)
-    member = lax.axis_index(TP).astype(jnp.int32)
-    share = context.shape[0] // (nx * nc)
+    at_x = lax.axis_index("x").astype(jnp.int32)
     parts = pl.pallas_call(
         parts_kernel,
-        out_shape=shape_of((nz, share + 2, width), BF16),
-        in_specs=[SMEM] + [VMEM] * 6,
+        out_shape=shape_of((nz, 1, 5 * columns), F32),
+        in_specs=[VMEM] * 5,
         out_specs=VMEM,
         name="parts",
     )(
-        member[None],
         condition.reshape(1, -1),
         context_condition.reshape(1, -1),
         shift_weight,
         scale_weight,
         gate_weight,
-        context,
     )
     parts = exchanged(parts, "z")
-    latent_x = from_all_x(latent)
-    sums = jnp.sum(parts[:, share:, : 5 * columns].astype(F32), axis=(0, 1)).reshape(1, -1)
-    planes = exchanged(copies(sums, PLANE), PLANE)
-    ctx_x = from_all_x(parts[:, :share].reshape(nz * share, width))
-    latent_c = swapped(latent_x)
-    ctx_c = swapped(ctx_x)
+    latent_others = from_other_x(latent)
     pair_weight = jnp.concatenate([key_matrix, value_matrix], axis=1)
     cosine, sine = tables(place * group_rows + jnp.arange(group_rows, dtype=jnp.int32))
-    ctx_pairs = pl.pallas_call(
+    planes = exchanged(copies(jnp.sum(parts, axis=0), PLANE), PLANE)
+    out_others = from_other_x(out_weight)
+    latent_x = jnp.stack([latent, *latent_others])
+    latent_c = swapped(latent_x)
+    ctx_rows = context.shape[0]
+    pairs = pl.pallas_call(
         context_kernel,
-        out_shape=shape_of((ny, nx * nc * nz * share, 2 * HEAD_DIM), BF16),
-        in_specs=[VMEM] * 5,
+        out_shape=shape_of((nz, ctx_rows, 2 * HEAD_DIM), BF16),
+        in_specs=[VMEM] * 4,
         out_specs=VMEM,
-        scratch_shapes=[pltpu.VMEM((nx * nc * nz * share, width), BF16)],
         name="context_pairs",
-    )(ctx_x, ctx_c, planes, gain, pair_weight)
-    ctx_pairs = exchanged(ctx_pairs, "y")
-    sources = (lax.axis_index("x").astype(jnp.int32) - jnp.array(SHIFTS, jnp.int32)) % nx
+    )(context, planes, gain, pair_weight)
+    ctx_z = exchanged(pairs, "z")
+    ctx_pairs = exchanged(copies(ctx_z.reshape(nz * ctx_rows, -1), "y"), "y")
+    ctx_pairs = ctx_pairs.reshape(-1, 2 * HEAD_DIM)
+    sources = (at_x - jnp.array(SHIFTS, jnp.int32)) % nx
     bases = jnp.concatenate([2 * sources + core, 2 * sources + 1 - core]) * rows
     queries, pairs = pl.pallas_call(
         qkv_kernel,
@@ -335,44 +305,37 @@
     )(bases, latent_x, latent_c, planes, gain, query_weight, pair_weight, cosine, sine)
     count = nz * ny
     forward = [(i, i + 1) for i in range(count - 1)]
+    low = lax.ppermute(pairs[group_rows - WINDOW_REACH :], SP, forward)
     backward = [(i + 1, i) for i in range(count - 1)]
-    low = lax.ppermute(pairs[group_rows - WINDOW_REACH :], SP, forward)
     high = lax.ppermute(pairs[:WINDOW_REACH], SP, backward)
-    where = jnp.stack(
-        [core, (place == 0).astype(jnp.int32), (place == count - 1).astype(jnp.int32)]
-    )
-    half = group_rows // nc
-    keep, send = pl.pallas_call(
+    where = jnp.stack([(place == 0).astype(jnp.int32), (place == count - 1).astype(jnp.int32)])
+    attended = pl.pallas_call(
         attention_kernel,
-        out_shape=(
-            shape_of((half, 2 * HEAD_DIM), BF16),
-            shape_of((half, width), BF16),
-        ),
-        in_specs=[SMEM] * 2 + [VMEM] * 6,
-        out_specs=(VMEM, VMEM),
+        out_shape=shape_of((group_rows, 2 * HEAD_DIM), BF16),
+        in_specs=[SMEM] * 2 + [VMEM] * 5,
+        out_specs=VMEM,
         scratch_shapes=[
             pltpu.VMEM((group_rows + 2 * WINDOW_REACH, 2 * HEAD_DIM), BF16),
-            pltpu.VMEM((group_rows, 2 * HEAD_DIM), BF16),
-            pltpu.VMEM((half, 2 * HEAD_DIM), BF16),
         ],
         name="attention",
-    )(where, sink_logit_head, queries, low, pairs, high, ctx_pairs, out_weight)
+    )(where, sink_logit_head, queries, low, pairs, high, ctx_pairs)
+    attended = exchanged(attended.reshape(nx, nc * rows, 2 * HEAD_DIM), "x")
+    send, keep = pl.pallas_call(
+        project_kernel,
+        out_shape=(shape_of((rows, width), BF16), shape_of((rows, width), F32)),
+        in_specs=[SMEM] + [VMEM] * 5,
+        out_specs=(VMEM, VMEM),
+        scratch_shapes=[pltpu.VMEM((nc * rows, nx * 2 * HEAD_DIM), BF16)],
+        name="project",
+    )(jnp.concatenate([sources, core[None]]), attended, out_weight, *out_others)
     got = swapped(send)
-    paired = pl.pallas_call(
-        pair_kernel,
-        out_shape=shape_of((nx, rows, width), BF16),
-        in_specs=[VMEM] * 3,
-        out_specs=VMEM,
-        name="pair",
-    )(keep, out_weight, got)
-    mixed = exchanged(paired, "x")
     return pl.pallas_call(
         final_kernel,
         out_shape=shape_of((rows, width), BF16),
-        in_specs=[VMEM] * 3,
+        in_specs=[VMEM] * 4,
         out_specs=VMEM,
         name="final",
-    )(latent, mixed, planes)
+    )(latent, keep, got, planes)
 
 
 def solution(mesh):

time: 158 us -> 164 us (1.038)
  the two profiles are of different devices: /device:TPU:24 before, /device:TPU:25 now
where the time goes in v3:
time: 164 us; the launch traced here: 163 us
  starting transfers between devices  82.5 us (50%)
  waiting for transfers between devices  37.7 us (23%)
  Pallas kernels  27.2 us (17%)
  other arithmetic  8.03 us (5%)
  local copies, waits for them, and re-layouts  7.43 us (5%)
    all_to_all x5, starting transfers between devices, exchanged(): return lax.all_to_all(blocks, axis, 0, 0, tiled=True)  46.6 us
    all_to_all x5, waiting for transfers between devices, exchanged(): return lax.all_to_all(blocks, axis, 0, 0, tiled=True)  31.5 us
    ppermute x6, starting transfers between devices, from_other_x(): lax.ppermute(block, 'x', [(i, (i + shift) % 4) for i in range(4)])  19.1 us
    ppermute x2, starting transfers between devices, swapped(): return lax.ppermute(x, 'c', [(0, 1), (1, 0)])  10.6 us
    pallas_call x1, Pallas kernels, shards(): pl.pallas_call(qkv_kernel, out_shape=(shape_of((group_rows, 2 * HEAD_DIM)...  9.22 us
    pallas_call x1, Pallas kernels, shards(): pl.pallas_call(attention_kernel, out_shape=shape_of((group_rows, 2 * HEAD...  7.49 us
    unnamed x27, local copies, waits for them, and re-layouts  4.79 us
    ppermute x1, waiting for transfers between devices, shards(): high = lax.ppermute(pairs[:WINDOW_REACH], SP, backward)  4.57 us
  transfers between devices with their start and end apart: 15, of which 6 were waited for; matrix products, arithmetic and copies ran while one was open for 7% of the time, Pallas kernels for 13%

profile of v3, /device:TPU:25, one launch (start us, length us, event | category | flops | bytes accessed | tf_op | source)
XLA Modules:
  0.0 163.1 jit_solution(14657767247357786344)
XLA Ops:
  0.0 4.8 %collective-permute-start.2 = (bf16[96,2048]{1,0:T(8,128)(2,1)}, bf16[96,2048]{1,0:T(8,128)(2,1)S(1)}, u32[]{:S(2)}, u32[]{:S(2)}) collective-permute-start(bf16[96,2048]{1,0:T(8,128)(2,1)} %latent_ref.1), channel_id=1, source_target_pairs={{0,4},{2,6},{4,0},{6,2},{1,5},{3,7},{5,1},{7,3},{8,12},{10,14},{12... | collective-permute-start | bytes 1179656 | tf_op jit(solution)/shard_map/ppermute | solution.py:221
  4.8 2.8 %collective-permute-start.1 = (bf16[96,2048]{1,0:T(8,128)(2,1)}, bf16[96,2048]{1,0:T(8,128)(2,1)S(1)}, u32[]{:S(2)}, u32[]{:S(2)}) collective-permute-start(bf16[96,2048]{1,0:T(8,128)(2,1)} %latent_ref.1), channel_id=1, source_target_pairs={{0,6},{2,0},{4,2},{6,4},{1,7},{3,1},{5,3},{7,5},{8,14},{10,8},{12,... | collective-permute-start | bytes 1179656 | tf_op jit(solution)/shard_map/ppermute | solution.py:221
  7.6 2.5 %collective-permute-start = (bf16[96,2048]{1,0:T(8,128)(2,1)}, bf16[96,2048]{1,0:T(8,128)(2,1)S(1)}, u32[]{:S(2)}, u32[]{:S(2)}) collective-permute-start(bf16[96,2048]{1,0:T(8,128)(2,1)} %latent_ref.1), channel_id=1, source_target_pairs={{0,2},{2,4},{4,6},{6,0},{1,3},{3,5},{5,7},{7,1},{8,10},{10,12},{12... | collective-permute-start | bytes 1179656 | tf_op jit(solution)/shard_map/ppermute | solution.py:221
  10.1 2.2 %collective-permute-start.6 = (bf16[256,2048]{1,0:T(8,128)(2,1)}, bf16[256,2048]{1,0:T(8,128)(2,1)}, u32[]{:S(2)}, u32[]{:S(2)}) collective-permute-start(bf16[256,2048]{1,0:T(8,128)(2,1)} %w0_ref.1), channel_id=1, source_target_pairs={{0,2},{2,4},{4,6},{6,0},{1,3},{3,5},{5,7},{7,1},{8,10},{10,12},{12... | collective-permute-start | bytes 3145736 | tf_op jit(solution)/shard_map/ppermute | solution.py:221
  12.3 4.3 %collective-permute-start.7 = (bf16[256,2048]{1,0:T(8,128)(2,1)}, bf16[256,2048]{1,0:T(8,128)(2,1)}, u32[]{:S(2)}, u32[]{:S(2)}) collective-permute-start(bf16[256,2048]{1,0:T(8,128)(2,1)} %w0_ref.1), channel_id=1, source_target_pairs={{0,6},{2,0},{4,2},{6,4},{1,7},{3,1},{5,3},{7,5},{8,14},{10,8},{12,... | collective-permute-start | bytes 3145736 | tf_op jit(solution)/shard_map/ppermute | solution.py:221
  18.2 14.9 %all-to-all-start = ((f32[16,1,1280]{2,1,0:T(1,128)}), f32[16,1,1280]{2,1,0:T(1,128)S(1)}, u32[]{:S(2)}, u32[]{:S(2)}) async-start(f32[16,1,1280]{2,1,0:T(1,128)} %parts.1), calls=%async_computation | async-start | bytes 163840 | tf_op jit(solution)/shard_map/all_to_all | solution.py:37
  34.3 2.5 %collective-permute-start.8 = (bf16[256,2048]{1,0:T(8,128)(2,1)}, bf16[256,2048]{1,0:T(8,128)(2,1)}, u32[]{:S(2)}, u32[]{:S(2)}) collective-permute-start(bf16[256,2048]{1,0:T(8,128)(2,1)} %w0_ref.1), channel_id=1, source_target_pairs={{0,4},{2,6},{4,0},{6,2},{1,5},{3,7},{5,1},{7,3},{8,12},{10,14},{12... | collective-permute-start | bytes 3145736 | tf_op jit(solution)/shard_map/ppermute | solution.py:221
  39.0 4.4 %collective-permute-start.3 = (bf16[4,96,2048]{2,1,0:T(8,128)(2,1)S(1)}, bf16[4,96,2048]{2,1,0:T(8,128)(2,1)}, u32[]{:S(2)}, u32[]{:S(2)}) collective-permute-start(bf16[4,96,2048]{2,1,0:T(8,128)(2,1)S(1)} %pad_maximum_fusion.own_ref), channel_id=1, source_target_pairs={{0,1},{1,0},{2,3},{3,2},{4,5},{5,4},{6,7},{7,6},{8,9},{9,8},{10,11... | collective-permute-start | bytes 4718600 | tf_op jit(solution)/shard_map/ppermute | solution.py:226
  45.8 8.6 %all-to-all-start.1 = ((f32[32,1,1280]{2,1,0:T(1,128)}), f32[32,1,1280]{2,1,0:T(1,128)S(1)}, u32[]{:S(2)}, u32[]{:S(2)}) async-start(f32[32,1,1280]{2,1,0:T(1,128)} %broadcast_in_dim.30), calls=%async_computation.1 | async-start | bytes 327680 | tf_op jit(solution)/shard_map/all_to_all | solution.py:37
  54.4 17.2 %all-to-all-done.1.planes_ref = f32[32,1,1280]{2,1,0:T(1,128)S(1)} async-done(((f32[32,1,1280]{2,1,0:T(1,128)}), f32[32,1,1280]{2,1,0:T(1,128)S(1)}, u32[]{:S(2)}, u32[]{:S(2)}) %all-to-all-start.1) | async-done | bytes 163872 | tf_op jit(solution)/shard_map/all_to_all | solution.py:37
  72.3 2.4 %context_pairs.1 = bf16[16,16,256]{2,1,0:T(8,128)(2,1)} custom-call(bf16[16,2048]{1,0:T(8,128)(2,1)} %ctx_ref.1, f32[32,1,1280]{2,1,0:T(1,128)} %copy-done.2, f32[1,2048]{1,0:T(1,128)} %bitcast.20, bf16[2048,256]{1,0:T(8,128)(2,1)} %copy-done), custom_call_target="tpu_custom_call" | custom-call | tf_op jit(solution)/shard_map/context_pairs/pallas_call | solution.py:283
  74.6 13.6 %all-to-all-start.2 = ((bf16[16,16,256]{2,1,0:T(8,128)(2,1)}), bf16[16,16,256]{2,1,0:T(8,128)(2,1)S(1)}, u32[]{:S(2)}, u32[]{:S(2)}) async-start(bf16[16,16,256]{2,1,0:T(8,128)(2,1)} %context_pairs.1), calls=%async_computation.2 | async-start | bytes 262144 | tf_op jit(solution)/shard_map/all_to_all | solution.py:37
  88.2 3.6 %sine_multiply_fusion = (f32[768,128]{1,0:T(8,128)}, f32[768,128]{1,0:T(8,128)}) fusion(f32[128]{0:T(128)S(1)} %compare_select_fusion.2, f32[768,32]{1,0:T(8,128)} %get-tuple-element.20, f32[768,32]{1,0:T(8,128)S(1)} %get-tuple-element.19), kind=kLoop, calls=%fused_computation.2 | loop fusion | flops 393216 | bytes 983552 | tf_op jit(solution)/shard_map/mul | solution.py:235
  91.8 8.5 %all-to-all-done.2 = bf16[16,16,256]{2,1,0:T(8,128)(2,1)S(1)} async-done(((bf16[16,16,256]{2,1,0:T(8,128)(2,1)}), bf16[16,16,256]{2,1,0:T(8,128)(2,1)S(1)}, u32[]{:S(2)}, u32[]{:S(2)}) %all-to-all-start.2) | async-done | bytes 131104 | tf_op jit(solution)/shard_map/all_to_all | solution.py:37
  101.2 5.3 %all-to-all-start.3 = ((bf16[4,256,256]{2,1,0:T(8,128)(2,1)}), bf16[4,256,256]{2,1,0:T(8,128)(2,1)S(1)}, u32[]{:S(2)}, u32[]{:S(2)}) async-start(bf16[4,256,256]{2,1,0:T(8,128)(2,1)} %broadcast_in_dim.34), calls=%async_computation.3 | async-start | bytes 1048576 | tf_op jit(solution)/shard_map/all_to_all | solution.py:37
  107.2 9.2 %qkv.1 = (bf16[768,256]{1,0:T(8,128)(2,1)}, bf16[768,256]{1,0:T(8,128)(2,1)}) custom-call(s32[8]{0:T(128)} %add_multiply_fusion.base_ref, bf16[4,96,2048]{2,1,0:T(8,128)(2,1)} %copy-done.1, bf16[4,96,2048]{2,1,0:T(8,128)(2,1)} %collective-permute-done.3.other_ref, f32[32,1,1280]{2,1,0:T(1,128)} %copy-done.2, f32[1,2048]{1,0:T(1,128)} %bitcast.21, ...), custom_call_target="tpu_custom_call" | custom-call | tf_op jit(solution)/shard_map/qkv/pallas_call | solution.py:295
  117.3 4.3 %collective-permute-start.4 = (bf16[128,256]{1,0:T(8,128)(2,1)S(1)}, bf16[128,256]{1,0:T(8,128)(2,1)S(1)}, u32[]{:S(2)}, u32[]{:S(2)}) collective-permute-start(bf16[128,256]{1,0:T(8,128)(2,1)S(1)} %get-tuple-element.18), channel_id=1, source_target_pairs={{0,8},{8,16},{16,24},{24,32},{32,40},{40,48},{48,56},{56,64},{64,7... | collective-permute-start | bytes 196616 | tf_op jit(solution)/shard_map/ppermute | solution.py:308
  124.2 4.6 %collective-permute-done.5.high_ref = bf16[128,256]{1,0:T(8,128)(2,1)S(1)} collective-permute-done((bf16[128,256]{1,0:T(8,128)(2,1)S(1)}, bf16[128,256]{1,0:T(8,128)(2,1)S(1)}, u32[]{:S(2)}, u32[]{:S(2)}) %collective-permute-start.5) | collective-permute-done | bytes 65568 | tf_op jit(solution)/shard_map/ppermute | solution.py:310
  129.4 7.5 %attention.1 = bf16[768,256]{1,0:T(8,128)(2,1)} custom-call(s32[2]{0:T(128)} %add_convert_fusion.place_ref, f32[2]{0:T(128)} %sink_ref.1, bf16[768,256]{1,0:T(8,128)(2,1)} %get-tuple-element.9.q_ref, bf16[128,256]{1,0:T(8,128)(2,1)} %copy-done.10, bf16[768,256]{1,0:T(8,128)(2,1)} %get-tuple-element.10.kv_ref, bf16[128,256]{1,0:T(8,128)(2,1)} %copy-done.11, ...), custom_call_target="tpu_custom_call" | custom-call | tf_op jit(solution)/shard_map/attention/pallas_call | solution.py:312
  136.9 4.2 %all-to-all-start.4 = ((bf16[4,192,256]{2,1,0:T(8,128)(2,1)}), bf16[4,192,256]{2,1,0:T(8,128)(2,1)S(1)}, u32[]{:S(2)}, u32[]{:S(2)}) async-start(bf16[4,192,256]{2,1,0:T(8,128)(2,1)} %bitcast.15), calls=%async_computation.4 | async-start | bytes 786432 | tf_op jit(solution)/shard_map/all_to_all | solution.py:37
  141.7 5.6 %all-to-all-done.4.attended_ref = bf16[4,192,256]{2,1,0:T(8,128)(2,1)S(1)} async-done(((bf16[4,192,256]{2,1,0:T(8,128)(2,1)}), bf16[4,192,256]{2,1,0:T(8,128)(2,1)S(1)}, u32[]{:S(2)}, u32[]{:S(2)}) %all-to-all-start.4) | async-done | bytes 393248 | tf_op jit(solution)/shard_map/all_to_all | solution.py:37
  148.0 4.3 %project.1 = (bf16[96,2048]{1,0:T(8,128)(2,1)}, f32[96,2048]{1,0:T(8,128)}) custom-call(s32[5]{0:T(128)} %pad_add_fusion.source_ref, bf16[4,192,256]{2,1,0:T(8,128)(2,1)} %copy-done.5, bf16[256,2048]{1,0:T(8,128)(2,1)} %w0_ref.1, bf16[256,2048]{1,0:T(8,128)(2,1)} %collective-permute-done.6.w1_ref, bf16[256,2048]{1,0:T(8,128)(2,1)} %collective-permute-done.7.w2_ref, ...), custom_call_target="tpu_custom_call" | custom-call | tf_op jit(solution)/shard_map/project/pallas_call | solution.py:323
  152.3 6.2 %collective-permute-start.9 = (bf16[96,2048]{1,0:T(8,128)(2,1)}, bf16[96,2048]{1,0:T(8,128)(2,1)S(1)}, u32[]{:S(2)}, u32[]{:S(2)}) collective-permute-start(bf16[96,2048]{1,0:T(8,128)(2,1)} %get-tuple-element.12), channel_id=1, source_target_pairs={{0,1},{1,0},{2,3},{3,2},{4,5},{5,4},{6,7},{7,6},{8,9},{9,8},{10,11... | collective-permute-start | bytes 1179656 | tf_op jit(solution)/shard_map/ppermute | solution.py:226
  160.8 2.3 %final.1 = bf16[96,2048]{1,0:T(8,128)(2,1)} custom-call(bf16[96,2048]{1,0:T(8,128)(2,1)} %latent_ref.1, f32[96,2048]{1,0:T(8,128)} %get-tuple-element.11.keep_ref, bf16[96,2048]{1,0:T(8,128)(2,1)} %copy-done.9, f32[32,1,1280]{2,1,0:T(1,128)} %copy-done.2), custom_call_target="tpu_custom_call" | custom-call | tf_op jit(solution)/shard_map/final/pallas_call | solution.py:332
  (55 shorter events, 17.2 us)
Async XLA Ops:
  0.0 37.7 %copy-start.4 = (bf16[96,2048]{1,0:T(8,128)(2,1)S(1)}, bf16[96,2048]{1,0:T(8,128)(2,1)}, u32[]{:S(2)}) copy-start(bf16[96,2048]{1,0:T(8,128)(2,1)} %latent_ref.1) | copy-start | bytes 1179652
  0.0 34.2 %collective-permute-start.2 = (bf16[96,2048]{1,0:T(8,128)(2,1)}, bf16[96,2048]{1,0:T(8,128)(2,1)S(1)}, u32[]{:S(2)}, u32[]{:S(2)}) collective-permute-start(bf16[96,2048]{1,0:T(8,128)(2,1)} %latent_ref.1), channel_id=1, source_target_pairs={{0,4},{2,6},{4,0},{6,2},{1,5},{3,7},{5,1},{7,3},{8,12},{10,14},{12... | collective-permute-start | bytes 1179656 | tf_op jit(solution)/shard_map/ppermute | solution.py:221
  4.8 32.0 %collective-permute-start.1 = (bf16[96,2048]{1,0:T(8,128)(2,1)}, bf16[96,2048]{1,0:T(8,128)(2,1)S(1)}, u32[]{:S(2)}, u32[]{:S(2)}) collective-permute-start(bf16[96,2048]{1,0:T(8,128)(2,1)} %latent_ref.1), channel_id=1, source_target_pairs={{0,6},{2,0},{4,2},{6,4},{1,7},{3,1},{5,3},{7,5},{8,14},{10,8},{12,... | collective-permute-start | bytes 1179656 | tf_op jit(solution)/shard_map/ppermute | solution.py:221
  7.6 29.2 %collective-permute-start = (bf16[96,2048]{1,0:T(8,128)(2,1)}, bf16[96,2048]{1,0:T(8,128)(2,1)S(1)}, u32[]{:S(2)}, u32[]{:S(2)}) collective-permute-start(bf16[96,2048]{1,0:T(8,128)(2,1)} %latent_ref.1), channel_id=1, source_target_pairs={{0,2},{2,4},{4,6},{6,0},{1,3},{3,5},{5,7},{7,1},{8,10},{10,12},{12... | collective-permute-start | bytes 1179656 | tf_op jit(solution)/shard_map/ppermute | solution.py:221
  10.1 131.6 %collective-permute-start.6 = (bf16[256,2048]{1,0:T(8,128)(2,1)}, bf16[256,2048]{1,0:T(8,128)(2,1)}, u32[]{:S(2)}, u32[]{:S(2)}) collective-permute-start(bf16[256,2048]{1,0:T(8,128)(2,1)} %w0_ref.1), channel_id=1, source_target_pairs={{0,2},{2,4},{4,6},{6,0},{1,3},{3,5},{5,7},{7,1},{8,10},{10,12},{12... | collective-permute-start | bytes 3145736 | tf_op jit(solution)/shard_map/ppermute | solution.py:221
  12.3 129.4 %collective-permute-start.7 = (bf16[256,2048]{1,0:T(8,128)(2,1)}, bf16[256,2048]{1,0:T(8,128)(2,1)}, u32[]{:S(2)}, u32[]{:S(2)}) collective-permute-start(bf16[256,2048]{1,0:T(8,128)(2,1)} %w0_ref.1), channel_id=1, source_target_pairs={{0,6},{2,0},{4,2},{6,4},{1,7},{3,1},{5,3},{7,5},{8,14},{10,8},{12,... | collective-permute-start | bytes 3145736 | tf_op jit(solution)/shard_map/ppermute | solution.py:221
  18.2 26.8 %all-to-all-start = ((f32[16,1,1280]{2,1,0:T(1,128)}), f32[16,1,1280]{2,1,0:T(1,128)S(1)}, u32[]{:S(2)}, u32[]{:S(2)}) async-start(f32[16,1,1280]{2,1,0:T(1,128)} %parts.1), calls=%async_computation | async-start | bytes 163840 | tf_op jit(solution)/shard_map/all_to_all | solution.py:37
  34.3 107.5 %collective-permute-start.8 = (bf16[256,2048]{1,0:T(8,128)(2,1)}, bf16[256,2048]{1,0:T(8,128)(2,1)}, u32[]{:S(2)}, u32[]{:S(2)}) collective-permute-start(bf16[256,2048]{1,0:T(8,128)(2,1)} %w0_ref.1), channel_id=1, source_target_pairs={{0,4},{2,6},{4,0},{6,2},{1,5},{3,7},{5,1},{7,3},{8,12},{10,14},{12... | collective-permute-start | bytes 3145736 | tf_op jit(solution)/shard_map/ppermute | solution.py:221
  36.8 0.9 copy-start.8
  37.7 5.8 %copy-start.6 = (bf16[2048,128]{1,0:T(8,128)(2,1)S(1)}, bf16[2048,128]{1,0:T(8,128)(2,1)}, u32[]{:S(2)}) copy-start(bf16[2048,128]{1,0:T(8,128)(2,1)} %param.24) | copy-start | bytes 1572868
  39.0 68.2 %copy-start.1 = (bf16[4,96,2048]{2,1,0:T(8,128)(2,1)}, bf16[4,96,2048]{2,1,0:T(8,128)(2,1)S(1)}, u32[]{:S(2)}) copy-start(bf16[4,96,2048]{2,1,0:T(8,128)(2,1)S(1)} %pad_maximum_fusion.own_ref) | copy-start | bytes 4718596
  39.0 15.4 %copy-start.12 = (s32[4]{0:T(128)S(1)}, s32[4]{0:T(128)}, u32[]{:S(2)}) copy-start(s32[4]{0:T(128)} %constant.103) | copy-start | bytes 52
  39.0 68.1 %collective-permute-start.3 = (bf16[4,96,2048]{2,1,0:T(8,128)(2,1)S(1)}, bf16[4,96,2048]{2,1,0:T(8,128)(2,1)}, u32[]{:S(2)}, u32[]{:S(2)}) collective-permute-start(bf16[4,96,2048]{2,1,0:T(8,128)(2,1)S(1)} %pad_maximum_fusion.own_ref), channel_id=1, source_target_pairs={{0,1},{1,0},{2,3},{3,2},{4,5},{5,4},{6,7},{7,6},{8,9},{9,8},{10,11... | collective-permute-start | bytes 4718600 | tf_op jit(solution)/shard_map/ppermute | solution.py:226
  43.6 28.0 %copy-start = (bf16[2048,256]{1,0:T(8,128)(2,1)}, bf16[2048,256]{1,0:T(8,128)(2,1)S(1)}, u32[]{:S(2)}) copy-start(bf16[2048,256]{1,0:T(8,128)(2,1)S(1)} %constant_dynamic-update-slice_fusion.wkv_ref) | copy-start | bytes 3145732
  45.8 25.8 %all-to-all-start.1 = ((f32[32,1,1280]{2,1,0:T(1,128)}), f32[32,1,1280]{2,1,0:T(1,128)S(1)}, u32[]{:S(2)}, u32[]{:S(2)}) async-start(f32[32,1,1280]{2,1,0:T(1,128)} %broadcast_in_dim.30), calls=%async_computation.1 | async-start | bytes 327680 | tf_op jit(solution)/shard_map/all_to_all | solution.py:37
  74.6 25.7 %all-to-all-start.2 = ((bf16[16,16,256]{2,1,0:T(8,128)(2,1)}), bf16[16,16,256]{2,1,0:T(8,128)(2,1)S(1)}, u32[]{:S(2)}, u32[]{:S(2)}) async-start(bf16[16,16,256]{2,1,0:T(8,128)(2,1)} %context_pairs.1), calls=%async_computation.2 | async-start | bytes 262144 | tf_op jit(solution)/shard_map/all_to_all | solution.py:37
  101.2 23.0 %all-to-all-start.3 = ((bf16[4,256,256]{2,1,0:T(8,128)(2,1)}), bf16[4,256,256]{2,1,0:T(8,128)(2,1)S(1)}, u32[]{:S(2)}, u32[]{:S(2)}) async-start(bf16[4,256,256]{2,1,0:T(8,128)(2,1)} %broadcast_in_dim.34), calls=%async_computation.3 | async-start | bytes 1048576 | tf_op jit(solution)/shard_map/all_to_all | solution.py:37
  117.3 6.9 %collective-permute-start.4 = (bf16[128,256]{1,0:T(8,128)(2,1)S(1)}, bf16[128,256]{1,0:T(8,128)(2,1)S(1)}, u32[]{:S(2)}, u32[]{:S(2)}) collective-permute-start(bf16[128,256]{1,0:T(8,128)(2,1)S(1)} %get-tuple-element.18), channel_id=1, source_target_pairs={{0,8},{8,16},{16,24},{24,32},{32,40},{40,48},{48,56},{56,64},{64,7... | collective-permute-start | bytes 196616 | tf_op jit(solution)/shard_map/ppermute | solution.py:308
  121.6 7.1 %collective-permute-start.5 = (bf16[128,256]{1,0:T(8,128)(2,1)S(1)}, bf16[128,256]{1,0:T(8,128)(2,1)S(1)}, u32[]{:S(2)}, u32[]{:S(2)}) collective-permute-start(bf16[128,256]{1,0:T(8,128)(2,1)S(1)} %get-tuple-element.17), channel_id=1, source_target_pairs={{8,0},{16,8},{24,16},{32,24},{40,32},{48,40},{56,48},{64,56},{72,6... | collective-permute-start | bytes 196616 | tf_op jit(solution)/shard_map/ppermute | solution.py:310
  124.2 4.6 %copy-start.3 = (bf16[4,256,256]{2,1,0:T(8,128)(2,1)}, bf16[4,256,256]{2,1,0:T(8,128)(2,1)S(1)}, u32[]{:S(2)}) copy-start(bf16[4,256,256]{2,1,0:T(8,128)(2,1)S(1)} %all-to-all-done.3) | copy-start | bytes 1572868
  124.2 4.6 %copy-start.10 = (bf16[128,256]{1,0:T(8,128)(2,1)}, bf16[128,256]{1,0:T(8,128)(2,1)S(1)}, u32[]{:S(2)}) copy-start(bf16[128,256]{1,0:T(8,128)(2,1)S(1)} %collective-permute-done.4.low_ref) | copy-start | bytes 196612
  136.9 10.4 %all-to-all-start.4 = ((bf16[4,192,256]{2,1,0:T(8,128)(2,1)}), bf16[4,192,256]{2,1,0:T(8,128)(2,1)S(1)}, u32[]{:S(2)}, u32[]{:S(2)}) async-start(bf16[4,192,256]{2,1,0:T(8,128)(2,1)} %bitcast.15), calls=%async_computation.4 | async-start | bytes 786432 | tf_op jit(solution)/shard_map/all_to_all | solution.py:37
  152.3 7.7 %collective-permute-start.9 = (bf16[96,2048]{1,0:T(8,128)(2,1)}, bf16[96,2048]{1,0:T(8,128)(2,1)S(1)}, u32[]{:S(2)}, u32[]{:S(2)}) collective-permute-start(bf16[96,2048]{1,0:T(8,128)(2,1)} %get-tuple-element.12), channel_id=1, source_target_pairs={{0,1},{1,0},{2,3},{3,2},{4,5},{5,4},{6,7},{7,6},{8,9},{9,8},{10,11... | collective-permute-start | bytes 1179656 | tf_op jit(solution)/shard_map/ppermute | solution.py:226
  160.0 0.8 copy-start.9
  (4 other events, 2.8 us)

commit v4 on v3

v4 whole, which is shorter than its diff:
```python
import jax
import jax.numpy as jnp
from jax import lax
from jax.experimental import pallas as pl
from jax.experimental.pallas import tpu as pltpu
from jax.sharding import Mesh
from jax.sharding import PartitionSpec as P

HEAD_DIM = 128
WINDOW_REACH = 128
GRID_W = 64
SP = ("z", "y")
TP = ("x", "c")
PLANE = ("y", "x", "c")
ALL = ("z", "y", "x", "c")
NORM_EPS = 1e-05
MASKED_SCORE = -1e30
LOG2_E = 1.4426950408889634
CHUNK = 16
SHIFTS = (0, 1, 3, 2)


VMEM = pl.BlockSpec(memory_space=pltpu.VMEM)
SMEM = pl.BlockSpec(memory_space=pltpu.SMEM)
F32 = jnp.float32
BF16 = jnp.bfloat16


def shape_of(shape, dtype):
    return jax.ShapeDtypeStruct(shape, dtype)


def vmem(mib):
    return pltpu.CompilerParams(vmem_limit_bytes=mib * 2**20)


def held(*arrays):
    return [pltpu.with_memory_space_constraint(a, pltpu.VMEM) for a in arrays]


def exchanged(blocks, axis):
    return lax.all_to_all(blocks, axis, 0, 0, tiled=True)


def dot(a, b):
    return jnp.dot(a, b, preferred_element_type=F32)


def row_vector(planes_ref, index, columns):
    count = planes_ref.shape[0] // 4
    cut = pl.ds(index * columns, columns)
    pieces = []
    for t in range(count):
        piece = planes_ref[t, :, cut]
        for y in range(1, 4):
            piece = piece + planes_ref[y * count + t, :, cut]
        pieces.append(piece)
    return jnp.concatenate(pieces, axis=1)


def parts_kernel(cond_ref, ctx_cond_ref, shift_ref, scale_ref, gate_ref, out_ref):
    def active(ref):
        v = ref[...]
        return (v / (1.0 + jnp.exp(-v))).astype(BF16)

    both = jnp.concatenate([active(cond_ref), active(ctx_cond_ref)], axis=0)
    both = jnp.concatenate([both, jnp.zeros((14, both.shape[1]), BF16)], axis=0)
    shift = dot(both, shift_ref[...])
    scale = dot(both, scale_ref[...])
    gate = dot(both, gate_ref[...])
    row = jnp.concatenate([shift[0:1], shift[1:2], scale[0:1], scale[1:2], gate[0:1]], axis=1)
    for i in range(out_ref.shape[0]):
        out_ref[i] = row


def normed_rows(ref, x, start, multiplier, shift):
    rows = ref[x, pl.ds(start, CHUNK), :].astype(F32)
    mean = jnp.mean(rows * rows, axis=-1, keepdims=True)
    return (rows * lax.rsqrt(mean + NORM_EPS) * multiplier + shift).astype(BF16)


def turned(u, cosine, sine):
    lane = lax.broadcasted_iota(jnp.int32, u.shape, 1)
    first = (lane % 64) < 32
    swapped = jnp.where(first, pltpu.roll(u, 96, 1), pltpu.roll(u, 32, 1))
    return u * cosine + swapped * sine


def sum_kernel(parts_ref, out_ref):
    total = parts_ref[0]
    for z in range(1, parts_ref.shape[0]):
        total = total + parts_ref[z]
    for p in range(out_ref.shape[0]):
        out_ref[p] = total


def qkv_kernel(
    place_ref, own_ref, other_ref, planes_ref, gain_ref, wq_ref, wk_ref, wv_ref, row_ref, col_ref,
    q_ref, kv_ref, top_ref, bottom_ref, hidden_ref, wkv_ref,
):
    columns = wq_ref.shape[1]
    shift = row_vector(planes_ref, 0, columns)
    multiplier = gain_ref[...] * (1.0 + row_vector(planes_ref, 2, columns))
    wkv_ref[:, :HEAD_DIM] = wk_ref[...]
    wkv_ref[:, HEAD_DIM:] = wv_ref[...]
    _, rows, _ = own_ref.shape
    at_x, core = place_ref[0], place_ref[1]
    for x, shift_x in enumerate(SHIFTS):
        source = lax.rem(at_x - shift_x + 4, 4)
        mine = (2 * source + core) * rows
        theirs = (2 * source + 1 - core) * rows

        def step(i, carry, x=x, mine=mine, theirs=theirs):
            start = pl.multiple_of(i * CHUNK, CHUNK)
            at = pl.multiple_of(mine + start, CHUNK)
            hidden_ref[pl.ds(at, CHUNK), :] = normed_rows(own_ref, x, start, multiplier, shift)
            at = pl.multiple_of(theirs + start, CHUNK)
            hidden_ref[pl.ds(at, CHUNK), :] = normed_rows(other_ref, x, start, multiplier, shift)
            return carry

        lax.fori_loop(0, rows // CHUNK, step, 0, unroll=2)
    block = 384
    lane = lax.broadcasted_iota(jnp.int32, (GRID_W, HEAD_DIM), 1) < 64
    col = col_ref[...]
    col_turned = pltpu.roll(col, 64, 1)
    row_turned = pltpu.roll(row_ref[...], 64, 1)
    factor = HEAD_DIM ** (-0.5) * LOG2_E
    for at in range(0, hidden_ref.shape[0], block):
        cut = slice(at, at + block)
        hidden = hidden_ref[cut, :]
        lines = range(at // GRID_W, (at + block) // GRID_W)
        cosine = jnp.concatenate(
            [jnp.where(lane, row_ref[g : g + 1, :], col_turned) for g in lines], axis=0
        )
        sine = jnp.concatenate(
            [jnp.where(lane, row_turned[g : g + 1, :], col) for g in lines], axis=0
        )
        queries = dot(hidden, wq_ref[...])
        for h in range(2):
            part = slice(h * HEAD_DIM, (h + 1) * HEAD_DIM)
            q_ref[cut, part] = (turned(queries[:, part], cosine, sine) * factor).astype(BF16)
        pairs = dot(hidden, wkv_ref[...])
        kv_ref[cut, :HEAD_DIM] = turned(pairs[:, :HEAD_DIM], cosine, sine).astype(BF16)
        kv_ref[cut, HEAD_DIM:] = pairs[:, HEAD_DIM:].astype(BF16)
    top_ref[...] = kv_ref[:WINDOW_REACH, :]
    bottom_ref[...] = kv_ref[hidden_ref.shape[0] - WINDOW_REACH :, :]


def context_kernel(ctx_ref, planes_ref, gain_ref, wk_ref, wv_ref, out_ref):
    columns = planes_ref.shape[2] // 5
    shift = row_vector(planes_ref, 1, columns)
    multiplier = gain_ref[...] * (1.0 + row_vector(planes_ref, 3, columns))
    rows = ctx_ref[...].astype(F32)
    mean = jnp.mean(rows * rows, axis=-1, keepdims=True)
    hidden = (rows * lax.rsqrt(mean + NORM_EPS) * multiplier + shift).astype(BF16)
    pairs = jnp.concatenate([dot(hidden, wk_ref[...]), dot(hidden, wv_ref[...])], axis=1)
    pairs = pairs.astype(BF16)
    for p in range(out_ref.shape[0]):
        out_ref[p] = pairs


def attention_kernel(
    place_ref, sink_ref, q_ref, low_ref, kv_ref, high_ref, ctx_ref, attended_ref,
    keys_ref, values_ref, ctx_values_ref,
):
    reach = WINDOW_REACH
    total = kv_ref.shape[0]
    first, last = place_ref[2], place_ref[3]
    for ref, at in ((low_ref, 0), (kv_ref, reach), (high_ref, reach + total)):
        cut = slice(at, at + ref.shape[0])
        keys_ref[cut, :] = ref[:, :HEAD_DIM]
        values_ref[cut, :HEAD_DIM] = ref[:, HEAD_DIM:]
    values_ref[:, HEAD_DIM:] = jnp.ones(keys_ref.shape, BF16)
    ctx_values_ref[:, :HEAD_DIM] = ctx_ref[:, HEAD_DIM:]
    ctx_values_ref[:, HEAD_DIM:] = jnp.ones((ctx_ref.shape[0], HEAD_DIM), BF16)
    row = lax.broadcasted_iota(jnp.int32, (2 * reach, 1), 0)
    sink = jnp.where(row < reach, sink_ref[0], sink_ref[1]) * LOG2_E
    position = lax.broadcasted_iota(jnp.int32, (2 * reach, 3 * reach), 0) % reach
    column = lax.broadcasted_iota(jnp.int32, (2 * reach, 3 * reach), 1)
    band = (column >= position) & (column <= position + 2 * reach)
    blocks = total // reach
    contract = (((1,), (1,)), ((), ()))

    def step(b, carry):
        at = pl.multiple_of(b * reach, reach)
        both = q_ref[pl.ds(at, reach), :]
        queries = jnp.concatenate([both[:, :HEAD_DIM], both[:, HEAD_DIM:]], axis=0)
        keys = keys_ref[pl.ds(at, 3 * reach), :]
        values = values_ref[pl.ds(at, 3 * reach), :]
        lowest = jnp.where(b == 0, first * reach, 0)
        highest = jnp.where(b == blocks - 1, (3 - last) * reach, 3 * reach)
        allowed = band & (column >= lowest) & (column < highest)
        near = lax.dot_general(queries, keys, contract, preferred_element_type=F32)
        near = jnp.where(allowed, near, MASKED_SCORE)
        far = lax.dot_general(
            queries, ctx_ref[:, :HEAD_DIM], contract, preferred_element_type=F32
        )
        top = jnp.maximum(
            jnp.max(near, axis=-1, keepdims=True), jnp.max(far, axis=-1, keepdims=True)
        )
        top = jnp.maximum(top, sink)
        near = jnp.exp2(near - top).astype(BF16)
        far = jnp.exp2(far - top).astype(BF16)
        mixed = dot(near, values) + dot(far, ctx_values_ref[...])
        share = mixed[:, HEAD_DIM:] + jnp.exp2(sink - top)
        mixed = (mixed[:, :HEAD_DIM] / share).astype(BF16)
        attended_ref[pl.ds(at, reach), :HEAD_DIM] = mixed[:reach]
        attended_ref[pl.ds(at, reach), HEAD_DIM:] = mixed[reach:]
        return carry

    lax.fori_loop(0, blocks, step, 0, unroll=2)


def project_kernel(
    place_ref, attended_ref, w0_ref, w1_ref, w2_ref, w3_ref, send_ref, keep_ref, rows_ref
):
    weights = (w0_ref, w1_ref, w2_ref, w3_ref)
    at_x, core = place_ref[0], place_ref[1]
    rows = send_ref.shape[0]
    deep = attended_ref.shape[2]
    mine = pl.multiple_of(core * rows, CHUNK)
    theirs = pl.multiple_of((1 - core) * rows, CHUNK)
    for j, shift_x in enumerate(SHIFTS):
        source = lax.rem(at_x - shift_x + 4, 4)
        cut = slice(j * deep, (j + 1) * deep)
        rows_ref[:rows, cut] = attended_ref[source, pl.ds(theirs, rows), :]
        rows_ref[rows:, cut] = attended_ref[source, pl.ds(mine, rows), :]
    width = 512
    for n in range(0, send_ref.shape[1], width):
        cut = slice(n, n + width)
        total = dot(rows_ref[:, :deep], w0_ref[:, cut])
        for j in range(1, 4):
            total = total + dot(rows_ref[:, j * deep : (j + 1) * deep], weights[j][:, cut])
        send_ref[:, cut] = total[:rows].astype(BF16)
        keep_ref[:, cut] = total[rows:]


def final_kernel(latent_ref, keep_ref, got_ref, planes_ref, out_ref):
    gate = row_vector(planes_ref, 4, planes_ref.shape[2] // 5)

    def step(i, carry):
        cut = pl.ds(pl.multiple_of(i * CHUNK, CHUNK), CHUNK)
        mixed = keep_ref[cut, :] + got_ref[cut, :].astype(F32)
        out_ref[cut, :] = (latent_ref[cut, :].astype(F32) + gate * mixed).astype(BF16)
        return carry

    lax.fori_loop(0, latent_ref.shape[0] // CHUNK, step, 0)


def from_other_x(block):
    got = []
    for shift in SHIFTS[1:]:
        got.append(lax.ppermute(block, "x", [(i, (i + shift) % 4) for i in range(4)]))
    return got


def swapped(x):
    return lax.ppermute(x, "c", [(0, 1), (1, 0)])


def tables(first_line, lines):
    inv_freq = 10000.0 ** (-jnp.arange(0, HEAD_DIM // 2, 2, dtype=F32) / (HEAD_DIM // 2))
    at = jnp.concatenate([first_line + jnp.arange(lines), jnp.arange(GRID_W)])
    angles = at.astype(F32)[:, None] * inv_freq
    cosine, sine = jnp.cos(angles), jnp.sin(angles)
    table = jnp.concatenate([cosine, cosine, -sine, sine], axis=1)
    return table[:lines], table[lines:]


def shards(
    latent,
    condition,
    context_condition,
    context,
    norm_gain,
    shift_weight,
    scale_weight,
    gate_weight,
    query_weight,
    key_matrix,
    value_matrix,
    sink_logit_head,
    out_weight,
):
    nz, ny, nx, nc = (lax.axis_size(a) for a in ALL)
    rows, width = latent.shape
    group_rows = rows * nx * nc
    columns = shift_weight.shape[1]
    place = lax.axis_index(SP)
    gain = norm_gain.reshape(1, width)
    parts = pl.pallas_call(
        parts_kernel,
        out_shape=shape_of((nz, 1, 5 * columns), F32),
        in_specs=[VMEM] * 5,
        out_specs=VMEM,
        name="parts",
        compiler_params=vmem(6),
    )(
        condition.reshape(1, -1),
        context_condition.reshape(1, -1),
        shift_weight,
        scale_weight,
        gate_weight,
    )
    parts = exchanged(parts, "z")
    latent_others = from_other_x(latent)
    lines, cols = tables(place * (group_rows // GRID_W), group_rows // GRID_W)
    count = nz * ny
    where = jnp.stack(
        [
            lax.axis_index("x").astype(jnp.int32),
            lax.axis_index("c").astype(jnp.int32),
            (place == 0).astype(jnp.int32),
            (place == count - 1).astype(jnp.int32),
        ]
    )
    members = ny * nx * nc
    sums = pl.pallas_call(
        sum_kernel,
        out_shape=shape_of((members, 1, 5 * columns), F32),
        in_specs=[VMEM],
        out_specs=VMEM,
        name="sums",
        compiler_params=vmem(4),
    )(*held(parts))
    planes = exchanged(sums, PLANE)
    out_others = from_other_x(out_weight)
    latent_x = jnp.stack([latent, *latent_others])
    latent_c = swapped(latent_x)
    ctx_rows = context.shape[0]
    pairs = pl.pallas_call(
        context_kernel,
        out_shape=shape_of((count, ctx_rows, 2 * HEAD_DIM), BF16),
        in_specs=[VMEM] * 5,
        out_specs=VMEM,
        name="context_pairs",
        compiler_params=vmem(8),
    )(*held(context, planes, gain, key_matrix, value_matrix))
    ctx_pairs = exchanged(pairs, SP).reshape(-1, 2 * HEAD_DIM)
    wide = (group_rows, 2 * HEAD_DIM)
    edge = (WINDOW_REACH, 2 * HEAD_DIM)
    queries, pairs, top, bottom = pl.pallas_call(
        qkv_kernel,
        out_shape=[pltpu.VMEM(shape, BF16) for shape in (wide, wide, edge, edge)],
        in_specs=[SMEM] + [VMEM] * 9,
        out_specs=[VMEM] * 4,
        scratch_shapes=[
            pltpu.VMEM((group_rows, width), BF16),
            pltpu.VMEM((width, 2 * HEAD_DIM), BF16),
        ],
        name="qkv",
        compiler_params=vmem(20),
    )(
        where,
        *held(latent_x, latent_c, planes, gain),
        *held(query_weight, key_matrix, value_matrix, lines, cols),
    )
    low = lax.ppermute(bottom, SP, [(i, i + 1) for i in range(count - 1)])
    high = lax.ppermute(top, SP, [(i + 1, i) for i in range(count - 1)])
    long = group_rows + 2 * WINDOW_REACH
    attended = pl.pallas_call(
        attention_kernel,
        out_shape=shape_of(wide, BF16),
        in_specs=[SMEM] * 2 + [VMEM] * 5,
        out_specs=VMEM,
        scratch_shapes=[
            pltpu.VMEM((long, HEAD_DIM), BF16),
            pltpu.VMEM((long, 2 * HEAD_DIM), BF16),
            pltpu.VMEM((count * ctx_rows, 2 * HEAD_DIM), BF16),
        ],
        name="attention",
        compiler_params=vmem(16),
    )(where, sink_logit_head, *held(queries, low, pairs, high, ctx_pairs))
    attended = exchanged(attended.reshape(nx, nc * rows, 2 * HEAD_DIM), "x")
    send, keep = pl.pallas_call(
        project_kernel,
        out_shape=[pltpu.VMEM((rows, width), BF16), pltpu.VMEM((rows, width), F32)],
        in_specs=[SMEM] + [VMEM] * 5,
        out_specs=(VMEM, VMEM),
        scratch_shapes=[pltpu.VMEM((nc * rows, nx * 2 * HEAD_DIM), BF16)],
        name="project",
        compiler_params=vmem(14),
    )(where, *held(attended, out_weight, *out_others))
    got = swapped(send)
    return pl.pallas_call(
        final_kernel,
        out_shape=shape_of((rows, width), BF16),
        in_specs=[VMEM] * 4,
        out_specs=VMEM,
        name="final",
        compiler_params=vmem(8),
    )(*held(latent, keep, got, planes))


def solution(mesh):
    torus = Mesh(mesh.devices.reshape(16, 4, 4, 2), ALL)

    return jax.shard_map(
        shards,
        mesh=torus,
        in_specs=(
            P(ALL, None),
            P(SP),
            P(SP),
            P(SP, None),
            P(),
            P(SP, TP),
            P(SP, TP),
            P(SP, TP),
            P(None, TP),
            P(None, TP),
            P(None, TP),
            P(TP),
            P(TP, None),
        ),
        out_specs=P(ALL, None),
        check_vma=False,
    )
```

time: 164 us -> 138 us (0.84)
  the two profiles are of different devices: /device:TPU:25 before, /device:TPU:3 now
where the time goes in v4:
time: 138 us; the launch traced here: 137 us
  starting transfers between devices  59.8 us (43%)
  waiting for transfers between devices  27.1 us (20%)
  blocking collectives  17.6 us (13%)
  Pallas kernels  17.1 us (12%)
  local copies, waits for them, and re-layouts  12.8 us (9%)
  other arithmetic  2.2 us (2%)
    all_to_all x3, starting transfers between devices, exchanged(): return lax.all_to_all(blocks, axis, 0, 0, tiled=True)  32.2 us
    all_to_all x1, blocking collectives, exchanged(): return lax.all_to_all(blocks, axis, 0, 0, tiled=True)  17.6 us
    ppermute x6, starting transfers between devices, from_other_x(): lax.ppermute(block, 'x', [(i, (i + shift) % 4) for i in range(4)])  17.5 us
    ppermute x6, waiting for transfers between devices, from_other_x(): lax.ppermute(block, 'x', [(i, (i + shift) % 4) for i in range(4)])  14.8 us
    unnamed x44, local copies, waits for them, and re-layouts  12.8 us
    all_to_all x3, waiting for transfers between devices, exchanged(): return lax.all_to_all(blocks, axis, 0, 0, tiled=True)  6.83 us
    pallas_call x1, Pallas kernels, shards(): pl.pallas_call(qkv_kernel, out_shape=[pltpu.VMEM(shape, BF16) for shape i...  5.91 us
    ppermute x2, starting transfers between devices, swapped(): return lax.ppermute(x, 'c', [(0, 1), (1, 0)])  5.65 us
  transfers between devices with their start and end apart: 13, of which 5 were waited for; matrix products, arithmetic and copies ran while one was open for 2% of the time, Pallas kernels for 9%

profile of v4, /device:TPU:3, one launch (start us, length us, event | category | flops | bytes accessed | tf_op | source)
XLA Modules:
  0.0 136.9 jit_solution(4200018079832233286)
XLA Ops:
  4.3 14.9 %all-to-all-start = ((f32[16,1,1280]{2,1,0:T(1,128)}), f32[16,1,1280]{2,1,0:T(1,128)S(1)}, u32[]{:S(2)}, u32[]{:S(2)}) async-start(f32[16,1,1280]{2,1,0:T(1,128)} %parts.1), calls=%async_computation | async-start | bytes 163840 | tf_op jit(solution)/shard_map/all_to_all | solution.py:42
  19.2 3.1 %collective-permute-start = (bf16[96,2048]{1,0:T(8,128)(2,1)}, bf16[96,2048]{1,0:T(8,128)(2,1)S(1)}, u32[]{:S(2)}, u32[]{:S(2)}) collective-permute-start(bf16[96,2048]{1,0:T(8,128)(2,1)} %latent_ref.1), channel_id=1, source_target_pairs={{0,2},{2,4},{4,6},{6,0},{1,3},{3,5},{5,7},{7,1},{8,10},{10,12},{12... | collective-permute-start | bytes 1179656 | tf_op jit(solution)/shard_map/ppermute | solution.py:253
  22.3 2.2 %collective-permute-start.1 = (bf16[96,2048]{1,0:T(8,128)(2,1)}, bf16[96,2048]{1,0:T(8,128)(2,1)S(1)}, u32[]{:S(2)}, u32[]{:S(2)}) collective-permute-start(bf16[96,2048]{1,0:T(8,128)(2,1)} %latent_ref.1), channel_id=1, source_target_pairs={{0,6},{2,0},{4,2},{6,4},{1,7},{3,1},{5,3},{7,5},{8,14},{10,8},{12,... | collective-permute-start | bytes 1179656 | tf_op jit(solution)/shard_map/ppermute | solution.py:253
  24.5 3.8 %collective-permute-start.2 = (bf16[96,2048]{1,0:T(8,128)(2,1)}, bf16[96,2048]{1,0:T(8,128)(2,1)S(1)}, u32[]{:S(2)}, u32[]{:S(2)}) collective-permute-start(bf16[96,2048]{1,0:T(8,128)(2,1)} %latent_ref.1), channel_id=1, source_target_pairs={{0,4},{2,6},{4,0},{6,2},{1,5},{3,7},{5,1},{7,3},{8,12},{10,14},{12... | collective-permute-start | bytes 1179656 | tf_op jit(solution)/shard_map/ppermute | solution.py:253
  28.2 2.7 %all-to-all-done.parts_ref = f32[16,1,1280]{2,1,0:T(1,128)S(1)} async-done(((f32[16,1,1280]{2,1,0:T(1,128)}), f32[16,1,1280]{2,1,0:T(1,128)S(1)}, u32[]{:S(2)}, u32[]{:S(2)}) %all-to-all-start) | async-done | bytes 81952 | tf_op jit(solution)/shard_map/all_to_all | solution.py:42
  31.0 17.6 %all_to_all.20.planes_ref = f32[32,1,1280]{2,1,0:T(1,128)S(1)} all-to-all(f32[32,1,1280]{2,1,0:T(1,128)S(1)} %sums.1), channel_id=1, replica_groups=mesh['z'=16,'y'=4,'x'=4,'c'=2] {'y','x','c'}, dimensions={0} | all-to-all | bytes 327680 | tf_op jit(solution)/shard_map/all_to_all | solution.py:42
  53.5 13.2 %all-to-all-start.2 = ((bf16[64,16,256]{2,1,0:T(8,128)(2,1)}), bf16[64,16,256]{2,1,0:T(8,128)(2,1)S(1)}, u32[]{:S(2)}, u32[]{:S(2)}) async-start(bf16[64,16,256]{2,1,0:T(8,128)(2,1)} %context_pairs.1), calls=%async_computation.2 | async-start | bytes 1048576 | tf_op jit(solution)/shard_map/all_to_all | solution.py:42
  67.7 1.6 %pad_maximum_fusion.own_ref = bf16[4,96,2048]{2,1,0:T(8,128)(2,1)S(1)} fusion(bf16[1,96,2048]{2,1,0:T(8,128)(2,1)} %bitcast.21, bf16[1,96,2048]{2,1,0:T(8,128)(2,1)} %bitcast.20, bf16[1,96,2048]{2,1,0:T(8,128)(2,1)} %bitcast.19, bf16[1,96,2048]{2,1,0:T(8,128)(2,1)} %bitcast.14), kind=kLoop, calls=%fused_computation | loop fusion | flops 2359296 | bytes 3145728 | tf_op jit(solution)/shard_map/stack | solution.py:328
  69.3 2.6 %collective-permute-start.3 = (bf16[4,96,2048]{2,1,0:T(8,128)(2,1)S(1)}, bf16[4,96,2048]{2,1,0:T(8,128)(2,1)}, u32[]{:S(2)}, u32[]{:S(2)}) collective-permute-start(bf16[4,96,2048]{2,1,0:T(8,128)(2,1)S(1)} %pad_maximum_fusion.own_ref), channel_id=1, source_target_pairs={{0,1},{1,0},{2,3},{3,2},{4,5},{5,4},{6,7},{7,6},{8,9},{9,8},{10,11... | collective-permute-start | bytes 4718600 | tf_op jit(solution)/shard_map/ppermute | solution.py:258
  71.9 1.9 %collective-permute-start.6 = (bf16[256,2048]{1,0:T(8,128)(2,1)}, bf16[256,2048]{1,0:T(8,128)(2,1)}, u32[]{:S(2)}, u32[]{:S(2)}) collective-permute-start(bf16[256,2048]{1,0:T(8,128)(2,1)} %w0_ref.1), channel_id=1, source_target_pairs={{0,2},{2,4},{4,6},{6,0},{1,3},{3,5},{5,7},{7,1},{8,10},{10,12},{12... | collective-permute-start | bytes 3145736 | tf_op jit(solution)/shard_map/ppermute | solution.py:253
  73.9 3.4 %collective-permute-start.7 = (bf16[256,2048]{1,0:T(8,128)(2,1)}, bf16[256,2048]{1,0:T(8,128)(2,1)}, u32[]{:S(2)}, u32[]{:S(2)}) collective-permute-start(bf16[256,2048]{1,0:T(8,128)(2,1)} %w0_ref.1), channel_id=1, source_target_pairs={{0,6},{2,0},{4,2},{6,4},{1,7},{3,1},{5,3},{7,5},{8,14},{10,8},{12,... | collective-permute-start | bytes 3145736 | tf_op jit(solution)/shard_map/ppermute | solution.py:253
  77.2 3.2 %collective-permute-start.8 = (bf16[256,2048]{1,0:T(8,128)(2,1)}, bf16[256,2048]{1,0:T(8,128)(2,1)}, u32[]{:S(2)}, u32[]{:S(2)}) collective-permute-start(bf16[256,2048]{1,0:T(8,128)(2,1)} %w0_ref.1), channel_id=1, source_target_pairs={{0,4},{2,6},{4,0},{6,2},{1,5},{3,7},{5,1},{7,3},{8,12},{10,14},{12... | collective-permute-start | bytes 3145736 | tf_op jit(solution)/shard_map/ppermute | solution.py:253
  81.1 1.2 copy-done.5
  82.3 5.9 %qkv.1 = (bf16[768,256]{1,0:T(8,128)(2,1)S(1)}, bf16[768,256]{1,0:T(8,128)(2,1)S(1)}, bf16[128,256]{1,0:T(8,128)(2,1)S(1)}, bf16[128,256]{1,0:T(8,128)(2,1)S(1)}) custom-call(s32[4]{0:T(128)S(1)} %pad_add_fusion.place_ref, bf16[4,96,2048]{2,1,0:T(8,128)(2,1)S(1)} %pad_maximum_fusion.own_ref, bf16[4,96,2048]{2,1,0:T(8,128)(2,1)} %collective-permute-done.3.other_ref, ...), custom_call_target="tpu_custom_call" | custom-call | tf_op jit(solution)/shard_map/qkv/pallas_call | solution.py:342
  89.7 3.2 %collective-permute-start.4 = (bf16[128,256]{1,0:T(8,128)(2,1)S(1)}, bf16[128,256]{1,0:T(8,128)(2,1)S(1)}, u32[]{:S(2)}, u32[]{:S(2)}) collective-permute-start(bf16[128,256]{1,0:T(8,128)(2,1)S(1)} %get-tuple-element.12), channel_id=1, source_target_pairs={{0,8},{8,16},{16,24},{24,32},{32,40},{40,48},{48,56},{56,64},{64,7... | collective-permute-start | bytes 196616 | tf_op jit(solution)/shard_map/ppermute | solution.py:358
  92.9 1.3 collective-permute-start.5
  94.2 4.1 %collective-permute-done.5.high_ref = bf16[128,256]{1,0:T(8,128)(2,1)S(1)} collective-permute-done((bf16[128,256]{1,0:T(8,128)(2,1)S(1)}, bf16[128,256]{1,0:T(8,128)(2,1)S(1)}, u32[]{:S(2)}, u32[]{:S(2)}) %collective-permute-start.5) | collective-permute-done | bytes 65568 | tf_op jit(solution)/shard_map/ppermute | solution.py:359
  100.3 5.0 %attention.1 = bf16[768,256]{1,0:T(8,128)(2,1)} custom-call(s32[4]{0:T(128)S(1)} %pad_add_fusion.place_ref, f32[2]{0:T(128)S(1)} %copy-done.18, bf16[768,256]{1,0:T(8,128)(2,1)S(1)} %copy-done.7, bf16[128,256]{1,0:T(8,128)(2,1)S(1)} %collective-permute-done.4.low_ref, bf16[768,256]{1,0:T(8,128)(2,1)S(1)} %copy-done.9, ...), custom_call_target="tpu_custom_call" | custom-call | tf_op jit(solution)/shard_map/attention/pallas_call | solution.py:361
  105.3 4.1 %all-to-all-start.3 = ((bf16[4,192,256]{2,1,0:T(8,128)(2,1)}), bf16[4,192,256]{2,1,0:T(8,128)(2,1)S(1)}, u32[]{:S(2)}, u32[]{:S(2)}) async-start(bf16[4,192,256]{2,1,0:T(8,128)(2,1)} %bitcast.12), calls=%async_computation.3 | async-start | bytes 786432 | tf_op jit(solution)/shard_map/all_to_all | solution.py:42
  109.5 14.8 %collective-permute-done.8.w3_ref = bf16[256,2048]{1,0:T(8,128)(2,1)} collective-permute-done((bf16[256,2048]{1,0:T(8,128)(2,1)}, bf16[256,2048]{1,0:T(8,128)(2,1)}, u32[]{:S(2)}, u32[]{:S(2)}) %collective-permute-start.8) | collective-permute-done | bytes 1048608 | tf_op jit(solution)/shard_map/ppermute | solution.py:253
  124.3 4.1 %all-to-all-done.3.attended_ref = bf16[4,192,256]{2,1,0:T(8,128)(2,1)S(1)} async-done(((bf16[4,192,256]{2,1,0:T(8,128)(2,1)}), bf16[4,192,256]{2,1,0:T(8,128)(2,1)S(1)}, u32[]{:S(2)}, u32[]{:S(2)}) %all-to-all-start.3) | async-done | bytes 393248 | tf_op jit(solution)/shard_map/all_to_all | solution.py:42
  128.4 3.2 %project.1 = (bf16[96,2048]{1,0:T(8,128)(2,1)S(1)}, f32[96,2048]{1,0:T(8,128)S(1)}) custom-call(s32[4]{0:T(128)S(1)} %pad_add_fusion.place_ref, bf16[4,192,256]{2,1,0:T(8,128)(2,1)S(1)} %all-to-all-done.3.attended_ref, bf16[256,2048]{1,0:T(8,128)(2,1)} %w0_ref.1, bf16[256,2048]{1,0:T(8,128)(2,1)} %collective-permute-done.6.w1_ref, ...), custom_call_target="tpu_custom_call" | custom-call | tf_op jit(solution)/shard_map/project/pallas_call | solution.py:375
  131.5 3.1 %collective-permute-start.9 = (bf16[96,2048]{1,0:T(8,128)(2,1)S(1)}, bf16[96,2048]{1,0:T(8,128)(2,1)S(1)}, u32[]{:S(2)}, u32[]{:S(2)}) collective-permute-start(bf16[96,2048]{1,0:T(8,128)(2,1)S(1)} %get-tuple-element.16), channel_id=1, source_target_pairs={{0,1},{1,0},{2,3},{3,2},{4,5},{5,4},{6,7},{7,6},{8,9},{9,8},{10,11... | collective-permute-start | bytes 1179656 | tf_op jit(solution)/shard_map/ppermute | solution.py:258
  134.6 1.3 collective-permute-done.9.got_ref
  (63 shorter events, 15.1 us)
Async XLA Ops:
  4.3 26.7 %all-to-all-start = ((f32[16,1,1280]{2,1,0:T(1,128)}), f32[16,1,1280]{2,1,0:T(1,128)S(1)}, u32[]{:S(2)}, u32[]{:S(2)}) async-start(f32[16,1,1280]{2,1,0:T(1,128)} %parts.1), calls=%async_computation | async-start | bytes 163840 | tf_op jit(solution)/shard_map/all_to_all | solution.py:42
  19.2 47.5 %collective-permute-start = (bf16[96,2048]{1,0:T(8,128)(2,1)}, bf16[96,2048]{1,0:T(8,128)(2,1)S(1)}, u32[]{:S(2)}, u32[]{:S(2)}) collective-permute-start(bf16[96,2048]{1,0:T(8,128)(2,1)} %latent_ref.1), channel_id=1, source_target_pairs={{0,2},{2,4},{4,6},{6,0},{1,3},{3,5},{5,7},{7,1},{8,10},{10,12},{12... | collective-permute-start | bytes 1179656 | tf_op jit(solution)/shard_map/ppermute | solution.py:253
  22.3 44.4 %collective-permute-start.1 = (bf16[96,2048]{1,0:T(8,128)(2,1)}, bf16[96,2048]{1,0:T(8,128)(2,1)S(1)}, u32[]{:S(2)}, u32[]{:S(2)}) collective-permute-start(bf16[96,2048]{1,0:T(8,128)(2,1)} %latent_ref.1), channel_id=1, source_target_pairs={{0,6},{2,0},{4,2},{6,4},{1,7},{3,1},{5,3},{7,5},{8,14},{10,8},{12,... | collective-permute-start | bytes 1179656 | tf_op jit(solution)/shard_map/ppermute | solution.py:253
  24.5 42.2 %collective-permute-start.2 = (bf16[96,2048]{1,0:T(8,128)(2,1)}, bf16[96,2048]{1,0:T(8,128)(2,1)S(1)}, u32[]{:S(2)}, u32[]{:S(2)}) collective-permute-start(bf16[96,2048]{1,0:T(8,128)(2,1)} %latent_ref.1), channel_id=1, source_target_pairs={{0,4},{2,6},{4,0},{6,2},{1,5},{3,7},{5,1},{7,3},{8,12},{10,14},{12... | collective-permute-start | bytes 1179656 | tf_op jit(solution)/shard_map/ppermute | solution.py:253
  48.6 1.0 copy-start
  49.7 1.0 copy-start.2
  53.5 44.9 %all-to-all-start.2 = ((bf16[64,16,256]{2,1,0:T(8,128)(2,1)}), bf16[64,16,256]{2,1,0:T(8,128)(2,1)S(1)}, u32[]{:S(2)}, u32[]{:S(2)}) async-start(bf16[64,16,256]{2,1,0:T(8,128)(2,1)} %context_pairs.1), calls=%async_computation.2 | async-start | bytes 1048576 | tf_op jit(solution)/shard_map/all_to_all | solution.py:42
  66.7 1.0 copy-start.21
  67.7 13.4 %copy-start.1 = (bf16[2048,128]{1,0:T(8,128)(2,1)S(1)}, bf16[2048,128]{1,0:T(8,128)(2,1)}, u32[]{:S(2)}) copy-start(bf16[2048,128]{1,0:T(8,128)(2,1)} %wk_ref.3) | copy-start | bytes 1572868
  67.7 13.4 %copy-start.3 = (bf16[2048,128]{1,0:T(8,128)(2,1)S(1)}, bf16[2048,128]{1,0:T(8,128)(2,1)}, u32[]{:S(2)}) copy-start(bf16[2048,128]{1,0:T(8,128)(2,1)} %wv_ref.3) | copy-start | bytes 1572868
  67.7 13.4 %copy-start.12 = (f32[2048]{0:T(1024)S(1)}, f32[2048]{0:T(1024)}, u32[]{:S(2)}) copy-start(f32[2048]{0:T(1024)} %param.17) | copy-start | bytes 24580
  69.3 11.7 %collective-permute-start.3 = (bf16[4,96,2048]{2,1,0:T(8,128)(2,1)S(1)}, bf16[4,96,2048]{2,1,0:T(8,128)(2,1)}, u32[]{:S(2)}, u32[]{:S(2)}) collective-permute-start(bf16[4,96,2048]{2,1,0:T(8,128)(2,1)S(1)} %pad_maximum_fusion.own_ref), channel_id=1, source_target_pairs={{0,1},{1,0},{2,3},{3,2},{4,5},{5,4},{6,7},{7,6},{8,9},{9,8},{10,11... | collective-permute-start | bytes 4718600 | tf_op jit(solution)/shard_map/ppermute | solution.py:258
  71.9 37.5 %collective-permute-start.6 = (bf16[256,2048]{1,0:T(8,128)(2,1)}, bf16[256,2048]{1,0:T(8,128)(2,1)}, u32[]{:S(2)}, u32[]{:S(2)}) collective-permute-start(bf16[256,2048]{1,0:T(8,128)(2,1)} %w0_ref.1), channel_id=1, source_target_pairs={{0,2},{2,4},{4,6},{6,0},{1,3},{3,5},{5,7},{7,1},{8,10},{10,12},{12... | collective-permute-start | bytes 3145736 | tf_op jit(solution)/shard_map/ppermute | solution.py:253
  73.9 35.6 %collective-permute-start.7 = (bf16[256,2048]{1,0:T(8,128)(2,1)}, bf16[256,2048]{1,0:T(8,128)(2,1)}, u32[]{:S(2)}, u32[]{:S(2)}) collective-permute-start(bf16[256,2048]{1,0:T(8,128)(2,1)} %w0_ref.1), channel_id=1, source_target_pairs={{0,6},{2,0},{4,2},{6,4},{1,7},{3,1},{5,3},{7,5},{8,14},{10,8},{12,... | collective-permute-start | bytes 3145736 | tf_op jit(solution)/shard_map/ppermute | solution.py:253
  77.2 47.0 %collective-permute-start.8 = (bf16[256,2048]{1,0:T(8,128)(2,1)}, bf16[256,2048]{1,0:T(8,128)(2,1)}, u32[]{:S(2)}, u32[]{:S(2)}) collective-permute-start(bf16[256,2048]{1,0:T(8,128)(2,1)} %w0_ref.1), channel_id=1, source_target_pairs={{0,4},{2,6},{4,0},{6,2},{1,5},{3,7},{5,1},{7,3},{8,12},{10,14},{12... | collective-permute-start | bytes 3145736 | tf_op jit(solution)/shard_map/ppermute | solution.py:253
  81.1 1.2 copy-start.5
  82.3 16.0 %copy-start.18 = (f32[2]{0:T(128)S(1)}, f32[2]{0:T(128)}, u32[]{:S(2)}) copy-start(f32[2]{0:T(128)} %sink_ref.1) | copy-start | bytes 28
  89.7 4.5 %collective-permute-start.4 = (bf16[128,256]{1,0:T(8,128)(2,1)S(1)}, bf16[128,256]{1,0:T(8,128)(2,1)S(1)}, u32[]{:S(2)}, u32[]{:S(2)}) collective-permute-start(bf16[128,256]{1,0:T(8,128)(2,1)S(1)} %get-tuple-element.12), channel_id=1, source_target_pairs={{0,8},{8,16},{16,24},{24,32},{32,40},{40,48},{48,56},{56,64},{64,7... | collective-permute-start | bytes 196616 | tf_op jit(solution)/shard_map/ppermute | solution.py:358
  92.9 5.4 %collective-permute-start.5 = (bf16[128,256]{1,0:T(8,128)(2,1)S(1)}, bf16[128,256]{1,0:T(8,128)(2,1)S(1)}, u32[]{:S(2)}, u32[]{:S(2)}) collective-permute-start(bf16[128,256]{1,0:T(8,128)(2,1)S(1)} %get-tuple-element.14), channel_id=1, source_target_pairs={{8,0},{16,8},{24,16},{32,24},{40,32},{48,40},{56,48},{64,56},{72,6... | collective-permute-start | bytes 196616 | tf_op jit(solution)/shard_map/ppermute | solution.py:359
  98.3 1.0 copy-start.7
  99.3 1.0 copy-start.9
  105.3 23.0 %all-to-all-start.3 = ((bf16[4,192,256]{2,1,0:T(8,128)(2,1)}), bf16[4,192,256]{2,1,0:T(8,128)(2,1)S(1)}, u32[]{:S(2)}, u32[]{:S(2)}) async-start(bf16[4,192,256]{2,1,0:T(8,128)(2,1)} %bitcast.12), calls=%async_computation.3 | async-start | bytes 786432 | tf_op jit(solution)/shard_map/all_to_all | solution.py:42
  109.5 26.5 %copy-start.4 = (bf16[96,2048]{1,0:T(8,128)(2,1)S(1)}, bf16[96,2048]{1,0:T(8,128)(2,1)}, u32[]{:S(2)}) copy-start(bf16[96,2048]{1,0:T(8,128)(2,1)} %latent_ref.1) | copy-start | bytes 1179652
  131.5 4.4 %collective-permute-start.9 = (bf16[96,2048]{1,0:T(8,128)(2,1)S(1)}, bf16[96,2048]{1,0:T(8,128)(2,1)S(1)}, u32[]{:S(2)}, u32[]{:S(2)}) collective-permute-start(bf16[96,2048]{1,0:T(8,128)(2,1)S(1)} %get-tuple-element.16), channel_id=1, source_target_pairs={{0,1},{1,0},{2,3},{3,2},{4,5},{5,4},{6,7},{7,6},{8,9},{9,8},{10,11... | collective-permute-start | bytes 1179656 | tf_op jit(solution)/shard_map/ppermute | solution.py:258
  (11 other events, 8.1 us)

commit v5 on v4

--- a/solution.py
+++ b/solution.py
@@ -22,6 +22,7 @@
 
 VMEM = pl.BlockSpec(memory_space=pltpu.VMEM)
 SMEM = pl.BlockSpec(memory_space=pltpu.SMEM)
+HBM = pl.BlockSpec(memory_space=pltpu.HBM)
 F32 = jnp.float32
 BF16 = jnp.bfloat16
 
@@ -30,12 +31,20 @@
     return jax.ShapeDtypeStruct(shape, dtype)
 
 
+def copies(x, axis):
+    return jnp.broadcast_to(x[None], (lax.axis_size(axis), *x.shape))
+
+
 def vmem(mib):
     return pltpu.CompilerParams(vmem_limit_bytes=mib * 2**20)
 
 
 def held(*arrays):
     return [pltpu.with_memory_space_constraint(a, pltpu.VMEM) for a in arrays]
+
+
+def far(*arrays):
+    return [pltpu.with_memory_space_constraint(a, pltpu.HBM) for a in arrays]
 
 
 def exchanged(blocks, axis):
@@ -96,13 +105,18 @@
 
 def qkv_kernel(
     place_ref, own_ref, other_ref, planes_ref, gain_ref, wq_ref, wk_ref, wv_ref, row_ref, col_ref,
-    q_ref, kv_ref, top_ref, bottom_ref, hidden_ref, wkv_ref,
+    q_ref, kv_ref, top_ref, bottom_ref, hidden_ref, wq_held_ref, wkv_ref, sems,
 ):
     columns = wq_ref.shape[1]
+    loads = (
+        pltpu.make_async_copy(wq_ref, wq_held_ref, sems.at[0]),
+        pltpu.make_async_copy(wk_ref, wkv_ref.at[:, :HEAD_DIM], sems.at[1]),
+        pltpu.make_async_copy(wv_ref, wkv_ref.at[:, HEAD_DIM:], sems.at[2]),
+    )
+    for load in loads:
+        load.start()
     shift = row_vector(planes_ref, 0, columns)
     multiplier = gain_ref[...] * (1.0 + row_vector(planes_ref, 2, columns))
-    wkv_ref[:, :HEAD_DIM] = wk_ref[...]
-    wkv_ref[:, HEAD_DIM:] = wv_ref[...]
     _, rows, _ = own_ref.shape
     at_x, core = place_ref[0], place_ref[1]
     for x, shift_x in enumerate(SHIFTS):
@@ -119,6 +133,8 @@
             return carry
 
         lax.fori_loop(0, rows // CHUNK, step, 0, unroll=2)
+    for load in loads:
+        load.wait()
     block = 384
     lane = lax.broadcasted_iota(jnp.int32, (GRID_W, HEAD_DIM), 1) < 64
     col = col_ref[...]
@@ -135,7 +151,7 @@
         sine = jnp.concatenate(
             [jnp.where(lane, row_turned[g : g + 1, :], col) for g in lines], axis=0
         )
-        queries = dot(hidden, wq_ref[...])
+        queries = dot(hidden, wq_held_ref[...])
         for h in range(2):
             part = slice(h * HEAD_DIM, (h + 1) * HEAD_DIM)
             q_ref[cut, part] = (turned(queries[:, part], cosine, sine) * factor).astype(BF16)
@@ -212,9 +228,15 @@
 
 
 def project_kernel(
-    place_ref, attended_ref, w0_ref, w1_ref, w2_ref, w3_ref, send_ref, keep_ref, rows_ref
+    place_ref, attended_ref, w0_ref, w1_ref, w2_ref, w3_ref, send_ref, keep_ref,
+    rows_ref, total_ref, weights_ref, sems,
 ):
-    weights = (w0_ref, w1_ref, w2_ref, w3_ref)
+    loads = [
+        pltpu.make_async_copy(w, weights_ref.at[j], sems.at[j])
+        for j, w in enumerate((w0_ref, w1_ref, w2_ref, w3_ref))
+    ]
+    for load in loads:
+        load.start()
     at_x, core = place_ref[0], place_ref[1]
     rows = send_ref.shape[0]
     deep = attended_ref.shape[2]
@@ -226,13 +248,20 @@
         rows_ref[:rows, cut] = attended_ref[source, pl.ds(theirs, rows), :]
         rows_ref[rows:, cut] = attended_ref[source, pl.ds(mine, rows), :]
     width = 512
-    for n in range(0, send_ref.shape[1], width):
-        cut = slice(n, n + width)
-        total = dot(rows_ref[:, :deep], w0_ref[:, cut])
-        for j in range(1, 4):
-            total = total + dot(rows_ref[:, j * deep : (j + 1) * deep], weights[j][:, cut])
-        send_ref[:, cut] = total[:rows].astype(BF16)
-        keep_ref[:, cut] = total[rows:]
+    for half in range(2):
+        for load in loads[2 * half : 2 * half + 2]:
+            load.wait()
+        for n in range(0, send_ref.shape[1], width):
+            cut = slice(n, n + width)
+            total = 0.0
+            for j in (2 * half, 2 * half + 1):
+                total = total + dot(rows_ref[:, j * deep : (j + 1) * deep], weights_ref[j, :, cut])
+            if half == 0:
+                total_ref[:, cut] = total
+            else:
+                total = total + total_ref[:, cut]
+                send_ref[:, cut] = total[:rows].astype(BF16)
+                keep_ref[:, cut] = total[rows:]
 
 
 def final_kernel(latent_ref, keep_ref, got_ref, planes_ref, out_ref):
@@ -296,11 +325,8 @@
         name="parts",
         compiler_params=vmem(6),
     )(
-        condition.reshape(1, -1),
-        context_condition.reshape(1, -1),
-        shift_weight,
-        scale_weight,
-        gate_weight,
+        *far(condition.reshape(1, -1), context_condition.reshape(1, -1)),
+        *far(shift_weight, scale_weight, gate_weight),
     )
     parts = exchanged(parts, "z")
     latent_others = from_other_x(latent)
@@ -330,30 +356,34 @@
     ctx_rows = context.shape[0]
     pairs = pl.pallas_call(
         context_kernel,
-        out_shape=shape_of((count, ctx_rows, 2 * HEAD_DIM), BF16),
+        out_shape=shape_of((nz, ctx_rows, 2 * HEAD_DIM), BF16),
         in_specs=[VMEM] * 5,
         out_specs=VMEM,
         name="context_pairs",
         compiler_params=vmem(8),
-    )(*held(context, planes, gain, key_matrix, value_matrix))
-    ctx_pairs = exchanged(pairs, SP).reshape(-1, 2 * HEAD_DIM)
+    )(*far(context), *held(planes), *far(gain, key_matrix, value_matrix))
+    ctx_z = exchanged(pairs, "z").reshape(nz * ctx_rows, 2 * HEAD_DIM)
+    ctx_pairs = exchanged(copies(ctx_z, "y"), "y").reshape(-1, 2 * HEAD_DIM)
     wide = (group_rows, 2 * HEAD_DIM)
     edge = (WINDOW_REACH, 2 * HEAD_DIM)
     queries, pairs, top, bottom = pl.pallas_call(
         qkv_kernel,
-        out_shape=[pltpu.VMEM(shape, BF16) for shape in (wide, wide, edge, edge)],
-        in_specs=[SMEM] + [VMEM] * 9,
+        out_shape=[shape_of(wide, BF16)] * 2 + [pltpu.VMEM(edge, BF16)] * 2,
+        in_specs=[SMEM] + [VMEM] * 4 + [HBM] * 3 + [VMEM] * 2,
         out_specs=[VMEM] * 4,
         scratch_shapes=[
             pltpu.VMEM((group_rows, width), BF16),
             pltpu.VMEM((width, 2 * HEAD_DIM), BF16),
+            pltpu.VMEM((width, 2 * HEAD_DIM), BF16),
+            pltpu.SemaphoreType.DMA((3,)),
         ],
         name="qkv",
         compiler_params=vmem(20),
     )(
         where,
         *held(latent_x, latent_c, planes, gain),
-        *held(query_weight, key_matrix, value_matrix, lines, cols),
+        *far(query_weight, key_matrix, value_matrix),
+        *held(lines, cols),
     )
     low = lax.ppermute(bottom, SP, [(i, i + 1) for i in range(count - 1)])
     high = lax.ppermute(top, SP, [(i + 1, i) for i in range(count - 1)])
@@ -375,12 +405,17 @@
     send, keep = pl.pallas_call(
         project_kernel,
         out_shape=[pltpu.VMEM((rows, width), BF16), pltpu.VMEM((rows, width), F32)],
-        in_specs=[SMEM] + [VMEM] * 5,
+        in_specs=[SMEM, VMEM] + [HBM] * 4,
         out_specs=(VMEM, VMEM),
-        scratch_shapes=[pltpu.VMEM((nc * rows, nx * 2 * HEAD_DIM), BF16)],
+        scratch_shapes=[
+            pltpu.VMEM((nc * rows, nx * 2 * HEAD_DIM), BF16),
+            pltpu.VMEM((nc * rows, width), F32),
+            pltpu.VMEM((nx, 2 * HEAD_DIM, width), BF16),
+            pltpu.SemaphoreType.DMA((4,)),
+        ],
         name="project",
         compiler_params=vmem(14),
-    )(where, *held(attended, out_weight, *out_others))
+    )(where, *held(attended), *far(out_weight, *out_others))
     got = swapped(send)
     return pl.pallas_call(
         final_kernel,
@@ -389,7 +424,7 @@
         out_specs=VMEM,
         name="final",
         compiler_params=vmem(8),
-    )(*held(latent, keep, got, planes))
+    )(*far(latent), *held(keep, got, planes))
 
 
 def solution(mesh):

time: 138 us -> 145 us (1.051)
  the two profiles are of different devices: /device:TPU:3 before, /device:TPU:25 now
where the time goes in v5:
time: 145 us; the launch traced here: 144 us
  starting transfers between devices  57.8 us (40%)
  waiting for transfers between devices  36.7 us (25%)
  blocking collectives  26.6 us (18%)
  Pallas kernels  19.9 us (14%)
  other arithmetic  1.75 us (1%)
    all_to_all x1, blocking collectives, exchanged(): return lax.all_to_all(blocks, axis, 0, 0, tiled=True)  26.6 us
    all_to_all x4, starting transfers between devices, exchanged(): return lax.all_to_all(blocks, axis, 0, 0, tiled=True)  20.9 us
    ppermute x6, starting transfers between devices, from_other_x(): lax.ppermute(block, 'x', [(i, (i + shift) % 4) for i in range(4)])  19.8 us
    all_to_all x4, waiting for transfers between devices, exchanged(): return lax.all_to_all(blocks, axis, 0, 0, tiled=True)  17.7 us
    ppermute x6, waiting for transfers between devices, from_other_x(): lax.ppermute(block, 'x', [(i, (i + shift) % 4) for i in range(4)])  12.8 us
    ppermute x2, starting transfers between devices, swapped(): return lax.ppermute(x, 'c', [(0, 1), (1, 0)])  11.8 us
    pallas_call x1, Pallas kernels, shards(): pl.pallas_call(qkv_kernel, out_shape=[shape_of(wide, BF16)] * 2 + [pltpu....  5.72 us
    pallas_call x1, Pallas kernels, shards(): pl.pallas_call(attention_kernel, out_shape=shape_of(wide, BF16), in_specs...  5.02 us
  transfers between devices with their start and end apart: 14, of which 8 were waited for; matrix products, arithmetic and copies ran while one was open for 1% of the time, Pallas kernels for 10%

profile of v5, /device:TPU:25, one launch (start us, length us, event | category | flops | bytes accessed | tf_op | source)
XLA Modules:
  0.0 143.9 jit_solution(9677832425905393746)
XLA Ops:
  0.0 3.1 %collective-permute-start = (bf16[96,2048]{1,0:T(8,128)(2,1)}, bf16[96,2048]{1,0:T(8,128)(2,1)S(1)}, u32[]{:S(2)}, u32[]{:S(2)}) collective-permute-start(bf16[96,2048]{1,0:T(8,128)(2,1)} %latent_ref.1), channel_id=1, source_target_pairs={{0,2},{2,4},{4,6},{6,0},{1,3},{3,5},{5,7},{7,1},{8,10},{10,12},{12... | collective-permute-start | bytes 1179656 | tf_op jit(solution)/shard_map/ppermute | solution.py:282
  3.1 3.4 %collective-permute-start.1 = (bf16[96,2048]{1,0:T(8,128)(2,1)}, bf16[96,2048]{1,0:T(8,128)(2,1)S(1)}, u32[]{:S(2)}, u32[]{:S(2)}) collective-permute-start(bf16[96,2048]{1,0:T(8,128)(2,1)} %latent_ref.1), channel_id=1, source_target_pairs={{0,6},{2,0},{4,2},{6,4},{1,7},{3,1},{5,3},{7,5},{8,14},{10,8},{12,... | collective-permute-start | bytes 1179656 | tf_op jit(solution)/shard_map/ppermute | solution.py:282
  6.5 3.4 %collective-permute-start.2 = (bf16[96,2048]{1,0:T(8,128)(2,1)}, bf16[96,2048]{1,0:T(8,128)(2,1)S(1)}, u32[]{:S(2)}, u32[]{:S(2)}) collective-permute-start(bf16[96,2048]{1,0:T(8,128)(2,1)} %latent_ref.1), channel_id=1, source_target_pairs={{0,4},{2,6},{4,0},{6,2},{1,5},{3,7},{5,1},{7,3},{8,12},{10,14},{12... | collective-permute-start | bytes 1179656 | tf_op jit(solution)/shard_map/ppermute | solution.py:282
  10.0 3.4 %collective-permute-done = bf16[96,2048]{1,0:T(8,128)(2,1)S(1)} collective-permute-done((bf16[96,2048]{1,0:T(8,128)(2,1)}, bf16[96,2048]{1,0:T(8,128)(2,1)S(1)}, u32[]{:S(2)}, u32[]{:S(2)}) %collective-permute-start) | collective-permute-done | bytes 393248 | tf_op jit(solution)/shard_map/ppermute | solution.py:282
  14.9 7.8 %collective-permute-done.2 = bf16[96,2048]{1,0:T(8,128)(2,1)S(1)} collective-permute-done((bf16[96,2048]{1,0:T(8,128)(2,1)}, bf16[96,2048]{1,0:T(8,128)(2,1)S(1)}, u32[]{:S(2)}, u32[]{:S(2)}) %collective-permute-start.2) | collective-permute-done | bytes 393248 | tf_op jit(solution)/shard_map/ppermute | solution.py:282
  23.9 3.8 %collective-permute-start.3 = (bf16[4,96,2048]{2,1,0:T(8,128)(2,1)S(1)}, bf16[4,96,2048]{2,1,0:T(8,128)(2,1)}, u32[]{:S(2)}, u32[]{:S(2)}) collective-permute-start(bf16[4,96,2048]{2,1,0:T(8,128)(2,1)S(1)} %pad_maximum_fusion.own_ref), channel_id=1, source_target_pairs={{0,1},{1,0},{2,3},{3,2},{4,5},{5,4},{6,7},{7,6},{8,9},{9,8},{10,11... | collective-permute-start | bytes 4718600 | tf_op jit(solution)/shard_map/ppermute | solution.py:287
  28.6 26.6 %all_to_all.25.parts_ref = f32[16,1,1280]{2,1,0:T(1,128)S(1)} all-to-all(f32[16,1,1280]{2,1,0:T(1,128)S(1)} %parts.1), channel_id=1, replica_groups=mesh['z'=16,'y'=4,'x'=4,'c'=2] {'z'}, dimensions={0} | all-to-all | bytes 163840 | tf_op jit(solution)/shard_map/all_to_all | solution.py:51
  56.0 9.6 %all-to-all-start.1 = ((f32[32,1,1280]{2,1,0:T(1,128)}), f32[32,1,1280]{2,1,0:T(1,128)S(1)}, u32[]{:S(2)}, u32[]{:S(2)}) async-start(f32[32,1,1280]{2,1,0:T(1,128)} %sums.1), calls=%async_computation.1 | async-start | bytes 327680 | tf_op jit(solution)/shard_map/all_to_all | solution.py:51
  65.6 3.1 %collective-permute-start.6 = (bf16[256,2048]{1,0:T(8,128)(2,1)}, bf16[256,2048]{1,0:T(8,128)(2,1)}, u32[]{:S(2)}, u32[]{:S(2)}) collective-permute-start(bf16[256,2048]{1,0:T(8,128)(2,1)} %w0_ref.1), channel_id=1, source_target_pairs={{0,2},{2,4},{4,6},{6,0},{1,3},{3,5},{5,7},{7,1},{8,10},{10,12},{12... | collective-permute-start | bytes 3145736 | tf_op jit(solution)/shard_map/ppermute | solution.py:282
  68.7 3.4 %collective-permute-start.7 = (bf16[256,2048]{1,0:T(8,128)(2,1)}, bf16[256,2048]{1,0:T(8,128)(2,1)}, u32[]{:S(2)}, u32[]{:S(2)}) collective-permute-start(bf16[256,2048]{1,0:T(8,128)(2,1)} %w0_ref.1), channel_id=1, source_target_pairs={{0,6},{2,0},{4,2},{6,4},{1,7},{3,1},{5,3},{7,5},{8,14},{10,8},{12,... | collective-permute-start | bytes 3145736 | tf_op jit(solution)/shard_map/ppermute | solution.py:282
  72.1 3.4 %collective-permute-start.8 = (bf16[256,2048]{1,0:T(8,128)(2,1)}, bf16[256,2048]{1,0:T(8,128)(2,1)}, u32[]{:S(2)}, u32[]{:S(2)}) collective-permute-start(bf16[256,2048]{1,0:T(8,128)(2,1)} %w0_ref.1), channel_id=1, source_target_pairs={{0,4},{2,6},{4,0},{6,2},{1,5},{3,7},{5,1},{7,3},{8,12},{10,14},{12... | collective-permute-start | bytes 3145736 | tf_op jit(solution)/shard_map/ppermute | solution.py:282
  75.5 2.3 %context_pairs.1 = bf16[16,16,256]{2,1,0:T(8,128)(2,1)} custom-call(bf16[16,2048]{1,0:T(8,128)(2,1)} %ctx_ref.1, f32[32,1,1280]{2,1,0:T(1,128)S(1)} %all-to-all-done.1.planes_ref, f32[1,2048]{1,0:T(1,128)} %bitcast.15, bf16[2048,128]{1,0:T(8,128)(2,1)} %wk_ref.3, bf16[2048,128]{1,0:T(8,128)(2,1)} %wv_ref.3), custom_call_target="tpu_custom_call" | custom-call | tf_op jit(solution)/shard_map/context_pairs/pallas_call | solution.py:357
  77.8 3.6 %all-to-all-start.2 = ((bf16[16,16,256]{2,1,0:T(8,128)(2,1)}), bf16[16,16,256]{2,1,0:T(8,128)(2,1)S(1)}, u32[]{:S(2)}, u32[]{:S(2)}) async-start(bf16[16,16,256]{2,1,0:T(8,128)(2,1)} %context_pairs.1), calls=%async_computation.2 | async-start | bytes 262144 | tf_op jit(solution)/shard_map/all_to_all | solution.py:51
  81.8 11.5 %all-to-all-done.2 = bf16[16,16,256]{2,1,0:T(8,128)(2,1)S(1)} async-done(((bf16[16,16,256]{2,1,0:T(8,128)(2,1)}), bf16[16,16,256]{2,1,0:T(8,128)(2,1)S(1)}, u32[]{:S(2)}, u32[]{:S(2)}) %all-to-all-start.2) | async-done | bytes 131104 | tf_op jit(solution)/shard_map/all_to_all | solution.py:51
  94.1 4.2 %all-to-all-start.3 = ((bf16[4,256,256]{2,1,0:T(8,128)(2,1)}), bf16[4,256,256]{2,1,0:T(8,128)(2,1)S(1)}, u32[]{:S(2)}, u32[]{:S(2)}) async-start(bf16[4,256,256]{2,1,0:T(8,128)(2,1)} %broadcast_in_dim.10), calls=%async_computation.3 | async-start | bytes 1048576 | tf_op jit(solution)/shard_map/all_to_all | solution.py:51
  98.6 5.7 %qkv.1 = (bf16[768,256]{1,0:T(8,128)(2,1)S(1)}, bf16[768,256]{1,0:T(8,128)(2,1)S(1)}, bf16[128,256]{1,0:T(8,128)(2,1)S(1)}, bf16[128,256]{1,0:T(8,128)(2,1)S(1)}) custom-call(s32[4]{0:T(128)S(1)} %pad_add_fusion.place_ref, bf16[4,96,2048]{2,1,0:T(8,128)(2,1)S(1)} %pad_maximum_fusion.own_ref, bf16[4,96,2048]{2,1,0:T(8,128)(2,1)} %collective-permute-done.3.other_ref, ...), custom_call_target="tpu_custom_call" | custom-call | tf_op jit(solution)/shard_map/qkv/pallas_call | solution.py:369
  104.3 2.7 %collective-permute-start.4 = (bf16[128,256]{1,0:T(8,128)(2,1)S(1)}, bf16[128,256]{1,0:T(8,128)(2,1)S(1)}, u32[]{:S(2)}, u32[]{:S(2)}) collective-permute-start(bf16[128,256]{1,0:T(8,128)(2,1)S(1)} %get-tuple-element.12), channel_id=1, source_target_pairs={{0,8},{8,16},{16,24},{24,32},{32,40},{40,48},{48,56},{56,64},{64,7... | collective-permute-start | bytes 196616 | tf_op jit(solution)/shard_map/ppermute | solution.py:388
  107.1 2.6 %collective-permute-start.5 = (bf16[128,256]{1,0:T(8,128)(2,1)S(1)}, bf16[128,256]{1,0:T(8,128)(2,1)S(1)}, u32[]{:S(2)}, u32[]{:S(2)}) collective-permute-start(bf16[128,256]{1,0:T(8,128)(2,1)S(1)} %get-tuple-element.14), channel_id=1, source_target_pairs={{8,0},{16,8},{24,16},{32,24},{40,32},{48,40},{56,48},{64,56},{72,6... | collective-permute-start | bytes 196616 | tf_op jit(solution)/shard_map/ppermute | solution.py:389
  109.8 4.8 %collective-permute-done.5.high_ref = bf16[128,256]{1,0:T(8,128)(2,1)S(1)} collective-permute-done((bf16[128,256]{1,0:T(8,128)(2,1)S(1)}, bf16[128,256]{1,0:T(8,128)(2,1)S(1)}, u32[]{:S(2)}, u32[]{:S(2)}) %collective-permute-start.5) | collective-permute-done | bytes 65568 | tf_op jit(solution)/shard_map/ppermute | solution.py:389
  114.6 5.0 %attention.1 = bf16[768,256]{1,0:T(8,128)(2,1)} custom-call(s32[4]{0:T(128)S(1)} %pad_add_fusion.place_ref, f32[2]{0:T(128)S(1)} %copy-done.1, bf16[768,256]{1,0:T(8,128)(2,1)S(1)} %get-tuple-element.11.q_ref, bf16[128,256]{1,0:T(8,128)(2,1)S(1)} %collective-permute-done.4.low_ref, bf16[768,256]{1,0:T(8,128)(2,1)S(1)} %get-tuple-element.13.kv_ref, ...), custom_call_target="tpu_custom_call" | custom-call | tf_op jit(solution)/shard_map/attention/pallas_call | solution.py:391
  119.6 3.5 %all-to-all-start.4 = ((bf16[4,192,256]{2,1,0:T(8,128)(2,1)}), bf16[4,192,256]{2,1,0:T(8,128)(2,1)S(1)}, u32[]{:S(2)}, u32[]{:S(2)}) async-start(bf16[4,192,256]{2,1,0:T(8,128)(2,1)} %bitcast.13), calls=%async_computation.4 | async-start | bytes 786432 | tf_op jit(solution)/shard_map/all_to_all | solution.py:51
  123.1 6.2 %all-to-all-done.4.attended_ref = bf16[4,192,256]{2,1,0:T(8,128)(2,1)S(1)} async-done(((bf16[4,192,256]{2,1,0:T(8,128)(2,1)}), bf16[4,192,256]{2,1,0:T(8,128)(2,1)S(1)}, u32[]{:S(2)}, u32[]{:S(2)}) %all-to-all-start.4) | async-done | bytes 393248 | tf_op jit(solution)/shard_map/all_to_all | solution.py:51
  129.3 3.3 %project.1 = (bf16[96,2048]{1,0:T(8,128)(2,1)S(1)}, f32[96,2048]{1,0:T(8,128)S(1)}) custom-call(s32[4]{0:T(128)S(1)} %pad_add_fusion.place_ref, bf16[4,192,256]{2,1,0:T(8,128)(2,1)S(1)} %all-to-all-done.4.attended_ref, bf16[256,2048]{1,0:T(8,128)(2,1)} %w0_ref.1, bf16[256,2048]{1,0:T(8,128)(2,1)} %collective-permute-done.6.w1_ref, ...), custom_call_target="tpu_custom_call" | custom-call | tf_op jit(solution)/shard_map/project/pallas_call | solution.py:405
  132.6 8.0 %collective-permute-start.9 = (bf16[96,2048]{1,0:T(8,128)(2,1)S(1)}, bf16[96,2048]{1,0:T(8,128)(2,1)S(1)}, u32[]{:S(2)}, u32[]{:S(2)}) collective-permute-start(bf16[96,2048]{1,0:T(8,128)(2,1)S(1)} %get-tuple-element.16), channel_id=1, source_target_pairs={{0,1},{1,0},{2,3},{3,2},{4,5},{5,4},{6,7},{7,6},{8,9},{9,8},{10,11... | collective-permute-start | bytes 1179656 | tf_op jit(solution)/shard_map/ppermute | solution.py:287
  (26 shorter events, 9.2 us)
Async XLA Ops:
  0.0 13.3 %collective-permute-start = (bf16[96,2048]{1,0:T(8,128)(2,1)}, bf16[96,2048]{1,0:T(8,128)(2,1)S(1)}, u32[]{:S(2)}, u32[]{:S(2)}) collective-permute-start(bf16[96,2048]{1,0:T(8,128)(2,1)} %latent_ref.1), channel_id=1, source_target_pairs={{0,2},{2,4},{4,6},{6,0},{1,3},{3,5},{5,7},{7,1},{8,10},{10,12},{12... | collective-permute-start | bytes 1179656 | tf_op jit(solution)/shard_map/ppermute | solution.py:282
  3.1 11.8 %collective-permute-start.1 = (bf16[96,2048]{1,0:T(8,128)(2,1)}, bf16[96,2048]{1,0:T(8,128)(2,1)S(1)}, u32[]{:S(2)}, u32[]{:S(2)}) collective-permute-start(bf16[96,2048]{1,0:T(8,128)(2,1)} %latent_ref.1), channel_id=1, source_target_pairs={{0,6},{2,0},{4,2},{6,4},{1,7},{3,1},{5,3},{7,5},{8,14},{10,8},{12,... | collective-permute-start | bytes 1179656 | tf_op jit(solution)/shard_map/ppermute | solution.py:282
  6.5 16.2 %collective-permute-start.2 = (bf16[96,2048]{1,0:T(8,128)(2,1)}, bf16[96,2048]{1,0:T(8,128)(2,1)S(1)}, u32[]{:S(2)}, u32[]{:S(2)}) collective-permute-start(bf16[96,2048]{1,0:T(8,128)(2,1)} %latent_ref.1), channel_id=1, source_target_pairs={{0,4},{2,6},{4,0},{6,2},{1,5},{3,7},{5,1},{7,3},{8,12},{10,14},{12... | collective-permute-start | bytes 1179656 | tf_op jit(solution)/shard_map/ppermute | solution.py:282
  23.9 74.7 %collective-permute-start.3 = (bf16[4,96,2048]{2,1,0:T(8,128)(2,1)S(1)}, bf16[4,96,2048]{2,1,0:T(8,128)(2,1)}, u32[]{:S(2)}, u32[]{:S(2)}) collective-permute-start(bf16[4,96,2048]{2,1,0:T(8,128)(2,1)S(1)} %pad_maximum_fusion.own_ref), channel_id=1, source_target_pairs={{0,1},{1,0},{2,3},{3,2},{4,5},{5,4},{6,7},{7,6},{8,9},{9,8},{10,11... | collective-permute-start | bytes 4718600 | tf_op jit(solution)/shard_map/ppermute | solution.py:287
  56.0 19.5 %all-to-all-start.1 = ((f32[32,1,1280]{2,1,0:T(1,128)}), f32[32,1,1280]{2,1,0:T(1,128)S(1)}, u32[]{:S(2)}, u32[]{:S(2)}) async-start(f32[32,1,1280]{2,1,0:T(1,128)} %sums.1), calls=%async_computation.1 | async-start | bytes 327680 | tf_op jit(solution)/shard_map/all_to_all | solution.py:51
  65.6 57.5 %collective-permute-start.6 = (bf16[256,2048]{1,0:T(8,128)(2,1)}, bf16[256,2048]{1,0:T(8,128)(2,1)}, u32[]{:S(2)}, u32[]{:S(2)}) collective-permute-start(bf16[256,2048]{1,0:T(8,128)(2,1)} %w0_ref.1), channel_id=1, source_target_pairs={{0,2},{2,4},{4,6},{6,0},{1,3},{3,5},{5,7},{7,1},{8,10},{10,12},{12... | collective-permute-start | bytes 3145736 | tf_op jit(solution)/shard_map/ppermute | solution.py:282
  68.7 54.4 %collective-permute-start.7 = (bf16[256,2048]{1,0:T(8,128)(2,1)}, bf16[256,2048]{1,0:T(8,128)(2,1)}, u32[]{:S(2)}, u32[]{:S(2)}) collective-permute-start(bf16[256,2048]{1,0:T(8,128)(2,1)} %w0_ref.1), channel_id=1, source_target_pairs={{0,6},{2,0},{4,2},{6,4},{1,7},{3,1},{5,3},{7,5},{8,14},{10,8},{12,... | collective-permute-start | bytes 3145736 | tf_op jit(solution)/shard_map/ppermute | solution.py:282
  72.1 51.0 %collective-permute-start.8 = (bf16[256,2048]{1,0:T(8,128)(2,1)}, bf16[256,2048]{1,0:T(8,128)(2,1)}, u32[]{:S(2)}, u32[]{:S(2)}) collective-permute-start(bf16[256,2048]{1,0:T(8,128)(2,1)} %w0_ref.1), channel_id=1, source_target_pairs={{0,4},{2,6},{4,0},{6,2},{1,5},{3,7},{5,1},{7,3},{8,12},{10,14},{12... | collective-permute-start | bytes 3145736 | tf_op jit(solution)/shard_map/ppermute | solution.py:282
  77.8 20.8 %copy-start = (f32[2048]{0:T(1024)S(1)}, f32[2048]{0:T(1024)}, u32[]{:S(2)}) copy-start(f32[2048]{0:T(1024)} %param.17) | copy-start | bytes 24580
  77.8 15.5 %all-to-all-start.2 = ((bf16[16,16,256]{2,1,0:T(8,128)(2,1)}), bf16[16,16,256]{2,1,0:T(8,128)(2,1)S(1)}, u32[]{:S(2)}, u32[]{:S(2)}) async-start(bf16[16,16,256]{2,1,0:T(8,128)(2,1)} %context_pairs.1), calls=%async_computation.2 | async-start | bytes 262144 | tf_op jit(solution)/shard_map/all_to_all | solution.py:51
  94.1 15.5 %all-to-all-start.3 = ((bf16[4,256,256]{2,1,0:T(8,128)(2,1)}), bf16[4,256,256]{2,1,0:T(8,128)(2,1)S(1)}, u32[]{:S(2)}, u32[]{:S(2)}) async-start(bf16[4,256,256]{2,1,0:T(8,128)(2,1)} %broadcast_in_dim.10), calls=%async_computation.3 | async-start | bytes 1048576 | tf_op jit(solution)/shard_map/all_to_all | solution.py:51
  98.6 16.0 %copy-start.1 = (f32[2]{0:T(128)S(1)}, f32[2]{0:T(128)}, u32[]{:S(2)}) copy-start(f32[2]{0:T(128)} %sink_ref.1) | copy-start | bytes 28
  104.3 5.4 %collective-permute-start.4 = (bf16[128,256]{1,0:T(8,128)(2,1)S(1)}, bf16[128,256]{1,0:T(8,128)(2,1)S(1)}, u32[]{:S(2)}, u32[]{:S(2)}) collective-permute-start(bf16[128,256]{1,0:T(8,128)(2,1)S(1)} %get-tuple-element.12), channel_id=1, source_target_pairs={{0,8},{8,16},{16,24},{24,32},{32,40},{40,48},{48,56},{56,64},{64,7... | collective-permute-start | bytes 196616 | tf_op jit(solution)/shard_map/ppermute | solution.py:388
  107.1 7.5 %collective-permute-start.5 = (bf16[128,256]{1,0:T(8,128)(2,1)S(1)}, bf16[128,256]{1,0:T(8,128)(2,1)S(1)}, u32[]{:S(2)}, u32[]{:S(2)}) collective-permute-start(bf16[128,256]{1,0:T(8,128)(2,1)S(1)} %get-tuple-element.14), channel_id=1, source_target_pairs={{8,0},{16,8},{24,16},{32,24},{40,32},{48,40},{56,48},{64,56},{72,6... | collective-permute-start | bytes 196616 | tf_op jit(solution)/shard_map/ppermute | solution.py:389
  119.6 9.7 %all-to-all-start.4 = ((bf16[4,192,256]{2,1,0:T(8,128)(2,1)}), bf16[4,192,256]{2,1,0:T(8,128)(2,1)S(1)}, u32[]{:S(2)}, u32[]{:S(2)}) async-start(bf16[4,192,256]{2,1,0:T(8,128)(2,1)} %bitcast.13), calls=%async_computation.4 | async-start | bytes 786432 | tf_op jit(solution)/shard_map/all_to_all | solution.py:51
  132.6 9.3 %collective-permute-start.9 = (bf16[96,2048]{1,0:T(8,128)(2,1)S(1)}, bf16[96,2048]{1,0:T(8,128)(2,1)S(1)}, u32[]{:S(2)}, u32[]{:S(2)}) collective-permute-start(bf16[96,2048]{1,0:T(8,128)(2,1)S(1)} %get-tuple-element.16), channel_id=1, source_target_pairs={{0,1},{1,0},{2,3},{3,2},{4,5},{5,4},{6,7},{7,6},{8,9},{9,8},{10,11... | collective-permute-start | bytes 1179656 | tf_op jit(solution)/shard_map/ppermute | solution.py:287

commit v6 on v5

--- a/solution.py
+++ b/solution.py
@@ -29,10 +29,6 @@
 
 def shape_of(shape, dtype):
     return jax.ShapeDtypeStruct(shape, dtype)
-
-
-def copies(x, axis):
-    return jnp.broadcast_to(x[None], (lax.axis_size(axis), *x.shape))
 
 
 def vmem(mib):
@@ -175,6 +171,17 @@
         out_ref[p] = pairs
 
 
+def spread_kernel(block_ref, out_ref, sems):
+    sends = [
+        pltpu.make_async_copy(block_ref, out_ref.at[y], sems.at[y])
+        for y in range(out_ref.shape[0])
+    ]
+    for send in sends:
+        send.start()
+    for send in sends:
+        send.wait()
+
+
 def attention_kernel(
     place_ref, sink_ref, q_ref, low_ref, kv_ref, high_ref, ctx_ref, attended_ref,
     keys_ref, values_ref, ctx_values_ref,
@@ -229,14 +236,20 @@
 
 def project_kernel(
     place_ref, attended_ref, w0_ref, w1_ref, w2_ref, w3_ref, send_ref, keep_ref,
-    rows_ref, total_ref, weights_ref, sems,
+    rows_ref, weights_ref, sems,
 ):
+    width = 512
+    cuts = [slice(n, n + width) for n in range(0, send_ref.shape[1], width)]
     loads = [
-        pltpu.make_async_copy(w, weights_ref.at[j], sems.at[j])
-        for j, w in enumerate((w0_ref, w1_ref, w2_ref, w3_ref))
+        [
+            pltpu.make_async_copy(w.at[:, cut], weights_ref.at[j, :, cut], sems.at[n, j])
+            for j, w in enumerate((w0_ref, w1_ref, w2_ref, w3_ref))
+        ]
+        for n, cut in enumerate(cuts)
     ]
-    for load in loads:
-        load.start()
+    for group in loads:
+        for load in group:
+            load.start()
     at_x, core = place_ref[0], place_ref[1]
     rows = send_ref.shape[0]
     deep = attended_ref.shape[2]
@@ -247,21 +260,14 @@
         cut = slice(j * deep, (j + 1) * deep)
         rows_ref[:rows, cut] = attended_ref[source, pl.ds(theirs, rows), :]
         rows_ref[rows:, cut] = attended_ref[source, pl.ds(mine, rows), :]
-    width = 512
-    for half in range(2):
-        for load in loads[2 * half : 2 * half + 2]:
+    for group, cut in zip(loads, cuts):
+        for load in group:
             load.wait()
-        for n in range(0, send_ref.shape[1], width):
-            cut = slice(n, n + width)
-            total = 0.0
-            for j in (2 * half, 2 * half + 1):
-                total = total + dot(rows_ref[:, j * deep : (j + 1) * deep], weights_ref[j, :, cut])
-            if half == 0:
-                total_ref[:, cut] = total
-            else:
-                total = total + total_ref[:, cut]
-                send_ref[:, cut] = total[:rows].astype(BF16)
-                keep_ref[:, cut] = total[rows:]
+        total = dot(rows_ref[:, :deep], weights_ref[0, :, cut])
+        for j in range(1, 4):
+            total = total + dot(rows_ref[:, j * deep : (j + 1) * deep], weights_ref[j, :, cut])
+        send_ref[:, cut] = total[:rows].astype(BF16)
+        keep_ref[:, cut] = total[rows:]
 
 
 def final_kernel(latent_ref, keep_ref, got_ref, planes_ref, out_ref):
@@ -361,14 +367,23 @@
         out_specs=VMEM,
         name="context_pairs",
         compiler_params=vmem(8),
-    )(*far(context), *held(planes), *far(gain, key_matrix, value_matrix))
+    )(*held(context, planes, gain, key_matrix, value_matrix))
     ctx_z = exchanged(pairs, "z").reshape(nz * ctx_rows, 2 * HEAD_DIM)
-    ctx_pairs = exchanged(copies(ctx_z, "y"), "y").reshape(-1, 2 * HEAD_DIM)
+    spread = pl.pallas_call(
+        spread_kernel,
+        out_shape=pltpu.HBM((ny, *ctx_z.shape), BF16),
+        in_specs=[VMEM],
+        out_specs=HBM,
+        scratch_shapes=[pltpu.SemaphoreType.DMA((ny,))],
+        name="spread",
+        compiler_params=vmem(4),
+    )(*held(ctx_z))
+    ctx_pairs = exchanged(spread, "y").reshape(-1, 2 * HEAD_DIM)
     wide = (group_rows, 2 * HEAD_DIM)
     edge = (WINDOW_REACH, 2 * HEAD_DIM)
     queries, pairs, top, bottom = pl.pallas_call(
         qkv_kernel,
-        out_shape=[shape_of(wide, BF16)] * 2 + [pltpu.VMEM(edge, BF16)] * 2,
+        out_shape=[pltpu.HBM(wide, BF16)] * 2 + [pltpu.VMEM(edge, BF16)] * 2,
         in_specs=[SMEM] + [VMEM] * 4 + [HBM] * 3 + [VMEM] * 2,
         out_specs=[VMEM] * 4,
         scratch_shapes=[
@@ -409,9 +424,8 @@
         out_specs=(VMEM, VMEM),
         scratch_shapes=[
             pltpu.VMEM((nc * rows, nx * 2 * HEAD_DIM), BF16),
-            pltpu.VMEM((nc * rows, width), F32),
             pltpu.VMEM((nx, 2 * HEAD_DIM, width), BF16),
-            pltpu.SemaphoreType.DMA((4,)),
+            pltpu.SemaphoreType.DMA((4, 4)),
         ],
         name="project",
         compiler_params=vmem(14),
@@ -424,7 +438,7 @@
         out_specs=VMEM,
         name="final",
         compiler_params=vmem(8),
-    )(*far(latent), *held(keep, got, planes))
+    )(*held(latent, keep, got, planes))
 
 
 def solution(mesh):

time: 145 us -> 146 us (level)
    unnamed x4 -> x16, local copies, waits for them, and re-layouts: 0.01 us -> 2.02 us
    pallas_call x1 -> x2, Pallas kernels: 5.72 us -> 7.45 us  [the longest x1 6.61 us: shards(): pl.pallas_call(qkv_kernel, out_shape=[pltpu.HBM(wide, BF16)] * 2 + [pltpu...]
  transfers between devices with their start and end apart: 14 -> 14, of which waited for: 8 -> 8; matrix products, arithmetic and copies ran while one was open for 1% -> 0% of each run, Pallas kernels for 10% -> 10%
where the time goes in v6:
time: 146 us; the launch traced here: 145 us
  starting transfers between devices  57.7 us (40%)
  waiting for transfers between devices  36.7 us (25%)
  blocking collectives  26.6 us (18%)
  Pallas kernels  19.5 us (13%)
  local copies, waits for them, and re-layouts  2.02 us (1%)
  other arithmetic  1.85 us (1%)
    all_to_all x1, blocking collectives, exchanged(): return lax.all_to_all(blocks, axis, 0, 0, tiled=True)  26.6 us
    all_to_all x4, starting transfers between devices, exchanged(): return lax.all_to_all(blocks, axis, 0, 0, tiled=True)  20.8 us
    ppermute x6, starting transfers between devices, from_other_x(): lax.ppermute(block, 'x', [(i, (i + shift) % 4) for i in range(4)])  19.8 us
    all_to_all x4, waiting for transfers between devices, exchanged(): return lax.all_to_all(blocks, axis, 0, 0, tiled=True)  17.7 us
    ppermute x6, waiting for transfers between devices, from_other_x(): lax.ppermute(block, 'x', [(i, (i + shift) % 4) for i in range(4)])  12.8 us
    ppermute x2, starting transfers between devices, swapped(): return lax.ppermute(x, 'c', [(0, 1), (1, 0)])  11.8 us
    pallas_call x1, Pallas kernels, shards(): pl.pallas_call(qkv_kernel, out_shape=[pltpu.HBM(wide, BF16)] * 2 + [pltpu...  6.61 us
    pallas_call x1, Pallas kernels, shards(): pl.pallas_call(attention_kernel, out_shape=shape_of(wide, BF16), in_specs...  5.08 us
  transfers between devices with their start and end apart: 14, of which 8 were waited for; matrix products, arithmetic and copies ran while one was open for 0% of the time, Pallas kernels for 10%

profile of v6, /device:TPU:25, one launch (start us, length us, event | category | flops | bytes accessed | tf_op | source)
XLA Modules:
  0.0 144.7 jit_solution(9922959112827479033)
XLA Ops:
  0.0 3.1 %collective-permute-start = (bf16[96,2048]{1,0:T(8,128)(2,1)}, bf16[96,2048]{1,0:T(8,128)(2,1)S(1)}, u32[]{:S(2)}, u32[]{:S(2)}) collective-permute-start(bf16[96,2048]{1,0:T(8,128)(2,1)} %latent_ref.1), channel_id=1, source_target_pairs={{0,2},{2,4},{4,6},{6,0},{1,3},{3,5},{5,7},{7,1},{8,10},{10,12},{12... | collective-permute-start | bytes 1179656 | tf_op jit(solution)/shard_map/ppermute | solution.py:288
  3.1 3.4 %collective-permute-start.1 = (bf16[96,2048]{1,0:T(8,128)(2,1)}, bf16[96,2048]{1,0:T(8,128)(2,1)S(1)}, u32[]{:S(2)}, u32[]{:S(2)}) collective-permute-start(bf16[96,2048]{1,0:T(8,128)(2,1)} %latent_ref.1), channel_id=1, source_target_pairs={{0,6},{2,0},{4,2},{6,4},{1,7},{3,1},{5,3},{7,5},{8,14},{10,8},{12,... | collective-permute-start | bytes 1179656 | tf_op jit(solution)/shard_map/ppermute | solution.py:288
  6.5 3.4 %collective-permute-start.2 = (bf16[96,2048]{1,0:T(8,128)(2,1)}, bf16[96,2048]{1,0:T(8,128)(2,1)S(1)}, u32[]{:S(2)}, u32[]{:S(2)}) collective-permute-start(bf16[96,2048]{1,0:T(8,128)(2,1)} %latent_ref.1), channel_id=1, source_target_pairs={{0,4},{2,6},{4,0},{6,2},{1,5},{3,7},{5,1},{7,3},{8,12},{10,14},{12... | collective-permute-start | bytes 1179656 | tf_op jit(solution)/shard_map/ppermute | solution.py:288
  10.0 3.4 %collective-permute-done = bf16[96,2048]{1,0:T(8,128)(2,1)S(1)} collective-permute-done((bf16[96,2048]{1,0:T(8,128)(2,1)}, bf16[96,2048]{1,0:T(8,128)(2,1)S(1)}, u32[]{:S(2)}, u32[]{:S(2)}) %collective-permute-start) | collective-permute-done | bytes 393248 | tf_op jit(solution)/shard_map/ppermute | solution.py:288
  13.3 1.6 %collective-permute-done.1 = bf16[96,2048]{1,0:T(8,128)(2,1)S(1)} collective-permute-done((bf16[96,2048]{1,0:T(8,128)(2,1)}, bf16[96,2048]{1,0:T(8,128)(2,1)S(1)}, u32[]{:S(2)}, u32[]{:S(2)}) %collective-permute-start.1) | collective-permute-done | bytes 393248 | tf_op jit(solution)/shard_map/ppermute | solution.py:288
  14.9 7.8 %collective-permute-done.2 = bf16[96,2048]{1,0:T(8,128)(2,1)S(1)} collective-permute-done((bf16[96,2048]{1,0:T(8,128)(2,1)}, bf16[96,2048]{1,0:T(8,128)(2,1)S(1)}, u32[]{:S(2)}, u32[]{:S(2)}) %collective-permute-start.2) | collective-permute-done | bytes 393248 | tf_op jit(solution)/shard_map/ppermute | solution.py:288
  24.0 3.8 %collective-permute-start.3 = (bf16[4,96,2048]{2,1,0:T(8,128)(2,1)S(1)}, bf16[4,96,2048]{2,1,0:T(8,128)(2,1)}, u32[]{:S(2)}, u32[]{:S(2)}) collective-permute-start(bf16[4,96,2048]{2,1,0:T(8,128)(2,1)S(1)} %pad_maximum_fusion.own_ref), channel_id=1, source_target_pairs={{0,1},{1,0},{2,3},{3,2},{4,5},{5,4},{6,7},{7,6},{8,9},{9,8},{10,11... | collective-permute-start | bytes 4718600 | tf_op jit(solution)/shard_map/ppermute | solution.py:293
  28.8 26.6 %all_to_all.25.parts_ref = f32[16,1,1280]{2,1,0:T(1,128)S(1)} all-to-all(f32[16,1,1280]{2,1,0:T(1,128)S(1)} %parts.1), channel_id=1, replica_groups=mesh['z'=16,'y'=4,'x'=4,'c'=2] {'z'}, dimensions={0} | all-to-all | bytes 163840 | tf_op jit(solution)/shard_map/all_to_all | solution.py:47
  56.1 9.6 %all-to-all-start.1 = ((f32[32,1,1280]{2,1,0:T(1,128)}), f32[32,1,1280]{2,1,0:T(1,128)S(1)}, u32[]{:S(2)}, u32[]{:S(2)}) async-start(f32[32,1,1280]{2,1,0:T(1,128)} %sums.1), calls=%async_computation.1 | async-start | bytes 327680 | tf_op jit(solution)/shard_map/all_to_all | solution.py:47
  65.7 3.1 %collective-permute-start.6 = (bf16[256,2048]{1,0:T(8,128)(2,1)}, bf16[256,2048]{1,0:T(8,128)(2,1)}, u32[]{:S(2)}, u32[]{:S(2)}) collective-permute-start(bf16[256,2048]{1,0:T(8,128)(2,1)} %w0_ref.1), channel_id=1, source_target_pairs={{0,2},{2,4},{4,6},{6,0},{1,3},{3,5},{5,7},{7,1},{8,10},{10,12},{12... | collective-permute-start | bytes 3145736 | tf_op jit(solution)/shard_map/ppermute | solution.py:288
  68.8 3.4 %collective-permute-start.7 = (bf16[256,2048]{1,0:T(8,128)(2,1)}, bf16[256,2048]{1,0:T(8,128)(2,1)}, u32[]{:S(2)}, u32[]{:S(2)}) collective-permute-start(bf16[256,2048]{1,0:T(8,128)(2,1)} %w0_ref.1), channel_id=1, source_target_pairs={{0,6},{2,0},{4,2},{6,4},{1,7},{3,1},{5,3},{7,5},{8,14},{10,8},{12,... | collective-permute-start | bytes 3145736 | tf_op jit(solution)/shard_map/ppermute | solution.py:288
  72.2 3.4 %collective-permute-start.8 = (bf16[256,2048]{1,0:T(8,128)(2,1)}, bf16[256,2048]{1,0:T(8,128)(2,1)}, u32[]{:S(2)}, u32[]{:S(2)}) collective-permute-start(bf16[256,2048]{1,0:T(8,128)(2,1)} %w0_ref.1), channel_id=1, source_target_pairs={{0,4},{2,6},{4,0},{6,2},{1,5},{3,7},{5,1},{7,3},{8,12},{10,14},{12... | collective-permute-start | bytes 3145736 | tf_op jit(solution)/shard_map/ppermute | solution.py:288
  76.7 3.5 %all-to-all-start.2 = ((bf16[16,16,256]{2,1,0:T(8,128)(2,1)}), bf16[16,16,256]{2,1,0:T(8,128)(2,1)S(1)}, u32[]{:S(2)}, u32[]{:S(2)}) async-start(bf16[16,16,256]{2,1,0:T(8,128)(2,1)} %context_pairs.1), calls=%async_computation.2 | async-start | bytes 262144 | tf_op jit(solution)/shard_map/all_to_all | solution.py:47
  80.6 11.5 %all-to-all-done.2 = bf16[16,16,256]{2,1,0:T(8,128)(2,1)S(1)} async-done(((bf16[16,16,256]{2,1,0:T(8,128)(2,1)}), bf16[16,16,256]{2,1,0:T(8,128)(2,1)S(1)}, u32[]{:S(2)}, u32[]{:S(2)}) %all-to-all-start.2) | async-done | bytes 131104 | tf_op jit(solution)/shard_map/all_to_all | solution.py:47
  92.9 4.2 %all-to-all-start.3 = ((bf16[4,256,256]{2,1,0:T(8,128)(2,1)}), bf16[4,256,256]{2,1,0:T(8,128)(2,1)S(1)}, u32[]{:S(2)}, u32[]{:S(2)}) async-start(bf16[4,256,256]{2,1,0:T(8,128)(2,1)} %spread.1), calls=%async_computation.3 | async-start | bytes 1048576 | tf_op jit(solution)/shard_map/all_to_all | solution.py:47
  97.4 6.6 %qkv.1 = (bf16[768,256]{1,0:T(8,128)(2,1)}, bf16[768,256]{1,0:T(8,128)(2,1)}, bf16[128,256]{1,0:T(8,128)(2,1)S(1)}, bf16[128,256]{1,0:T(8,128)(2,1)S(1)}) custom-call(s32[4]{0:T(128)S(1)} %pad_add_fusion.place_ref, bf16[4,96,2048]{2,1,0:T(8,128)(2,1)S(1)} %pad_maximum_fusion.own_ref, bf16[4,96,2048]{2,1,0:T(8,128)(2,1)} %collective-permute-done.3.other_ref, ...), custom_call_target="tpu_custom_call" | custom-call | tf_op jit(solution)/shard_map/qkv/pallas_call | solution.py:384
  104.0 2.7 %collective-permute-start.4 = (bf16[128,256]{1,0:T(8,128)(2,1)S(1)}, bf16[128,256]{1,0:T(8,128)(2,1)S(1)}, u32[]{:S(2)}, u32[]{:S(2)}) collective-permute-start(bf16[128,256]{1,0:T(8,128)(2,1)S(1)} %get-tuple-element.12), channel_id=1, source_target_pairs={{0,8},{8,16},{16,24},{24,32},{32,40},{40,48},{48,56},{56,64},{64,7... | collective-permute-start | bytes 196616 | tf_op jit(solution)/shard_map/ppermute | solution.py:403
  106.7 2.6 %collective-permute-start.5 = (bf16[128,256]{1,0:T(8,128)(2,1)S(1)}, bf16[128,256]{1,0:T(8,128)(2,1)S(1)}, u32[]{:S(2)}, u32[]{:S(2)}) collective-permute-start(bf16[128,256]{1,0:T(8,128)(2,1)S(1)} %get-tuple-element.14), channel_id=1, source_target_pairs={{8,0},{16,8},{24,16},{32,24},{40,32},{48,40},{56,48},{64,56},{72,6... | collective-permute-start | bytes 196616 | tf_op jit(solution)/shard_map/ppermute | solution.py:404
  109.4 4.8 %collective-permute-done.5.high_ref = bf16[128,256]{1,0:T(8,128)(2,1)S(1)} collective-permute-done((bf16[128,256]{1,0:T(8,128)(2,1)S(1)}, bf16[128,256]{1,0:T(8,128)(2,1)S(1)}, u32[]{:S(2)}, u32[]{:S(2)}) %collective-permute-start.5) | collective-permute-done | bytes 65568 | tf_op jit(solution)/shard_map/ppermute | solution.py:404
  116.3 5.1 %attention.1 = bf16[768,256]{1,0:T(8,128)(2,1)} custom-call(s32[4]{0:T(128)S(1)} %pad_add_fusion.place_ref, f32[2]{0:T(128)S(1)} %copy-done.7, bf16[768,256]{1,0:T(8,128)(2,1)S(1)} %copy-done.3, bf16[128,256]{1,0:T(8,128)(2,1)S(1)} %collective-permute-done.4.low_ref, bf16[768,256]{1,0:T(8,128)(2,1)S(1)} %copy-done.4, ...), custom_call_target="tpu_custom_call" | custom-call | tf_op jit(solution)/shard_map/attention/pallas_call | solution.py:406
  121.3 3.5 %all-to-all-start.4 = ((bf16[4,192,256]{2,1,0:T(8,128)(2,1)}), bf16[4,192,256]{2,1,0:T(8,128)(2,1)S(1)}, u32[]{:S(2)}, u32[]{:S(2)}) async-start(bf16[4,192,256]{2,1,0:T(8,128)(2,1)} %bitcast.13), calls=%async_computation.4 | async-start | bytes 786432 | tf_op jit(solution)/shard_map/all_to_all | solution.py:47
  124.8 6.2 %all-to-all-done.4.attended_ref = bf16[4,192,256]{2,1,0:T(8,128)(2,1)S(1)} async-done(((bf16[4,192,256]{2,1,0:T(8,128)(2,1)}), bf16[4,192,256]{2,1,0:T(8,128)(2,1)S(1)}, u32[]{:S(2)}, u32[]{:S(2)}) %all-to-all-start.4) | async-done | bytes 393248 | tf_op jit(solution)/shard_map/all_to_all | solution.py:47
  131.0 3.4 %project.1 = (bf16[96,2048]{1,0:T(8,128)(2,1)S(1)}, f32[96,2048]{1,0:T(8,128)S(1)}) custom-call(s32[4]{0:T(128)S(1)} %pad_add_fusion.place_ref, bf16[4,192,256]{2,1,0:T(8,128)(2,1)S(1)} %all-to-all-done.4.attended_ref, bf16[256,2048]{1,0:T(8,128)(2,1)} %w0_ref.1, bf16[256,2048]{1,0:T(8,128)(2,1)} %collective-permute-done.6.w1_ref, ...), custom_call_target="tpu_custom_call" | custom-call | tf_op jit(solution)/shard_map/project/pallas_call | solution.py:420
  134.4 8.0 %collective-permute-start.9 = (bf16[96,2048]{1,0:T(8,128)(2,1)S(1)}, bf16[96,2048]{1,0:T(8,128)(2,1)S(1)}, u32[]{:S(2)}, u32[]{:S(2)}) collective-permute-start(bf16[96,2048]{1,0:T(8,128)(2,1)S(1)} %get-tuple-element.16), channel_id=1, source_target_pairs={{0,1},{1,0},{2,3},{3,2},{4,5},{5,4},{6,7},{7,6},{8,9},{9,8},{10,11... | collective-permute-start | bytes 1179656 | tf_op jit(solution)/shard_map/ppermute | solution.py:293
  (38 shorter events, 9.7 us)
Async XLA Ops:
  0.0 13.3 %collective-permute-start = (bf16[96,2048]{1,0:T(8,128)(2,1)}, bf16[96,2048]{1,0:T(8,128)(2,1)S(1)}, u32[]{:S(2)}, u32[]{:S(2)}) collective-permute-start(bf16[96,2048]{1,0:T(8,128)(2,1)} %latent_ref.1), channel_id=1, source_target_pairs={{0,2},{2,4},{4,6},{6,0},{1,3},{3,5},{5,7},{7,1},{8,10},{10,12},{12... | collective-permute-start | bytes 1179656 | tf_op jit(solution)/shard_map/ppermute | solution.py:288
  3.1 11.8 %collective-permute-start.1 = (bf16[96,2048]{1,0:T(8,128)(2,1)}, bf16[96,2048]{1,0:T(8,128)(2,1)S(1)}, u32[]{:S(2)}, u32[]{:S(2)}) collective-permute-start(bf16[96,2048]{1,0:T(8,128)(2,1)} %latent_ref.1), channel_id=1, source_target_pairs={{0,6},{2,0},{4,2},{6,4},{1,7},{3,1},{5,3},{7,5},{8,14},{10,8},{12,... | collective-permute-start | bytes 1179656 | tf_op jit(solution)/shard_map/ppermute | solution.py:288
  6.5 16.2 %collective-permute-start.2 = (bf16[96,2048]{1,0:T(8,128)(2,1)}, bf16[96,2048]{1,0:T(8,128)(2,1)S(1)}, u32[]{:S(2)}, u32[]{:S(2)}) collective-permute-start(bf16[96,2048]{1,0:T(8,128)(2,1)} %latent_ref.1), channel_id=1, source_target_pairs={{0,4},{2,6},{4,0},{6,2},{1,5},{3,7},{5,1},{7,3},{8,12},{10,14},{12... | collective-permute-start | bytes 1179656 | tf_op jit(solution)/shard_map/ppermute | solution.py:288
  22.7 52.9 %copy-start = (bf16[2048,128]{1,0:T(8,128)(2,1)S(1)}, bf16[2048,128]{1,0:T(8,128)(2,1)}, u32[]{:S(2)}) copy-start(bf16[2048,128]{1,0:T(8,128)(2,1)} %wk_ref.3) | copy-start | bytes 1572868
  22.7 52.9 %copy-start.1 = (bf16[2048,128]{1,0:T(8,128)(2,1)S(1)}, bf16[2048,128]{1,0:T(8,128)(2,1)}, u32[]{:S(2)}) copy-start(bf16[2048,128]{1,0:T(8,128)(2,1)} %wv_ref.3) | copy-start | bytes 1572868
  22.7 52.9 %copy-start.5 = (bf16[16,2048]{1,0:T(8,128)(2,1)S(1)}, bf16[16,2048]{1,0:T(8,128)(2,1)}, u32[]{:S(2)}) copy-start(bf16[16,2048]{1,0:T(8,128)(2,1)} %ctx_ref.1) | copy-start | bytes 196612
  22.7 52.9 %copy-start.6 = (f32[2048]{0:T(1024)S(1)}, f32[2048]{0:T(1024)}, u32[]{:S(2)}) copy-start(f32[2048]{0:T(1024)} %param.17) | copy-start | bytes 24580
  24.0 73.4 %collective-permute-start.3 = (bf16[4,96,2048]{2,1,0:T(8,128)(2,1)S(1)}, bf16[4,96,2048]{2,1,0:T(8,128)(2,1)}, u32[]{:S(2)}, u32[]{:S(2)}) collective-permute-start(bf16[4,96,2048]{2,1,0:T(8,128)(2,1)S(1)} %pad_maximum_fusion.own_ref), channel_id=1, source_target_pairs={{0,1},{1,0},{2,3},{3,2},{4,5},{5,4},{6,7},{7,6},{8,9},{9,8},{10,11... | collective-permute-start | bytes 4718600 | tf_op jit(solution)/shard_map/ppermute | solution.py:293
  56.1 19.5 %all-to-all-start.1 = ((f32[32,1,1280]{2,1,0:T(1,128)}), f32[32,1,1280]{2,1,0:T(1,128)S(1)}, u32[]{:S(2)}, u32[]{:S(2)}) async-start(f32[32,1,1280]{2,1,0:T(1,128)} %sums.1), calls=%async_computation.1 | async-start | bytes 327680 | tf_op jit(solution)/shard_map/all_to_all | solution.py:47
  65.7 59.1 %collective-permute-start.6 = (bf16[256,2048]{1,0:T(8,128)(2,1)}, bf16[256,2048]{1,0:T(8,128)(2,1)}, u32[]{:S(2)}, u32[]{:S(2)}) collective-permute-start(bf16[256,2048]{1,0:T(8,128)(2,1)} %w0_ref.1), channel_id=1, source_target_pairs={{0,2},{2,4},{4,6},{6,0},{1,3},{3,5},{5,7},{7,1},{8,10},{10,12},{12... | collective-permute-start | bytes 3145736 | tf_op jit(solution)/shard_map/ppermute | solution.py:288
  68.8 56.0 %collective-permute-start.7 = (bf16[256,2048]{1,0:T(8,128)(2,1)}, bf16[256,2048]{1,0:T(8,128)(2,1)}, u32[]{:S(2)}, u32[]{:S(2)}) collective-permute-start(bf16[256,2048]{1,0:T(8,128)(2,1)} %w0_ref.1), channel_id=1, source_target_pairs={{0,6},{2,0},{4,2},{6,4},{1,7},{3,1},{5,3},{7,5},{8,14},{10,8},{12,... | collective-permute-start | bytes 3145736 | tf_op jit(solution)/shard_map/ppermute | solution.py:288
  72.2 52.7 %collective-permute-start.8 = (bf16[256,2048]{1,0:T(8,128)(2,1)}, bf16[256,2048]{1,0:T(8,128)(2,1)}, u32[]{:S(2)}, u32[]{:S(2)}) collective-permute-start(bf16[256,2048]{1,0:T(8,128)(2,1)} %w0_ref.1), channel_id=1, source_target_pairs={{0,4},{2,6},{4,0},{6,2},{1,5},{3,7},{5,1},{7,3},{8,12},{10,14},{12... | collective-permute-start | bytes 3145736 | tf_op jit(solution)/shard_map/ppermute | solution.py:288
  76.7 15.4 %all-to-all-start.2 = ((bf16[16,16,256]{2,1,0:T(8,128)(2,1)}), bf16[16,16,256]{2,1,0:T(8,128)(2,1)S(1)}, u32[]{:S(2)}, u32[]{:S(2)}) async-start(bf16[16,16,256]{2,1,0:T(8,128)(2,1)} %context_pairs.1), calls=%async_computation.2 | async-start | bytes 262144 | tf_op jit(solution)/shard_map/all_to_all | solution.py:47
  92.9 16.4 %all-to-all-start.3 = ((bf16[4,256,256]{2,1,0:T(8,128)(2,1)}), bf16[4,256,256]{2,1,0:T(8,128)(2,1)S(1)}, u32[]{:S(2)}, u32[]{:S(2)}) async-start(bf16[4,256,256]{2,1,0:T(8,128)(2,1)} %spread.1), calls=%async_computation.3 | async-start | bytes 1048576 | tf_op jit(solution)/shard_map/all_to_all | solution.py:47
  97.4 16.9 %copy-start.7 = (f32[2]{0:T(128)S(1)}, f32[2]{0:T(128)}, u32[]{:S(2)}) copy-start(f32[2]{0:T(128)} %sink_ref.1) | copy-start | bytes 28
  104.0 5.4 %collective-permute-start.4 = (bf16[128,256]{1,0:T(8,128)(2,1)S(1)}, bf16[128,256]{1,0:T(8,128)(2,1)S(1)}, u32[]{:S(2)}, u32[]{:S(2)}) collective-permute-start(bf16[128,256]{1,0:T(8,128)(2,1)S(1)} %get-tuple-element.12), channel_id=1, source_target_pairs={{0,8},{8,16},{16,24},{24,32},{32,40},{40,48},{48,56},{56,64},{64,7... | collective-permute-start | bytes 196616 | tf_op jit(solution)/shard_map/ppermute | solution.py:403
  106.7 7.5 %collective-permute-start.5 = (bf16[128,256]{1,0:T(8,128)(2,1)S(1)}, bf16[128,256]{1,0:T(8,128)(2,1)S(1)}, u32[]{:S(2)}, u32[]{:S(2)}) collective-permute-start(bf16[128,256]{1,0:T(8,128)(2,1)S(1)} %get-tuple-element.14), channel_id=1, source_target_pairs={{8,0},{16,8},{24,16},{32,24},{40,32},{48,40},{56,48},{64,56},{72,6... | collective-permute-start | bytes 196616 | tf_op jit(solution)/shard_map/ppermute | solution.py:404
  114.3 1.0 copy-start.3
  115.3 1.0 copy-start.4
  121.3 9.7 %all-to-all-start.4 = ((bf16[4,192,256]{2,1,0:T(8,128)(2,1)}), bf16[4,192,256]{2,1,0:T(8,128)(2,1)S(1)}, u32[]{:S(2)}, u32[]{:S(2)}) async-start(bf16[4,192,256]{2,1,0:T(8,128)(2,1)} %bitcast.13), calls=%async_computation.4 | async-start | bytes 786432 | tf_op jit(solution)/shard_map/all_to_all | solution.py:47
  124.8 19.0 %copy-start.2 = (bf16[96,2048]{1,0:T(8,128)(2,1)S(1)}, bf16[96,2048]{1,0:T(8,128)(2,1)}, u32[]{:S(2)}) copy-start(bf16[96,2048]{1,0:T(8,128)(2,1)} %latent_ref.1) | copy-start | bytes 1179652
  134.4 9.3 %collective-permute-start.9 = (bf16[96,2048]{1,0:T(8,128)(2,1)S(1)}, bf16[96,2048]{1,0:T(8,128)(2,1)S(1)}, u32[]{:S(2)}, u32[]{:S(2)}) collective-permute-start(bf16[96,2048]{1,0:T(8,128)(2,1)S(1)} %get-tuple-element.16), channel_id=1, source_target_pairs={{0,1},{1,0},{2,3},{3,2},{4,5},{5,4},{6,7},{7,6},{8,9},{9,8},{10,11... | collective-permute-start | bytes 1179656 | tf_op jit(solution)/shard_map/ppermute | solution.py:293

commit v7 on v6

--- a/solution.py
+++ b/solution.py
@@ -158,15 +158,24 @@
     bottom_ref[...] = kv_ref[hidden_ref.shape[0] - WINDOW_REACH :, :]
 
 
-def context_kernel(ctx_ref, planes_ref, gain_ref, wk_ref, wv_ref, out_ref):
+def context_kernel(
+    ctx_ref, planes_ref, gain_ref, wk_ref, wv_ref, out_ref, wkv_ref, sems
+):
+    loads = (
+        pltpu.make_async_copy(wk_ref, wkv_ref.at[:, :HEAD_DIM], sems.at[0]),
+        pltpu.make_async_copy(wv_ref, wkv_ref.at[:, HEAD_DIM:], sems.at[1]),
+    )
+    for load in loads:
+        load.start()
     columns = planes_ref.shape[2] // 5
     shift = row_vector(planes_ref, 1, columns)
     multiplier = gain_ref[...] * (1.0 + row_vector(planes_ref, 3, columns))
     rows = ctx_ref[...].astype(F32)
     mean = jnp.mean(rows * rows, axis=-1, keepdims=True)
     hidden = (rows * lax.rsqrt(mean + NORM_EPS) * multiplier + shift).astype(BF16)
-    pairs = jnp.concatenate([dot(hidden, wk_ref[...]), dot(hidden, wv_ref[...])], axis=1)
-    pairs = pairs.astype(BF16)
+    for load in loads:
+        load.wait()
+    pairs = dot(hidden, wkv_ref[...]).astype(BF16)
     for p in range(out_ref.shape[0]):
         out_ref[p] = pairs
 
@@ -234,16 +243,27 @@
     lax.fori_loop(0, blocks, step, 0, unroll=2)
 
 
+def load_kernel(w0_ref, w1_ref, out_ref, sems):
+    loads = [
+        pltpu.make_async_copy(w, out_ref.at[j], sems.at[j])
+        for j, w in enumerate((w0_ref, w1_ref))
+    ]
+    for load in loads:
+        load.start()
+    for load in loads:
+        load.wait()
+
+
 def project_kernel(
-    place_ref, attended_ref, w0_ref, w1_ref, w2_ref, w3_ref, send_ref, keep_ref,
-    rows_ref, weights_ref, sems,
+    place_ref, attended_ref, early_ref, w2_ref, w3_ref, send_ref, keep_ref,
+    rows_ref, late_ref, sems,
 ):
     width = 512
     cuts = [slice(n, n + width) for n in range(0, send_ref.shape[1], width)]
     loads = [
         [
-            pltpu.make_async_copy(w.at[:, cut], weights_ref.at[j, :, cut], sems.at[n, j])
-            for j, w in enumerate((w0_ref, w1_ref, w2_ref, w3_ref))
+            pltpu.make_async_copy(w.at[:, cut], late_ref.at[j, :, cut], sems.at[n, j])
+            for j, w in enumerate((w2_ref, w3_ref))
         ]
         for n, cut in enumerate(cuts)
     ]
@@ -261,11 +281,13 @@
         rows_ref[:rows, cut] = attended_ref[source, pl.ds(theirs, rows), :]
         rows_ref[rows:, cut] = attended_ref[source, pl.ds(mine, rows), :]
     for group, cut in zip(loads, cuts):
+        total = dot(rows_ref[:, :deep], early_ref[0, :, cut])
+        total = total + dot(rows_ref[:, deep : 2 * deep], early_ref[1, :, cut])
         for load in group:
             load.wait()
-        total = dot(rows_ref[:, :deep], weights_ref[0, :, cut])
-        for j in range(1, 4):
-            total = total + dot(rows_ref[:, j * deep : (j + 1) * deep], weights_ref[j, :, cut])
+        for j in range(2):
+            part = slice((2 + j) * deep, (3 + j) * deep)
+            total = total + dot(rows_ref[:, part], late_ref[j, :, cut])
         send_ref[:, cut] = total[:rows].astype(BF16)
         keep_ref[:, cut] = total[rows:]
 
@@ -363,11 +385,15 @@
     pairs = pl.pallas_call(
         context_kernel,
         out_shape=shape_of((nz, ctx_rows, 2 * HEAD_DIM), BF16),
-        in_specs=[VMEM] * 5,
+        in_specs=[VMEM] * 3 + [HBM] * 2,
         out_specs=VMEM,
+        scratch_shapes=[
+            pltpu.VMEM((width, 2 * HEAD_DIM), BF16),
+            pltpu.SemaphoreType.DMA((2,)),
+        ],
         name="context_pairs",
         compiler_params=vmem(8),
-    )(*held(context, planes, gain, key_matrix, value_matrix))
+    )(*far(context), *held(planes), *far(gain, key_matrix, value_matrix))
     ctx_z = exchanged(pairs, "z").reshape(nz * ctx_rows, 2 * HEAD_DIM)
     spread = pl.pallas_call(
         spread_kernel,
@@ -417,19 +443,28 @@
         compiler_params=vmem(16),
     )(where, sink_logit_head, *held(queries, low, pairs, high, ctx_pairs))
     attended = exchanged(attended.reshape(nx, nc * rows, 2 * HEAD_DIM), "x")
+    weights = pl.pallas_call(
+        load_kernel,
+        out_shape=pltpu.VMEM((2, *out_weight.shape), BF16),
+        in_specs=[HBM] * 2,
+        out_specs=VMEM,
+        scratch_shapes=[pltpu.SemaphoreType.DMA((2,))],
+        name="load",
+        compiler_params=vmem(2),
+    )(*far(out_weight, out_others[0]))
     send, keep = pl.pallas_call(
         project_kernel,
         out_shape=[pltpu.VMEM((rows, width), BF16), pltpu.VMEM((rows, width), F32)],
-        in_specs=[SMEM, VMEM] + [HBM] * 4,
+        in_specs=[SMEM, VMEM, VMEM, HBM, HBM],
         out_specs=(VMEM, VMEM),
         scratch_shapes=[
             pltpu.VMEM((nc * rows, nx * 2 * HEAD_DIM), BF16),
-            pltpu.VMEM((nx, 2 * HEAD_DIM, width), BF16),
-            pltpu.SemaphoreType.DMA((4, 4)),
+            pltpu.VMEM((2, 2 * HEAD_DIM, width), BF16),
+            pltpu.SemaphoreType.DMA((4, 2)),
         ],
         name="project",
         compiler_params=vmem(14),
-    )(where, *held(attended), *far(out_weight, *out_others))
+    )(where, *held(attended, weights), *far(*out_others[1:]))
     got = swapped(send)
     return pl.pallas_call(
         final_kernel,

time: 146 us -> 147 us (level)
  Pallas kernels: 19.5 us -> 22.4 us
  waiting for transfers between devices: 36.7 us -> 35.1 us
    pallas_call x1, Pallas kernels: 1.01 us -> 2.98 us  [shards(): pl.pallas_call(context_kernel, out_shape=shape_of((nz, ctx_rows, 2 * HEAD...]
    all_to_all x4, waiting for transfers between devices: 17.7 us -> 16.1 us  [exchanged(): return lax.all_to_all(blocks, axis, 0, 0, tiled=True)]
    pallas_call x0 -> x1, Pallas kernels: none -> 1.56 us  [shards(): pl.pallas_call(load_kernel, out_shape=pltpu.VMEM((2, *out_weight.shape),...]
  transfers between devices with their start and end apart: 14 -> 14, of which waited for: 8 -> 8; matrix products, arithmetic and copies ran while one was open for 0% -> 0% of each run, Pallas kernels for 10% -> 13%
where the time goes in v7:
time: 147 us; the launch traced here: 146 us
  starting transfers between devices  57.7 us (39%)
  waiting for transfers between devices  35.1 us (24%)
  blocking collectives  26.6 us (18%)
  Pallas kernels  22.4 us (15%)
  local copies, waits for them, and re-layouts  2.01 us (1%)
  other arithmetic  1.75 us (1%)
    all_to_all x1, blocking collectives, exchanged(): return lax.all_to_all(blocks, axis, 0, 0, tiled=True)  26.6 us
    all_to_all x4, starting transfers between devices, exchanged(): return lax.all_to_all(blocks, axis, 0, 0, tiled=True)  20.8 us
    ppermute x6, starting transfers between devices, from_other_x(): lax.ppermute(block, 'x', [(i, (i + shift) % 4) for i in range(4)])  19.8 us
    all_to_all x4, waiting for transfers between devices, exchanged(): return lax.all_to_all(blocks, axis, 0, 0, tiled=True)  16.1 us
    ppermute x6, waiting for transfers between devices, from_other_x(): lax.ppermute(block, 'x', [(i, (i + shift) % 4) for i in range(4)])  12.8 us
    ppermute x2, starting transfers between devices, swapped(): return lax.ppermute(x, 'c', [(0, 1), (1, 0)])  11.8 us
    pallas_call x1, Pallas kernels, shards(): pl.pallas_call(qkv_kernel, out_shape=[pltpu.HBM(wide, BF16)] * 2 + [pltpu...  6.61 us
    pallas_call x1, Pallas kernels, shards(): pl.pallas_call(attention_kernel, out_shape=shape_of(wide, BF16), in_specs...  5.02 us
  transfers between devices with their start and end apart: 14, of which 8 were waited for; matrix products, arithmetic and copies ran while one was open for 0% of the time, Pallas kernels for 13%

profile of v7, /device:TPU:25, one launch (start us, length us, event | category | flops | bytes accessed | tf_op | source)
XLA Modules:
  0.0 145.9 jit_solution(16470261151306853829)
XLA Ops:
  0.0 3.1 %collective-permute-start = (bf16[96,2048]{1,0:T(8,128)(2,1)}, bf16[96,2048]{1,0:T(8,128)(2,1)S(1)}, u32[]{:S(2)}, u32[]{:S(2)}) collective-permute-start(bf16[96,2048]{1,0:T(8,128)(2,1)} %latent_ref.1), channel_id=1, source_target_pairs={{0,2},{2,4},{4,6},{6,0},{1,3},{3,5},{5,7},{7,1},{8,10},{10,12},{12... | collective-permute-start | bytes 1179656 | tf_op jit(solution)/shard_map/ppermute | solution.py:310
  3.1 3.4 %collective-permute-start.1 = (bf16[96,2048]{1,0:T(8,128)(2,1)}, bf16[96,2048]{1,0:T(8,128)(2,1)S(1)}, u32[]{:S(2)}, u32[]{:S(2)}) collective-permute-start(bf16[96,2048]{1,0:T(8,128)(2,1)} %latent_ref.1), channel_id=1, source_target_pairs={{0,6},{2,0},{4,2},{6,4},{1,7},{3,1},{5,3},{7,5},{8,14},{10,8},{12,... | collective-permute-start | bytes 1179656 | tf_op jit(solution)/shard_map/ppermute | solution.py:310
  6.5 3.4 %collective-permute-start.2 = (bf16[96,2048]{1,0:T(8,128)(2,1)}, bf16[96,2048]{1,0:T(8,128)(2,1)S(1)}, u32[]{:S(2)}, u32[]{:S(2)}) collective-permute-start(bf16[96,2048]{1,0:T(8,128)(2,1)} %latent_ref.1), channel_id=1, source_target_pairs={{0,4},{2,6},{4,0},{6,2},{1,5},{3,7},{5,1},{7,3},{8,12},{10,14},{12... | collective-permute-start | bytes 1179656 | tf_op jit(solution)/shard_map/ppermute | solution.py:310
  10.0 3.4 %collective-permute-done = bf16[96,2048]{1,0:T(8,128)(2,1)S(1)} collective-permute-done((bf16[96,2048]{1,0:T(8,128)(2,1)}, bf16[96,2048]{1,0:T(8,128)(2,1)S(1)}, u32[]{:S(2)}, u32[]{:S(2)}) %collective-permute-start) | collective-permute-done | bytes 393248 | tf_op jit(solution)/shard_map/ppermute | solution.py:310
  14.9 7.8 %collective-permute-done.2 = bf16[96,2048]{1,0:T(8,128)(2,1)S(1)} collective-permute-done((bf16[96,2048]{1,0:T(8,128)(2,1)}, bf16[96,2048]{1,0:T(8,128)(2,1)S(1)}, u32[]{:S(2)}, u32[]{:S(2)}) %collective-permute-start.2) | collective-permute-done | bytes 393248 | tf_op jit(solution)/shard_map/ppermute | solution.py:310
  23.9 3.8 %collective-permute-start.3 = (bf16[4,96,2048]{2,1,0:T(8,128)(2,1)S(1)}, bf16[4,96,2048]{2,1,0:T(8,128)(2,1)}, u32[]{:S(2)}, u32[]{:S(2)}) collective-permute-start(bf16[4,96,2048]{2,1,0:T(8,128)(2,1)S(1)} %pad_maximum_fusion.own_ref), channel_id=1, source_target_pairs={{0,1},{1,0},{2,3},{3,2},{4,5},{5,4},{6,7},{7,6},{8,9},{9,8},{10,11... | collective-permute-start | bytes 4718600 | tf_op jit(solution)/shard_map/ppermute | solution.py:315
  28.6 26.6 %all_to_all.25.parts_ref = f32[16,1,1280]{2,1,0:T(1,128)S(1)} all-to-all(f32[16,1,1280]{2,1,0:T(1,128)S(1)} %parts.1), channel_id=1, replica_groups=mesh['z'=16,'y'=4,'x'=4,'c'=2] {'z'}, dimensions={0} | all-to-all | bytes 163840 | tf_op jit(solution)/shard_map/all_to_all | solution.py:47
  56.0 9.6 %all-to-all-start.1 = ((f32[32,1,1280]{2,1,0:T(1,128)}), f32[32,1,1280]{2,1,0:T(1,128)S(1)}, u32[]{:S(2)}, u32[]{:S(2)}) async-start(f32[32,1,1280]{2,1,0:T(1,128)} %sums.1), calls=%async_computation.1 | async-start | bytes 327680 | tf_op jit(solution)/shard_map/all_to_all | solution.py:47
  65.6 3.1 %collective-permute-start.6 = (bf16[256,2048]{1,0:T(8,128)(2,1)}, bf16[256,2048]{1,0:T(8,128)(2,1)}, u32[]{:S(2)}, u32[]{:S(2)}) collective-permute-start(bf16[256,2048]{1,0:T(8,128)(2,1)} %w0_ref.1), channel_id=1, source_target_pairs={{0,2},{2,4},{4,6},{6,0},{1,3},{3,5},{5,7},{7,1},{8,10},{10,12},{12... | collective-permute-start | bytes 3145736 | tf_op jit(solution)/shard_map/ppermute | solution.py:310
  68.7 3.4 %collective-permute-start.7 = (bf16[256,2048]{1,0:T(8,128)(2,1)}, bf16[256,2048]{1,0:T(8,128)(2,1)}, u32[]{:S(2)}, u32[]{:S(2)}) collective-permute-start(bf16[256,2048]{1,0:T(8,128)(2,1)} %w0_ref.1), channel_id=1, source_target_pairs={{0,6},{2,0},{4,2},{6,4},{1,7},{3,1},{5,3},{7,5},{8,14},{10,8},{12,... | collective-permute-start | bytes 3145736 | tf_op jit(solution)/shard_map/ppermute | solution.py:310
  72.1 3.4 %collective-permute-start.8 = (bf16[256,2048]{1,0:T(8,128)(2,1)}, bf16[256,2048]{1,0:T(8,128)(2,1)}, u32[]{:S(2)}, u32[]{:S(2)}) collective-permute-start(bf16[256,2048]{1,0:T(8,128)(2,1)} %w0_ref.1), channel_id=1, source_target_pairs={{0,4},{2,6},{4,0},{6,2},{1,5},{3,7},{5,1},{7,3},{8,12},{10,14},{12... | collective-permute-start | bytes 3145736 | tf_op jit(solution)/shard_map/ppermute | solution.py:310
  75.5 3.0 %context_pairs.1 = bf16[16,16,256]{2,1,0:T(8,128)(2,1)} custom-call(bf16[16,2048]{1,0:T(8,128)(2,1)} %ctx_ref.1, f32[32,1,1280]{2,1,0:T(1,128)S(1)} %all-to-all-done.1.planes_ref, f32[1,2048]{1,0:T(1,128)} %bitcast.17, bf16[2048,128]{1,0:T(8,128)(2,1)} %wk_ref.3, bf16[2048,128]{1,0:T(8,128)(2,1)} %wv_ref.3), custom_call_target="tpu_custom_call" | custom-call | tf_op jit(solution)/shard_map/context_pairs/pallas_call | solution.py:385
  78.5 3.5 %all-to-all-start.2 = ((bf16[16,16,256]{2,1,0:T(8,128)(2,1)}), bf16[16,16,256]{2,1,0:T(8,128)(2,1)S(1)}, u32[]{:S(2)}, u32[]{:S(2)}) async-start(bf16[16,16,256]{2,1,0:T(8,128)(2,1)} %context_pairs.1), calls=%async_computation.2 | async-start | bytes 262144 | tf_op jit(solution)/shard_map/all_to_all | solution.py:47
  82.4 11.5 %all-to-all-done.2 = bf16[16,16,256]{2,1,0:T(8,128)(2,1)S(1)} async-done(((bf16[16,16,256]{2,1,0:T(8,128)(2,1)}), bf16[16,16,256]{2,1,0:T(8,128)(2,1)S(1)}, u32[]{:S(2)}, u32[]{:S(2)}) %all-to-all-start.2) | async-done | bytes 131104 | tf_op jit(solution)/shard_map/all_to_all | solution.py:47
  94.8 4.2 %all-to-all-start.3 = ((bf16[4,256,256]{2,1,0:T(8,128)(2,1)}), bf16[4,256,256]{2,1,0:T(8,128)(2,1)S(1)}, u32[]{:S(2)}, u32[]{:S(2)}) async-start(bf16[4,256,256]{2,1,0:T(8,128)(2,1)} %spread.1), calls=%async_computation.3 | async-start | bytes 1048576 | tf_op jit(solution)/shard_map/all_to_all | solution.py:47
  99.3 6.6 %qkv.1 = (bf16[768,256]{1,0:T(8,128)(2,1)}, bf16[768,256]{1,0:T(8,128)(2,1)}, bf16[128,256]{1,0:T(8,128)(2,1)S(1)}, bf16[128,256]{1,0:T(8,128)(2,1)S(1)}) custom-call(s32[4]{0:T(128)S(1)} %pad_add_fusion.place_ref, bf16[4,96,2048]{2,1,0:T(8,128)(2,1)S(1)} %pad_maximum_fusion.own_ref, bf16[4,96,2048]{2,1,0:T(8,128)(2,1)} %collective-permute-done.3.other_ref, ...), custom_call_target="tpu_custom_call" | custom-call | tf_op jit(solution)/shard_map/qkv/pallas_call | solution.py:410
  105.9 2.7 %collective-permute-start.4 = (bf16[128,256]{1,0:T(8,128)(2,1)S(1)}, bf16[128,256]{1,0:T(8,128)(2,1)S(1)}, u32[]{:S(2)}, u32[]{:S(2)}) collective-permute-start(bf16[128,256]{1,0:T(8,128)(2,1)S(1)} %get-tuple-element.12), channel_id=1, source_target_pairs={{0,8},{8,16},{16,24},{24,32},{32,40},{40,48},{48,56},{56,64},{64,7... | collective-permute-start | bytes 196616 | tf_op jit(solution)/shard_map/ppermute | solution.py:429
  108.6 2.6 %collective-permute-start.5 = (bf16[128,256]{1,0:T(8,128)(2,1)S(1)}, bf16[128,256]{1,0:T(8,128)(2,1)S(1)}, u32[]{:S(2)}, u32[]{:S(2)}) collective-permute-start(bf16[128,256]{1,0:T(8,128)(2,1)S(1)} %get-tuple-element.14), channel_id=1, source_target_pairs={{8,0},{16,8},{24,16},{32,24},{40,32},{48,40},{56,48},{64,56},{72,6... | collective-permute-start | bytes 196616 | tf_op jit(solution)/shard_map/ppermute | solution.py:430
  111.3 4.8 %collective-permute-done.5.high_ref = bf16[128,256]{1,0:T(8,128)(2,1)S(1)} collective-permute-done((bf16[128,256]{1,0:T(8,128)(2,1)S(1)}, bf16[128,256]{1,0:T(8,128)(2,1)S(1)}, u32[]{:S(2)}, u32[]{:S(2)}) %collective-permute-start.5) | collective-permute-done | bytes 65568 | tf_op jit(solution)/shard_map/ppermute | solution.py:430
  118.1 5.0 %attention.1 = bf16[768,256]{1,0:T(8,128)(2,1)} custom-call(s32[4]{0:T(128)S(1)} %pad_add_fusion.place_ref, f32[2]{0:T(128)S(1)} %copy-done.4, bf16[768,256]{1,0:T(8,128)(2,1)S(1)} %copy-done.1, bf16[128,256]{1,0:T(8,128)(2,1)S(1)} %collective-permute-done.4.low_ref, bf16[768,256]{1,0:T(8,128)(2,1)S(1)} %copy-done.2, ...), custom_call_target="tpu_custom_call" | custom-call | tf_op jit(solution)/shard_map/attention/pallas_call | solution.py:432
  123.1 3.5 %all-to-all-start.4 = ((bf16[4,192,256]{2,1,0:T(8,128)(2,1)}), bf16[4,192,256]{2,1,0:T(8,128)(2,1)S(1)}, u32[]{:S(2)}, u32[]{:S(2)}) async-start(bf16[4,192,256]{2,1,0:T(8,128)(2,1)} %bitcast.13), calls=%async_computation.4 | async-start | bytes 786432 | tf_op jit(solution)/shard_map/all_to_all | solution.py:47
  128.2 4.6 %all-to-all-done.4.attended_ref = bf16[4,192,256]{2,1,0:T(8,128)(2,1)S(1)} async-done(((bf16[4,192,256]{2,1,0:T(8,128)(2,1)}), bf16[4,192,256]{2,1,0:T(8,128)(2,1)S(1)}, u32[]{:S(2)}, u32[]{:S(2)}) %all-to-all-start.4) | async-done | bytes 393248 | tf_op jit(solution)/shard_map/all_to_all | solution.py:47
  132.8 2.8 %project.1 = (bf16[96,2048]{1,0:T(8,128)(2,1)S(1)}, f32[96,2048]{1,0:T(8,128)S(1)}) custom-call(s32[4]{0:T(128)S(1)} %pad_add_fusion.place_ref, bf16[4,192,256]{2,1,0:T(8,128)(2,1)S(1)} %all-to-all-done.4.attended_ref, bf16[2,256,2048]{2,1,0:T(8,128)(2,1)S(1)} %load.1.early_ref, bf16[256,2048]{1,0:T(8,128)(2,1)} %collective-permute-done.7.w2_ref, ...), custom_call_target="tpu_custom_call" | custom-call | tf_op jit(solution)/shard_map/project/pallas_call | solution.py:455
  135.6 8.0 %collective-permute-start.9 = (bf16[96,2048]{1,0:T(8,128)(2,1)S(1)}, bf16[96,2048]{1,0:T(8,128)(2,1)S(1)}, u32[]{:S(2)}, u32[]{:S(2)}) collective-permute-start(bf16[96,2048]{1,0:T(8,128)(2,1)S(1)} %get-tuple-element.16), channel_id=1, source_target_pairs={{0,1},{1,0},{2,3},{3,2},{4,5},{5,4},{6,7},{7,6},{8,9},{9,8},{10,11... | collective-permute-start | bytes 1179656 | tf_op jit(solution)/shard_map/ppermute | solution.py:315
  (33 shorter events, 11.8 us)
Async XLA Ops:
  0.0 13.3 %collective-permute-start = (bf16[96,2048]{1,0:T(8,128)(2,1)}, bf16[96,2048]{1,0:T(8,128)(2,1)S(1)}, u32[]{:S(2)}, u32[]{:S(2)}) collective-permute-start(bf16[96,2048]{1,0:T(8,128)(2,1)} %latent_ref.1), channel_id=1, source_target_pairs={{0,2},{2,4},{4,6},{6,0},{1,3},{3,5},{5,7},{7,1},{8,10},{10,12},{12... | collective-permute-start | bytes 1179656 | tf_op jit(solution)/shard_map/ppermute | solution.py:310
  3.1 11.8 %collective-permute-start.1 = (bf16[96,2048]{1,0:T(8,128)(2,1)}, bf16[96,2048]{1,0:T(8,128)(2,1)S(1)}, u32[]{:S(2)}, u32[]{:S(2)}) collective-permute-start(bf16[96,2048]{1,0:T(8,128)(2,1)} %latent_ref.1), channel_id=1, source_target_pairs={{0,6},{2,0},{4,2},{6,4},{1,7},{3,1},{5,3},{7,5},{8,14},{10,8},{12,... | collective-permute-start | bytes 1179656 | tf_op jit(solution)/shard_map/ppermute | solution.py:310
  6.5 16.2 %collective-permute-start.2 = (bf16[96,2048]{1,0:T(8,128)(2,1)}, bf16[96,2048]{1,0:T(8,128)(2,1)S(1)}, u32[]{:S(2)}, u32[]{:S(2)}) collective-permute-start(bf16[96,2048]{1,0:T(8,128)(2,1)} %latent_ref.1), channel_id=1, source_target_pairs={{0,4},{2,6},{4,0},{6,2},{1,5},{3,7},{5,1},{7,3},{8,12},{10,14},{12... | collective-permute-start | bytes 1179656 | tf_op jit(solution)/shard_map/ppermute | solution.py:310
  23.9 75.3 %collective-permute-start.3 = (bf16[4,96,2048]{2,1,0:T(8,128)(2,1)S(1)}, bf16[4,96,2048]{2,1,0:T(8,128)(2,1)}, u32[]{:S(2)}, u32[]{:S(2)}) collective-permute-start(bf16[4,96,2048]{2,1,0:T(8,128)(2,1)S(1)} %pad_maximum_fusion.own_ref), channel_id=1, source_target_pairs={{0,1},{1,0},{2,3},{3,2},{4,5},{5,4},{6,7},{7,6},{8,9},{9,8},{10,11... | collective-permute-start | bytes 4718600 | tf_op jit(solution)/shard_map/ppermute | solution.py:315
  56.0 19.5 %all-to-all-start.1 = ((f32[32,1,1280]{2,1,0:T(1,128)}), f32[32,1,1280]{2,1,0:T(1,128)S(1)}, u32[]{:S(2)}, u32[]{:S(2)}) async-start(f32[32,1,1280]{2,1,0:T(1,128)} %sums.1), calls=%async_computation.1 | async-start | bytes 327680 | tf_op jit(solution)/shard_map/all_to_all | solution.py:47
  65.6 61.0 %collective-permute-start.6 = (bf16[256,2048]{1,0:T(8,128)(2,1)}, bf16[256,2048]{1,0:T(8,128)(2,1)}, u32[]{:S(2)}, u32[]{:S(2)}) collective-permute-start(bf16[256,2048]{1,0:T(8,128)(2,1)} %w0_ref.1), channel_id=1, source_target_pairs={{0,2},{2,4},{4,6},{6,0},{1,3},{3,5},{5,7},{7,1},{8,10},{10,12},{12... | collective-permute-start | bytes 3145736 | tf_op jit(solution)/shard_map/ppermute | solution.py:310
  68.7 59.5 %collective-permute-start.7 = (bf16[256,2048]{1,0:T(8,128)(2,1)}, bf16[256,2048]{1,0:T(8,128)(2,1)}, u32[]{:S(2)}, u32[]{:S(2)}) collective-permute-start(bf16[256,2048]{1,0:T(8,128)(2,1)} %w0_ref.1), channel_id=1, source_target_pairs={{0,6},{2,0},{4,2},{6,4},{1,7},{3,1},{5,3},{7,5},{8,14},{10,8},{12,... | collective-permute-start | bytes 3145736 | tf_op jit(solution)/shard_map/ppermute | solution.py:310
  72.1 56.1 %collective-permute-start.8 = (bf16[256,2048]{1,0:T(8,128)(2,1)}, bf16[256,2048]{1,0:T(8,128)(2,1)}, u32[]{:S(2)}, u32[]{:S(2)}) collective-permute-start(bf16[256,2048]{1,0:T(8,128)(2,1)} %w0_ref.1), channel_id=1, source_target_pairs={{0,4},{2,6},{4,0},{6,2},{1,5},{3,7},{5,1},{7,3},{8,12},{10,14},{12... | collective-permute-start | bytes 3145736 | tf_op jit(solution)/shard_map/ppermute | solution.py:310
  78.5 20.7 %copy-start.3 = (f32[2048]{0:T(1024)S(1)}, f32[2048]{0:T(1024)}, u32[]{:S(2)}) copy-start(f32[2048]{0:T(1024)} %param.17) | copy-start | bytes 24580
  78.5 15.4 %all-to-all-start.2 = ((bf16[16,16,256]{2,1,0:T(8,128)(2,1)}), bf16[16,16,256]{2,1,0:T(8,128)(2,1)S(1)}, u32[]{:S(2)}, u32[]{:S(2)}) async-start(bf16[16,16,256]{2,1,0:T(8,128)(2,1)} %context_pairs.1), calls=%async_computation.2 | async-start | bytes 262144 | tf_op jit(solution)/shard_map/all_to_all | solution.py:47
  94.8 16.4 %all-to-all-start.3 = ((bf16[4,256,256]{2,1,0:T(8,128)(2,1)}), bf16[4,256,256]{2,1,0:T(8,128)(2,1)S(1)}, u32[]{:S(2)}, u32[]{:S(2)}) async-start(bf16[4,256,256]{2,1,0:T(8,128)(2,1)} %spread.1), calls=%async_computation.3 | async-start | bytes 1048576 | tf_op jit(solution)/shard_map/all_to_all | solution.py:47
  99.2 16.9 %copy-start.4 = (f32[2]{0:T(128)S(1)}, f32[2]{0:T(128)}, u32[]{:S(2)}) copy-start(f32[2]{0:T(128)} %sink_ref.1) | copy-start | bytes 28
  105.9 5.4 %collective-permute-start.4 = (bf16[128,256]{1,0:T(8,128)(2,1)S(1)}, bf16[128,256]{1,0:T(8,128)(2,1)S(1)}, u32[]{:S(2)}, u32[]{:S(2)}) collective-permute-start(bf16[128,256]{1,0:T(8,128)(2,1)S(1)} %get-tuple-element.12), channel_id=1, source_target_pairs={{0,8},{8,16},{16,24},{24,32},{32,40},{40,48},{48,56},{56,64},{64,7... | collective-permute-start | bytes 196616 | tf_op jit(solution)/shard_map/ppermute | solution.py:429
  108.6 7.5 %collective-permute-start.5 = (bf16[128,256]{1,0:T(8,128)(2,1)S(1)}, bf16[128,256]{1,0:T(8,128)(2,1)S(1)}, u32[]{:S(2)}, u32[]{:S(2)}) collective-permute-start(bf16[128,256]{1,0:T(8,128)(2,1)S(1)} %get-tuple-element.14), channel_id=1, source_target_pairs={{8,0},{16,8},{24,16},{32,24},{40,32},{48,40},{56,48},{64,56},{72,6... | collective-permute-start | bytes 196616 | tf_op jit(solution)/shard_map/ppermute | solution.py:430
  116.1 1.0 copy-start.1
  117.1 1.0 copy-start.2
  123.1 9.7 %all-to-all-start.4 = ((bf16[4,192,256]{2,1,0:T(8,128)(2,1)}), bf16[4,192,256]{2,1,0:T(8,128)(2,1)S(1)}, u32[]{:S(2)}, u32[]{:S(2)}) async-start(bf16[4,192,256]{2,1,0:T(8,128)(2,1)} %bitcast.13), calls=%async_computation.4 | async-start | bytes 786432 | tf_op jit(solution)/shard_map/all_to_all | solution.py:47
  128.2 16.8 %copy-start = (bf16[96,2048]{1,0:T(8,128)(2,1)S(1)}, bf16[96,2048]{1,0:T(8,128)(2,1)}, u32[]{:S(2)}) copy-start(bf16[96,2048]{1,0:T(8,128)(2,1)} %latent_ref.1) | copy-start | bytes 1179652
  135.6 9.3 %collective-permute-start.9 = (bf16[96,2048]{1,0:T(8,128)(2,1)S(1)}, bf16[96,2048]{1,0:T(8,128)(2,1)S(1)}, u32[]{:S(2)}, u32[]{:S(2)}) collective-permute-start(bf16[96,2048]{1,0:T(8,128)(2,1)S(1)} %get-tuple-element.16), channel_id=1, source_target_pairs={{0,1},{1,0},{2,3},{3,2},{4,5},{5,4},{6,7},{7,6},{8,9},{9,8},{10,11... | collective-permute-start | bytes 1179656 | tf_op jit(solution)/shard_map/ppermute | solution.py:315

commit v8 on v7

--- a/solution.py
+++ b/solution.py
@@ -63,7 +63,10 @@
     return jnp.concatenate(pieces, axis=1)
 
 
-def parts_kernel(cond_ref, ctx_cond_ref, shift_ref, scale_ref, gate_ref, out_ref):
+def parts_kernel(
+    cond_ref, ctx_cond_ref, shift_ref, scale_ref, gate_ref, ctx_ref, gain_ref,
+    out_ref, ctx_held_ref, gain_held_ref,
+):
     def active(ref):
         v = ref[...]
         return (v / (1.0 + jnp.exp(-v))).astype(BF16)
@@ -76,6 +79,8 @@
     row = jnp.concatenate([shift[0:1], shift[1:2], scale[0:1], scale[1:2], gate[0:1]], axis=1)
     for i in range(out_ref.shape[0]):
         out_ref[i] = row
+    ctx_held_ref[...] = ctx_ref[...]
+    gain_held_ref[...] = gain_ref[...]
 
 
 def normed_rows(ref, x, start, multiplier, shift):
@@ -101,13 +106,13 @@
 
 def qkv_kernel(
     place_ref, own_ref, other_ref, planes_ref, gain_ref, wq_ref, wk_ref, wv_ref, row_ref, col_ref,
-    q_ref, kv_ref, top_ref, bottom_ref, hidden_ref, wq_held_ref, wkv_ref, sems,
+    q_ref, kv_ref, top_ref, bottom_ref, hidden_ref, wq_held_ref, wkv_ref, halves_ref, sems,
 ):
     columns = wq_ref.shape[1]
     loads = (
         pltpu.make_async_copy(wq_ref, wq_held_ref, sems.at[0]),
-        pltpu.make_async_copy(wk_ref, wkv_ref.at[:, :HEAD_DIM], sems.at[1]),
-        pltpu.make_async_copy(wv_ref, wkv_ref.at[:, HEAD_DIM:], sems.at[2]),
+        pltpu.make_async_copy(wk_ref, halves_ref.at[0], sems.at[1]),
+        pltpu.make_async_copy(wv_ref, halves_ref.at[1], sems.at[2]),
     )
     for load in loads:
         load.start()
@@ -131,6 +136,8 @@
         lax.fori_loop(0, rows // CHUNK, step, 0, unroll=2)
     for load in loads:
         load.wait()
+    wkv_ref[:, :HEAD_DIM] = halves_ref[0]
+    wkv_ref[:, HEAD_DIM:] = halves_ref[1]
     block = 384
     lane = lax.broadcasted_iota(jnp.int32, (GRID_W, HEAD_DIM), 1) < 64
     col = col_ref[...]
@@ -158,24 +165,15 @@
     bottom_ref[...] = kv_ref[hidden_ref.shape[0] - WINDOW_REACH :, :]
 
 
-def context_kernel(
-    ctx_ref, planes_ref, gain_ref, wk_ref, wv_ref, out_ref, wkv_ref, sems
-):
-    loads = (
-        pltpu.make_async_copy(wk_ref, wkv_ref.at[:, :HEAD_DIM], sems.at[0]),
-        pltpu.make_async_copy(wv_ref, wkv_ref.at[:, HEAD_DIM:], sems.at[1]),
-    )
-    for load in loads:
-        load.start()
+def context_kernel(ctx_ref, planes_ref, gain_ref, wk_ref, wv_ref, out_ref):
     columns = planes_ref.shape[2] // 5
     shift = row_vector(planes_ref, 1, columns)
     multiplier = gain_ref[...] * (1.0 + row_vector(planes_ref, 3, columns))
     rows = ctx_ref[...].astype(F32)
     mean = jnp.mean(rows * rows, axis=-1, keepdims=True)
     hidden = (rows * lax.rsqrt(mean + NORM_EPS) * multiplier + shift).astype(BF16)
-    for load in loads:
-        load.wait()
-    pairs = dot(hidden, wkv_ref[...]).astype(BF16)
+    pairs = jnp.concatenate([dot(hidden, wk_ref[...]), dot(hidden, wv_ref[...])], axis=1)
+    pairs = pairs.astype(BF16)
     for p in range(out_ref.shape[0]):
         out_ref[p] = pairs
 
@@ -240,7 +238,7 @@
         attended_ref[pl.ds(at, reach), HEAD_DIM:] = mixed[reach:]
         return carry
 
-    lax.fori_loop(0, blocks, step, 0, unroll=2)
+    lax.fori_loop(0, blocks, step, 0, unroll=True)
 
 
 def load_kernel(w0_ref, w1_ref, out_ref, sems):
@@ -345,16 +343,20 @@
     columns = shift_weight.shape[1]
     place = lax.axis_index(SP)
     gain = norm_gain.reshape(1, width)
-    parts = pl.pallas_call(
+    parts, context, gain = pl.pallas_call(
         parts_kernel,
-        out_shape=shape_of((nz, 1, 5 * columns), F32),
-        in_specs=[VMEM] * 5,
-        out_specs=VMEM,
+        out_shape=[
+            shape_of((nz, 1, 5 * columns), F32),
+            pltpu.VMEM(context.shape, BF16),
+            pltpu.VMEM((1, width), F32),
+        ],
+        in_specs=[VMEM] * 7,
+        out_specs=[VMEM] * 3,
         name="parts",
         compiler_params=vmem(6),
     )(
         *far(condition.reshape(1, -1), context_condition.reshape(1, -1)),
-        *far(shift_weight, scale_weight, gate_weight),
+        *far(shift_weight, scale_weight, gate_weight, context, gain),
     )
     parts = exchanged(parts, "z")
     latent_others = from_other_x(latent)
@@ -385,15 +387,11 @@
     pairs = pl.pallas_call(
         context_kernel,
         out_shape=shape_of((nz, ctx_rows, 2 * HEAD_DIM), BF16),
-        in_specs=[VMEM] * 3 + [HBM] * 2,
+        in_specs=[VMEM] * 5,
         out_specs=VMEM,
-        scratch_shapes=[
-            pltpu.VMEM((width, 2 * HEAD_DIM), BF16),
-            pltpu.SemaphoreType.DMA((2,)),
-        ],
         name="context_pairs",
         compiler_params=vmem(8),
-    )(*far(context), *held(planes), *far(gain, key_matrix, value_matrix))
+    )(*held(context, planes, gain, key_matrix, value_matrix))
     ctx_z = exchanged(pairs, "z").reshape(nz * ctx_rows, 2 * HEAD_DIM)
     spread = pl.pallas_call(
         spread_kernel,
@@ -409,13 +407,14 @@
     edge = (WINDOW_REACH, 2 * HEAD_DIM)
     queries, pairs, top, bottom = pl.pallas_call(
         qkv_kernel,
-        out_shape=[pltpu.HBM(wide, BF16)] * 2 + [pltpu.VMEM(edge, BF16)] * 2,
+        out_shape=[pltpu.VMEM(shape, BF16) for shape in (wide, wide, edge, edge)],
         in_specs=[SMEM] + [VMEM] * 4 + [HBM] * 3 + [VMEM] * 2,
         out_specs=[VMEM] * 4,
         scratch_shapes=[
             pltpu.VMEM((group_rows, width), BF16),
             pltpu.VMEM((width, 2 * HEAD_DIM), BF16),
             pltpu.VMEM((width, 2 * HEAD_DIM), BF16),
+            pltpu.VMEM((2, width, HEAD_DIM), BF16),
             pltpu.SemaphoreType.DMA((3,)),
         ],
         name="qkv",

time: 147 us -> 141 us (0.959)
  Pallas kernels: 22.4 us -> 19.1 us
  local copies, waits for them, and re-layouts: 2.01 us -> 0.02 us
    unnamed x10 -> x8, local copies, waits for them, and re-layouts: 2.01 us -> 0.02 us
    pallas_call x1, Pallas kernels: 2.98 us -> 1.01 us  [shards(): pl.pallas_call(context_kernel, out_shape=shape_of((nz, ctx_rows, 2 * HEAD...]
  transfers between devices with their start and end apart: 14 -> 14, of which waited for: 8 -> 8; matrix products, arithmetic and copies ran while one was open for 0% -> 0% of each run, Pallas kernels for 13% -> 11%
where the time goes in v8:
time: 141 us
  starting transfers between devices  57.7 us (41%)
  waiting for transfers between devices  35.1 us (25%)
  blocking collectives  26.6 us (19%)
  Pallas kernels  19.1 us (14%)
  other arithmetic  1.84 us (1%)
    all_to_all x1, blocking collectives, exchanged(): return lax.all_to_all(blocks, axis, 0, 0, tiled=True)  26.6 us
    all_to_all x4, starting transfers between devices, exchanged(): return lax.all_to_all(blocks, axis, 0, 0, tiled=True)  20.8 us
    ppermute x6, starting transfers between devices, from_other_x(): lax.ppermute(block, 'x', [(i, (i + shift) % 4) for i in range(4)])  19.8 us
    all_to_all x4, waiting for transfers between devices, exchanged(): return lax.all_to_all(blocks, axis, 0, 0, tiled=True)  16.1 us
    ppermute x6, waiting for transfers between devices, from_other_x(): lax.ppermute(block, 'x', [(i, (i + shift) % 4) for i in range(4)])  12.8 us
    ppermute x2, starting transfers between devices, swapped(): return lax.ppermute(x, 'c', [(0, 1), (1, 0)])  11.8 us
    pallas_call x1, Pallas kernels, shards(): pl.pallas_call(qkv_kernel, out_shape=[pltpu.VMEM(shape, BF16) for shape i...  5.77 us
    ppermute x1, waiting for transfers between devices, shards(): high = lax.ppermute(top, SP, [(i + 1, i) for i in range(count - 1)])  4.83 us
  transfers between devices with their start and end apart: 14, of which 8 were waited for; matrix products, arithmetic and copies ran while one was open for 0% of the time, Pallas kernels for 11%

profile of v8, /device:TPU:25, one launch (start us, length us, event | category | flops | bytes accessed | tf_op | source)
XLA Modules:
  0.0 140.7 jit_solution(16615028861038437374)
XLA Ops:
  0.0 3.1 %collective-permute-start = (bf16[96,2048]{1,0:T(8,128)(2,1)}, bf16[96,2048]{1,0:T(8,128)(2,1)S(1)}, u32[]{:S(2)}, u32[]{:S(2)}) collective-permute-start(bf16[96,2048]{1,0:T(8,128)(2,1)} %latent_ref.1), channel_id=1, source_target_pairs={{0,2},{2,4},{4,6},{6,0},{1,3},{3,5},{5,7},{7,1},{8,10},{10,12},{12... | collective-permute-start | bytes 1179656 | tf_op jit(solution)/shard_map/ppermute | solution.py:308
  3.1 3.4 %collective-permute-start.1 = (bf16[96,2048]{1,0:T(8,128)(2,1)}, bf16[96,2048]{1,0:T(8,128)(2,1)S(1)}, u32[]{:S(2)}, u32[]{:S(2)}) collective-permute-start(bf16[96,2048]{1,0:T(8,128)(2,1)} %latent_ref.1), channel_id=1, source_target_pairs={{0,6},{2,0},{4,2},{6,4},{1,7},{3,1},{5,3},{7,5},{8,14},{10,8},{12,... | collective-permute-start | bytes 1179656 | tf_op jit(solution)/shard_map/ppermute | solution.py:308
  6.5 3.4 %collective-permute-start.2 = (bf16[96,2048]{1,0:T(8,128)(2,1)}, bf16[96,2048]{1,0:T(8,128)(2,1)S(1)}, u32[]{:S(2)}, u32[]{:S(2)}) collective-permute-start(bf16[96,2048]{1,0:T(8,128)(2,1)} %latent_ref.1), channel_id=1, source_target_pairs={{0,4},{2,6},{4,0},{6,2},{1,5},{3,7},{5,1},{7,3},{8,12},{10,14},{12... | collective-permute-start | bytes 1179656 | tf_op jit(solution)/shard_map/ppermute | solution.py:308
  10.0 3.4 %collective-permute-done = bf16[96,2048]{1,0:T(8,128)(2,1)S(1)} collective-permute-done((bf16[96,2048]{1,0:T(8,128)(2,1)}, bf16[96,2048]{1,0:T(8,128)(2,1)S(1)}, u32[]{:S(2)}, u32[]{:S(2)}) %collective-permute-start) | collective-permute-done | bytes 393248 | tf_op jit(solution)/shard_map/ppermute | solution.py:308
  13.3 1.6 %collective-permute-done.1 = bf16[96,2048]{1,0:T(8,128)(2,1)S(1)} collective-permute-done((bf16[96,2048]{1,0:T(8,128)(2,1)}, bf16[96,2048]{1,0:T(8,128)(2,1)S(1)}, u32[]{:S(2)}, u32[]{:S(2)}) %collective-permute-start.1) | collective-permute-done | bytes 393248 | tf_op jit(solution)/shard_map/ppermute | solution.py:308
  14.9 7.8 %collective-permute-done.2 = bf16[96,2048]{1,0:T(8,128)(2,1)S(1)} collective-permute-done((bf16[96,2048]{1,0:T(8,128)(2,1)}, bf16[96,2048]{1,0:T(8,128)(2,1)S(1)}, u32[]{:S(2)}, u32[]{:S(2)}) %collective-permute-start.2) | collective-permute-done | bytes 393248 | tf_op jit(solution)/shard_map/ppermute | solution.py:308
  24.0 3.8 %collective-permute-start.3 = (bf16[4,96,2048]{2,1,0:T(8,128)(2,1)S(1)}, bf16[4,96,2048]{2,1,0:T(8,128)(2,1)}, u32[]{:S(2)}, u32[]{:S(2)}) collective-permute-start(bf16[4,96,2048]{2,1,0:T(8,128)(2,1)S(1)} %pad_maximum_fusion.own_ref), channel_id=1, source_target_pairs={{0,1},{1,0},{2,3},{3,2},{4,5},{5,4},{6,7},{7,6},{8,9},{9,8},{10,11... | collective-permute-start | bytes 4718600 | tf_op jit(solution)/shard_map/ppermute | solution.py:313
  28.8 26.6 %all_to_all.25.parts_ref = f32[16,1,1280]{2,1,0:T(1,128)S(1)} all-to-all(f32[16,1,1280]{2,1,0:T(1,128)S(1)} %get-tuple-element.14), channel_id=1, replica_groups=mesh['z'=16,'y'=4,'x'=4,'c'=2] {'z'}, dimensions={0} | all-to-all | bytes 163840 | tf_op jit(solution)/shard_map/all_to_all | solution.py:47
  56.1 9.6 %all-to-all-start.1 = ((f32[32,1,1280]{2,1,0:T(1,128)}), f32[32,1,1280]{2,1,0:T(1,128)S(1)}, u32[]{:S(2)}, u32[]{:S(2)}) async-start(f32[32,1,1280]{2,1,0:T(1,128)} %sums.1), calls=%async_computation.1 | async-start | bytes 327680 | tf_op jit(solution)/shard_map/all_to_all | solution.py:47
  65.8 3.1 %collective-permute-start.6 = (bf16[256,2048]{1,0:T(8,128)(2,1)}, bf16[256,2048]{1,0:T(8,128)(2,1)}, u32[]{:S(2)}, u32[]{:S(2)}) collective-permute-start(bf16[256,2048]{1,0:T(8,128)(2,1)} %w0_ref.1), channel_id=1, source_target_pairs={{0,2},{2,4},{4,6},{6,0},{1,3},{3,5},{5,7},{7,1},{8,10},{10,12},{12... | collective-permute-start | bytes 3145736 | tf_op jit(solution)/shard_map/ppermute | solution.py:308
  68.9 3.4 %collective-permute-start.7 = (bf16[256,2048]{1,0:T(8,128)(2,1)}, bf16[256,2048]{1,0:T(8,128)(2,1)}, u32[]{:S(2)}, u32[]{:S(2)}) collective-permute-start(bf16[256,2048]{1,0:T(8,128)(2,1)} %w0_ref.1), channel_id=1, source_target_pairs={{0,6},{2,0},{4,2},{6,4},{1,7},{3,1},{5,3},{7,5},{8,14},{10,8},{12,... | collective-permute-start | bytes 3145736 | tf_op jit(solution)/shard_map/ppermute | solution.py:308
  72.3 3.4 %collective-permute-start.8 = (bf16[256,2048]{1,0:T(8,128)(2,1)}, bf16[256,2048]{1,0:T(8,128)(2,1)}, u32[]{:S(2)}, u32[]{:S(2)}) collective-permute-start(bf16[256,2048]{1,0:T(8,128)(2,1)} %w0_ref.1), channel_id=1, source_target_pairs={{0,4},{2,6},{4,0},{6,2},{1,5},{3,7},{5,1},{7,3},{8,12},{10,14},{12... | collective-permute-start | bytes 3145736 | tf_op jit(solution)/shard_map/ppermute | solution.py:308
  76.7 3.5 %all-to-all-start.2 = ((bf16[16,16,256]{2,1,0:T(8,128)(2,1)}), bf16[16,16,256]{2,1,0:T(8,128)(2,1)S(1)}, u32[]{:S(2)}, u32[]{:S(2)}) async-start(bf16[16,16,256]{2,1,0:T(8,128)(2,1)} %context_pairs.1), calls=%async_computation.2 | async-start | bytes 262144 | tf_op jit(solution)/shard_map/all_to_all | solution.py:47
  80.6 11.5 %all-to-all-done.2 = bf16[16,16,256]{2,1,0:T(8,128)(2,1)S(1)} async-done(((bf16[16,16,256]{2,1,0:T(8,128)(2,1)}), bf16[16,16,256]{2,1,0:T(8,128)(2,1)S(1)}, u32[]{:S(2)}, u32[]{:S(2)}) %all-to-all-start.2) | async-done | bytes 131104 | tf_op jit(solution)/shard_map/all_to_all | solution.py:47
  93.0 4.2 %all-to-all-start.3 = ((bf16[4,256,256]{2,1,0:T(8,128)(2,1)}), bf16[4,256,256]{2,1,0:T(8,128)(2,1)S(1)}, u32[]{:S(2)}, u32[]{:S(2)}) async-start(bf16[4,256,256]{2,1,0:T(8,128)(2,1)} %spread.1), calls=%async_computation.3 | async-start | bytes 1048576 | tf_op jit(solution)/shard_map/all_to_all | solution.py:47
  97.5 5.8 %qkv.1 = (bf16[768,256]{1,0:T(8,128)(2,1)S(1)}, bf16[768,256]{1,0:T(8,128)(2,1)S(1)}, bf16[128,256]{1,0:T(8,128)(2,1)S(1)}, bf16[128,256]{1,0:T(8,128)(2,1)S(1)}) custom-call(s32[4]{0:T(128)S(1)} %pad_add_fusion.place_ref, bf16[4,96,2048]{2,1,0:T(8,128)(2,1)S(1)} %pad_maximum_fusion.own_ref, bf16[4,96,2048]{2,1,0:T(8,128)(2,1)} %collective-permute-done.3.other_ref, ...), custom_call_target="tpu_custom_call" | custom-call | tf_op jit(solution)/shard_map/qkv/pallas_call | solution.py:408
  103.2 2.7 %collective-permute-start.4 = (bf16[128,256]{1,0:T(8,128)(2,1)S(1)}, bf16[128,256]{1,0:T(8,128)(2,1)S(1)}, u32[]{:S(2)}, u32[]{:S(2)}) collective-permute-start(bf16[128,256]{1,0:T(8,128)(2,1)S(1)} %get-tuple-element.17), channel_id=1, source_target_pairs={{0,8},{8,16},{16,24},{24,32},{32,40},{40,48},{48,56},{56,64},{64,7... | collective-permute-start | bytes 196616 | tf_op jit(solution)/shard_map/ppermute | solution.py:428
  106.0 2.6 %collective-permute-start.5 = (bf16[128,256]{1,0:T(8,128)(2,1)S(1)}, bf16[128,256]{1,0:T(8,128)(2,1)S(1)}, u32[]{:S(2)}, u32[]{:S(2)}) collective-permute-start(bf16[128,256]{1,0:T(8,128)(2,1)S(1)} %get-tuple-element.19), channel_id=1, source_target_pairs={{8,0},{16,8},{24,16},{32,24},{40,32},{48,40},{56,48},{64,56},{72,6... | collective-permute-start | bytes 196616 | tf_op jit(solution)/shard_map/ppermute | solution.py:429
  108.6 4.8 %collective-permute-done.5.high_ref = bf16[128,256]{1,0:T(8,128)(2,1)S(1)} collective-permute-done((bf16[128,256]{1,0:T(8,128)(2,1)S(1)}, bf16[128,256]{1,0:T(8,128)(2,1)S(1)}, u32[]{:S(2)}, u32[]{:S(2)}) %collective-permute-start.5) | collective-permute-done | bytes 65568 | tf_op jit(solution)/shard_map/ppermute | solution.py:429
  113.5 4.5 %attention.1 = bf16[768,256]{1,0:T(8,128)(2,1)} custom-call(s32[4]{0:T(128)S(1)} %pad_add_fusion.place_ref, f32[2]{0:T(128)S(1)} %copy-done.3, bf16[768,256]{1,0:T(8,128)(2,1)S(1)} %get-tuple-element.16.q_ref, bf16[128,256]{1,0:T(8,128)(2,1)S(1)} %collective-permute-done.4.low_ref, bf16[768,256]{1,0:T(8,128)(2,1)S(1)} %get-tuple-element.18.kv_ref, ...), custom_call_target="tpu_custom_call" | custom-call | tf_op jit(solution)/shard_map/attention/pallas_call | solution.py:431
  117.9 3.5 %all-to-all-start.4 = ((bf16[4,192,256]{2,1,0:T(8,128)(2,1)}), bf16[4,192,256]{2,1,0:T(8,128)(2,1)S(1)}, u32[]{:S(2)}, u32[]{:S(2)}) async-start(bf16[4,192,256]{2,1,0:T(8,128)(2,1)} %bitcast.13), calls=%async_computation.4 | async-start | bytes 786432 | tf_op jit(solution)/shard_map/all_to_all | solution.py:47
  123.0 4.6 %all-to-all-done.4.attended_ref = bf16[4,192,256]{2,1,0:T(8,128)(2,1)S(1)} async-done(((bf16[4,192,256]{2,1,0:T(8,128)(2,1)}), bf16[4,192,256]{2,1,0:T(8,128)(2,1)S(1)}, u32[]{:S(2)}, u32[]{:S(2)}) %all-to-all-start.4) | async-done | bytes 393248 | tf_op jit(solution)/shard_map/all_to_all | solution.py:47
  127.6 2.8 %project.1 = (bf16[96,2048]{1,0:T(8,128)(2,1)S(1)}, f32[96,2048]{1,0:T(8,128)S(1)}) custom-call(s32[4]{0:T(128)S(1)} %pad_add_fusion.place_ref, bf16[4,192,256]{2,1,0:T(8,128)(2,1)S(1)} %all-to-all-done.4.attended_ref, bf16[2,256,2048]{2,1,0:T(8,128)(2,1)S(1)} %load.1.early_ref, bf16[256,2048]{1,0:T(8,128)(2,1)} %collective-permute-done.7.w2_ref, ...), custom_call_target="tpu_custom_call" | custom-call | tf_op jit(solution)/shard_map/project/pallas_call | solution.py:454
  130.4 8.0 %collective-permute-start.9 = (bf16[96,2048]{1,0:T(8,128)(2,1)S(1)}, bf16[96,2048]{1,0:T(8,128)(2,1)S(1)}, u32[]{:S(2)}, u32[]{:S(2)}) collective-permute-start(bf16[96,2048]{1,0:T(8,128)(2,1)S(1)} %get-tuple-element.22), channel_id=1, source_target_pairs={{0,1},{1,0},{2,3},{3,2},{4,5},{5,4},{6,7},{7,6},{8,9},{9,8},{10,11... | collective-permute-start | bytes 1179656 | tf_op jit(solution)/shard_map/ppermute | solution.py:313
  (31 shorter events, 9.4 us)
Async XLA Ops:
  0.0 13.3 %collective-permute-start = (bf16[96,2048]{1,0:T(8,128)(2,1)}, bf16[96,2048]{1,0:T(8,128)(2,1)S(1)}, u32[]{:S(2)}, u32[]{:S(2)}) collective-permute-start(bf16[96,2048]{1,0:T(8,128)(2,1)} %latent_ref.1), channel_id=1, source_target_pairs={{0,2},{2,4},{4,6},{6,0},{1,3},{3,5},{5,7},{7,1},{8,10},{10,12},{12... | collective-permute-start | bytes 1179656 | tf_op jit(solution)/shard_map/ppermute | solution.py:308
  3.1 11.8 %collective-permute-start.1 = (bf16[96,2048]{1,0:T(8,128)(2,1)}, bf16[96,2048]{1,0:T(8,128)(2,1)S(1)}, u32[]{:S(2)}, u32[]{:S(2)}) collective-permute-start(bf16[96,2048]{1,0:T(8,128)(2,1)} %latent_ref.1), channel_id=1, source_target_pairs={{0,6},{2,0},{4,2},{6,4},{1,7},{3,1},{5,3},{7,5},{8,14},{10,8},{12,... | collective-permute-start | bytes 1179656 | tf_op jit(solution)/shard_map/ppermute | solution.py:308
  6.5 16.2 %collective-permute-start.2 = (bf16[96,2048]{1,0:T(8,128)(2,1)}, bf16[96,2048]{1,0:T(8,128)(2,1)S(1)}, u32[]{:S(2)}, u32[]{:S(2)}) collective-permute-start(bf16[96,2048]{1,0:T(8,128)(2,1)} %latent_ref.1), channel_id=1, source_target_pairs={{0,4},{2,6},{4,0},{6,2},{1,5},{3,7},{5,1},{7,3},{8,12},{10,14},{12... | collective-permute-start | bytes 1179656 | tf_op jit(solution)/shard_map/ppermute | solution.py:308
  22.7 53.0 %copy-start = (bf16[2048,128]{1,0:T(8,128)(2,1)S(1)}, bf16[2048,128]{1,0:T(8,128)(2,1)}, u32[]{:S(2)}) copy-start(bf16[2048,128]{1,0:T(8,128)(2,1)} %wk_ref.3) | copy-start | bytes 1572868
  22.7 53.0 %copy-start.1 = (bf16[2048,128]{1,0:T(8,128)(2,1)S(1)}, bf16[2048,128]{1,0:T(8,128)(2,1)}, u32[]{:S(2)}) copy-start(bf16[2048,128]{1,0:T(8,128)(2,1)} %wv_ref.3) | copy-start | bytes 1572868
  24.0 73.4 %collective-permute-start.3 = (bf16[4,96,2048]{2,1,0:T(8,128)(2,1)S(1)}, bf16[4,96,2048]{2,1,0:T(8,128)(2,1)}, u32[]{:S(2)}, u32[]{:S(2)}) collective-permute-start(bf16[4,96,2048]{2,1,0:T(8,128)(2,1)S(1)} %pad_maximum_fusion.own_ref), channel_id=1, source_target_pairs={{0,1},{1,0},{2,3},{3,2},{4,5},{5,4},{6,7},{7,6},{8,9},{9,8},{10,11... | collective-permute-start | bytes 4718600 | tf_op jit(solution)/shard_map/ppermute | solution.py:313
  56.1 19.5 %all-to-all-start.1 = ((f32[32,1,1280]{2,1,0:T(1,128)}), f32[32,1,1280]{2,1,0:T(1,128)S(1)}, u32[]{:S(2)}, u32[]{:S(2)}) async-start(f32[32,1,1280]{2,1,0:T(1,128)} %sums.1), calls=%async_computation.1 | async-start | bytes 327680 | tf_op jit(solution)/shard_map/all_to_all | solution.py:47
  65.8 55.7 %collective-permute-start.6 = (bf16[256,2048]{1,0:T(8,128)(2,1)}, bf16[256,2048]{1,0:T(8,128)(2,1)}, u32[]{:S(2)}, u32[]{:S(2)}) collective-permute-start(bf16[256,2048]{1,0:T(8,128)(2,1)} %w0_ref.1), channel_id=1, source_target_pairs={{0,2},{2,4},{4,6},{6,0},{1,3},{3,5},{5,7},{7,1},{8,10},{10,12},{12... | collective-permute-start | bytes 3145736 | tf_op jit(solution)/shard_map/ppermute | solution.py:308
  68.9 54.1 %collective-permute-start.7 = (bf16[256,2048]{1,0:T(8,128)(2,1)}, bf16[256,2048]{1,0:T(8,128)(2,1)}, u32[]{:S(2)}, u32[]{:S(2)}) collective-permute-start(bf16[256,2048]{1,0:T(8,128)(2,1)} %w0_ref.1), channel_id=1, source_target_pairs={{0,6},{2,0},{4,2},{6,4},{1,7},{3,1},{5,3},{7,5},{8,14},{10,8},{12,... | collective-permute-start | bytes 3145736 | tf_op jit(solution)/shard_map/ppermute | solution.py:308
  72.3 50.7 %collective-permute-start.8 = (bf16[256,2048]{1,0:T(8,128)(2,1)}, bf16[256,2048]{1,0:T(8,128)(2,1)}, u32[]{:S(2)}, u32[]{:S(2)}) collective-permute-start(bf16[256,2048]{1,0:T(8,128)(2,1)} %w0_ref.1), channel_id=1, source_target_pairs={{0,4},{2,6},{4,0},{6,2},{1,5},{3,7},{5,1},{7,3},{8,12},{10,14},{12... | collective-permute-start | bytes 3145736 | tf_op jit(solution)/shard_map/ppermute | solution.py:308
  76.7 15.4 %all-to-all-start.2 = ((bf16[16,16,256]{2,1,0:T(8,128)(2,1)}), bf16[16,16,256]{2,1,0:T(8,128)(2,1)S(1)}, u32[]{:S(2)}, u32[]{:S(2)}) async-start(bf16[16,16,256]{2,1,0:T(8,128)(2,1)} %context_pairs.1), calls=%async_computation.2 | async-start | bytes 262144 | tf_op jit(solution)/shard_map/all_to_all | solution.py:47
  93.0 15.6 %all-to-all-start.3 = ((bf16[4,256,256]{2,1,0:T(8,128)(2,1)}), bf16[4,256,256]{2,1,0:T(8,128)(2,1)S(1)}, u32[]{:S(2)}, u32[]{:S(2)}) async-start(bf16[4,256,256]{2,1,0:T(8,128)(2,1)} %spread.1), calls=%async_computation.3 | async-start | bytes 1048576 | tf_op jit(solution)/shard_map/all_to_all | solution.py:47
  97.4 16.0 %copy-start.3 = (f32[2]{0:T(128)S(1)}, f32[2]{0:T(128)}, u32[]{:S(2)}) copy-start(f32[2]{0:T(128)} %sink_ref.1) | copy-start | bytes 28
  103.2 5.4 %collective-permute-start.4 = (bf16[128,256]{1,0:T(8,128)(2,1)S(1)}, bf16[128,256]{1,0:T(8,128)(2,1)S(1)}, u32[]{:S(2)}, u32[]{:S(2)}) collective-permute-start(bf16[128,256]{1,0:T(8,128)(2,1)S(1)} %get-tuple-element.17), channel_id=1, source_target_pairs={{0,8},{8,16},{16,24},{24,32},{32,40},{40,48},{48,56},{56,64},{64,7... | collective-permute-start | bytes 196616 | tf_op jit(solution)/shard_map/ppermute | solution.py:428
  106.0 7.5 %collective-permute-start.5 = (bf16[128,256]{1,0:T(8,128)(2,1)S(1)}, bf16[128,256]{1,0:T(8,128)(2,1)S(1)}, u32[]{:S(2)}, u32[]{:S(2)}) collective-permute-start(bf16[128,256]{1,0:T(8,128)(2,1)S(1)} %get-tuple-element.19), channel_id=1, source_target_pairs={{8,0},{16,8},{24,16},{32,24},{40,32},{48,40},{56,48},{64,56},{72,6... | collective-permute-start | bytes 196616 | tf_op jit(solution)/shard_map/ppermute | solution.py:429
  117.9 9.7 %all-to-all-start.4 = ((bf16[4,192,256]{2,1,0:T(8,128)(2,1)}), bf16[4,192,256]{2,1,0:T(8,128)(2,1)S(1)}, u32[]{:S(2)}, u32[]{:S(2)}) async-start(bf16[4,192,256]{2,1,0:T(8,128)(2,1)} %bitcast.13), calls=%async_computation.4 | async-start | bytes 786432 | tf_op jit(solution)/shard_map/all_to_all | solution.py:47
  123.0 16.8 %copy-start.2 = (bf16[96,2048]{1,0:T(8,128)(2,1)S(1)}, bf16[96,2048]{1,0:T(8,128)(2,1)}, u32[]{:S(2)}) copy-start(bf16[96,2048]{1,0:T(8,128)(2,1)} %latent_ref.1) | copy-start | bytes 1179652
  130.4 9.3 %collective-permute-start.9 = (bf16[96,2048]{1,0:T(8,128)(2,1)S(1)}, bf16[96,2048]{1,0:T(8,128)(2,1)S(1)}, u32[]{:S(2)}, u32[]{:S(2)}) collective-permute-start(bf16[96,2048]{1,0:T(8,128)(2,1)S(1)} %get-tuple-element.22), channel_id=1, source_target_pairs={{0,1},{1,0},{2,3},{3,2},{4,5},{5,4},{6,7},{7,6},{8,9},{9,8},{10,11... | collective-permute-start | bytes 1179656 | tf_op jit(solution)/shard_map/ppermute | solution.py:313

commit v9 on v8

--- a/solution.py
+++ b/solution.py
@@ -77,6 +77,8 @@
     scale = dot(both, scale_ref[...])
     gate = dot(both, gate_ref[...])
     row = jnp.concatenate([shift[0:1], shift[1:2], scale[0:1], scale[1:2], gate[0:1]], axis=1)
+    half = out_ref.shape[2]
+    row = jnp.concatenate([row[:, :half], row[:, half:]], axis=0).astype(BF16)
     for i in range(out_ref.shape[0]):
         out_ref[i] = row
     ctx_held_ref[...] = ctx_ref[...]
@@ -97,9 +99,10 @@
 
 
 def sum_kernel(parts_ref, out_ref):
-    total = parts_ref[0]
+    total = parts_ref[0].astype(F32)
     for z in range(1, parts_ref.shape[0]):
-        total = total + parts_ref[z]
+        total = total + parts_ref[z].astype(F32)
+    total = jnp.concatenate([total[0:1], total[1:2]], axis=1)
     for p in range(out_ref.shape[0]):
         out_ref[p] = total
 
@@ -346,7 +349,7 @@
     parts, context, gain = pl.pallas_call(
         parts_kernel,
         out_shape=[
-            shape_of((nz, 1, 5 * columns), F32),
+            shape_of((nz, 2, 5 * columns // 2), BF16),
             pltpu.VMEM(context.shape, BF16),
             pltpu.VMEM((1, width), F32),
         ],

time: 141 us -> 141 us (level)
  no operation moved by 1% of the time
where the time goes in v9:
time: 141 us; the launch traced here: 140 us
  starting transfers between devices  57.2 us (41%)
  waiting for transfers between devices  35.1 us (25%)
  blocking collectives  26.3 us (19%)
  Pallas kernels  19.1 us (14%)
  other arithmetic  1.84 us (1%)
    all_to_all x1, blocking collectives, exchanged(): return lax.all_to_all(blocks, axis, 0, 0, tiled=True)  26.3 us
    all_to_all x4, starting transfers between devices, exchanged(): return lax.all_to_all(blocks, axis, 0, 0, tiled=True)  20.3 us
    ppermute x6, starting transfers between devices, from_other_x(): lax.ppermute(block, 'x', [(i, (i + shift) % 4) for i in range(4)])  19.8 us
    all_to_all x4, waiting for transfers between devices, exchanged(): return lax.all_to_all(blocks, axis, 0, 0, tiled=True)  16.1 us
    ppermute x6, waiting for transfers between devices, from_other_x(): lax.ppermute(block, 'x', [(i, (i + shift) % 4) for i in range(4)])  12.8 us
    ppermute x2, starting transfers between devices, swapped(): return lax.ppermute(x, 'c', [(0, 1), (1, 0)])  11.8 us
    pallas_call x1, Pallas kernels, shards(): pl.pallas_call(qkv_kernel, out_shape=[pltpu.VMEM(shape, BF16) for shape i...  5.77 us
    ppermute x1, waiting for transfers between devices, shards(): high = lax.ppermute(top, SP, [(i + 1, i) for i in range(count - 1)])  4.83 us
  transfers between devices with their start and end apart: 14, of which 8 were waited for; matrix products, arithmetic and copies ran while one was open for 0% of the time, Pallas kernels for 11%

profile of v9, /device:TPU:25, one launch (start us, length us, event | category | flops | bytes accessed | tf_op | source)
XLA Modules:
  0.0 139.8 jit_solution(5404549811264161813)
XLA Ops:
  0.0 3.1 %collective-permute-start = (bf16[96,2048]{1,0:T(8,128)(2,1)}, bf16[96,2048]{1,0:T(8,128)(2,1)S(1)}, u32[]{:S(2)}, u32[]{:S(2)}) collective-permute-start(bf16[96,2048]{1,0:T(8,128)(2,1)} %latent_ref.1), channel_id=1, source_target_pairs={{0,2},{2,4},{4,6},{6,0},{1,3},{3,5},{5,7},{7,1},{8,10},{10,12},{12... | collective-permute-start | bytes 1179656 | tf_op jit(solution)/shard_map/ppermute | solution.py:311
  3.1 3.4 %collective-permute-start.1 = (bf16[96,2048]{1,0:T(8,128)(2,1)}, bf16[96,2048]{1,0:T(8,128)(2,1)S(1)}, u32[]{:S(2)}, u32[]{:S(2)}) collective-permute-start(bf16[96,2048]{1,0:T(8,128)(2,1)} %latent_ref.1), channel_id=1, source_target_pairs={{0,6},{2,0},{4,2},{6,4},{1,7},{3,1},{5,3},{7,5},{8,14},{10,8},{12,... | collective-permute-start | bytes 1179656 | tf_op jit(solution)/shard_map/ppermute | solution.py:311
  6.5 3.4 %collective-permute-start.2 = (bf16[96,2048]{1,0:T(8,128)(2,1)}, bf16[96,2048]{1,0:T(8,128)(2,1)S(1)}, u32[]{:S(2)}, u32[]{:S(2)}) collective-permute-start(bf16[96,2048]{1,0:T(8,128)(2,1)} %latent_ref.1), channel_id=1, source_target_pairs={{0,4},{2,6},{4,0},{6,2},{1,5},{3,7},{5,1},{7,3},{8,12},{10,14},{12... | collective-permute-start | bytes 1179656 | tf_op jit(solution)/shard_map/ppermute | solution.py:311
  10.0 3.4 %collective-permute-done = bf16[96,2048]{1,0:T(8,128)(2,1)S(1)} collective-permute-done((bf16[96,2048]{1,0:T(8,128)(2,1)}, bf16[96,2048]{1,0:T(8,128)(2,1)S(1)}, u32[]{:S(2)}, u32[]{:S(2)}) %collective-permute-start) | collective-permute-done | bytes 393248 | tf_op jit(solution)/shard_map/ppermute | solution.py:311
  13.3 1.6 %collective-permute-done.1 = bf16[96,2048]{1,0:T(8,128)(2,1)S(1)} collective-permute-done((bf16[96,2048]{1,0:T(8,128)(2,1)}, bf16[96,2048]{1,0:T(8,128)(2,1)S(1)}, u32[]{:S(2)}, u32[]{:S(2)}) %collective-permute-start.1) | collective-permute-done | bytes 393248 | tf_op jit(solution)/shard_map/ppermute | solution.py:311
  14.9 7.8 %collective-permute-done.2 = bf16[96,2048]{1,0:T(8,128)(2,1)S(1)} collective-permute-done((bf16[96,2048]{1,0:T(8,128)(2,1)}, bf16[96,2048]{1,0:T(8,128)(2,1)S(1)}, u32[]{:S(2)}, u32[]{:S(2)}) %collective-permute-start.2) | collective-permute-done | bytes 393248 | tf_op jit(solution)/shard_map/ppermute | solution.py:311
  24.0 3.8 %collective-permute-start.3 = (bf16[4,96,2048]{2,1,0:T(8,128)(2,1)S(1)}, bf16[4,96,2048]{2,1,0:T(8,128)(2,1)}, u32[]{:S(2)}, u32[]{:S(2)}) collective-permute-start(bf16[4,96,2048]{2,1,0:T(8,128)(2,1)S(1)} %pad_maximum_fusion.own_ref), channel_id=1, source_target_pairs={{0,1},{1,0},{2,3},{3,2},{4,5},{5,4},{6,7},{7,6},{8,9},{9,8},{10,11... | collective-permute-start | bytes 4718600 | tf_op jit(solution)/shard_map/ppermute | solution.py:316
  28.8 26.3 %all_to_all.25.parts_ref = bf16[16,2,640]{2,1,0:T(2,128)(2,1)S(1)} all-to-all(bf16[16,2,640]{2,1,0:T(2,128)(2,1)S(1)} %get-tuple-element.14), channel_id=1, replica_groups=mesh['z'=16,'y'=4,'x'=4,'c'=2] {'z'}, dimensions={0} | all-to-all | bytes 81920 | tf_op jit(solution)/shard_map/all_to_all | solution.py:47
  55.8 9.1 %all-to-all-start.1 = ((f32[32,1,1280]{2,1,0:T(1,128)}), f32[32,1,1280]{2,1,0:T(1,128)S(1)}, u32[]{:S(2)}, u32[]{:S(2)}) async-start(f32[32,1,1280]{2,1,0:T(1,128)} %sums.1), calls=%async_computation.1 | async-start | bytes 327680 | tf_op jit(solution)/shard_map/all_to_all | solution.py:47
  64.9 3.1 %collective-permute-start.6 = (bf16[256,2048]{1,0:T(8,128)(2,1)}, bf16[256,2048]{1,0:T(8,128)(2,1)}, u32[]{:S(2)}, u32[]{:S(2)}) collective-permute-start(bf16[256,2048]{1,0:T(8,128)(2,1)} %w0_ref.1), channel_id=1, source_target_pairs={{0,2},{2,4},{4,6},{6,0},{1,3},{3,5},{5,7},{7,1},{8,10},{10,12},{12... | collective-permute-start | bytes 3145736 | tf_op jit(solution)/shard_map/ppermute | solution.py:311
  68.0 3.4 %collective-permute-start.7 = (bf16[256,2048]{1,0:T(8,128)(2,1)}, bf16[256,2048]{1,0:T(8,128)(2,1)}, u32[]{:S(2)}, u32[]{:S(2)}) collective-permute-start(bf16[256,2048]{1,0:T(8,128)(2,1)} %w0_ref.1), channel_id=1, source_target_pairs={{0,6},{2,0},{4,2},{6,4},{1,7},{3,1},{5,3},{7,5},{8,14},{10,8},{12,... | collective-permute-start | bytes 3145736 | tf_op jit(solution)/shard_map/ppermute | solution.py:311
  71.4 3.4 %collective-permute-start.8 = (bf16[256,2048]{1,0:T(8,128)(2,1)}, bf16[256,2048]{1,0:T(8,128)(2,1)}, u32[]{:S(2)}, u32[]{:S(2)}) collective-permute-start(bf16[256,2048]{1,0:T(8,128)(2,1)} %w0_ref.1), channel_id=1, source_target_pairs={{0,4},{2,6},{4,0},{6,2},{1,5},{3,7},{5,1},{7,3},{8,12},{10,14},{12... | collective-permute-start | bytes 3145736 | tf_op jit(solution)/shard_map/ppermute | solution.py:311
  75.9 3.5 %all-to-all-start.2 = ((bf16[16,16,256]{2,1,0:T(8,128)(2,1)}), bf16[16,16,256]{2,1,0:T(8,128)(2,1)S(1)}, u32[]{:S(2)}, u32[]{:S(2)}) async-start(bf16[16,16,256]{2,1,0:T(8,128)(2,1)} %context_pairs.1), calls=%async_computation.2 | async-start | bytes 262144 | tf_op jit(solution)/shard_map/all_to_all | solution.py:47
  79.8 11.5 %all-to-all-done.2 = bf16[16,16,256]{2,1,0:T(8,128)(2,1)S(1)} async-done(((bf16[16,16,256]{2,1,0:T(8,128)(2,1)}), bf16[16,16,256]{2,1,0:T(8,128)(2,1)S(1)}, u32[]{:S(2)}, u32[]{:S(2)}) %all-to-all-start.2) | async-done | bytes 131104 | tf_op jit(solution)/shard_map/all_to_all | solution.py:47
  92.1 4.2 %all-to-all-start.3 = ((bf16[4,256,256]{2,1,0:T(8,128)(2,1)}), bf16[4,256,256]{2,1,0:T(8,128)(2,1)S(1)}, u32[]{:S(2)}, u32[]{:S(2)}) async-start(bf16[4,256,256]{2,1,0:T(8,128)(2,1)} %spread.1), calls=%async_computation.3 | async-start | bytes 1048576 | tf_op jit(solution)/shard_map/all_to_all | solution.py:47
  96.6 5.8 %qkv.1 = (bf16[768,256]{1,0:T(8,128)(2,1)S(1)}, bf16[768,256]{1,0:T(8,128)(2,1)S(1)}, bf16[128,256]{1,0:T(8,128)(2,1)S(1)}, bf16[128,256]{1,0:T(8,128)(2,1)S(1)}) custom-call(s32[4]{0:T(128)S(1)} %pad_add_fusion.place_ref, bf16[4,96,2048]{2,1,0:T(8,128)(2,1)S(1)} %pad_maximum_fusion.own_ref, bf16[4,96,2048]{2,1,0:T(8,128)(2,1)} %collective-permute-done.3.other_ref, ...), custom_call_target="tpu_custom_call" | custom-call | tf_op jit(solution)/shard_map/qkv/pallas_call | solution.py:411
  102.4 2.7 %collective-permute-start.4 = (bf16[128,256]{1,0:T(8,128)(2,1)S(1)}, bf16[128,256]{1,0:T(8,128)(2,1)S(1)}, u32[]{:S(2)}, u32[]{:S(2)}) collective-permute-start(bf16[128,256]{1,0:T(8,128)(2,1)S(1)} %get-tuple-element.17), channel_id=1, source_target_pairs={{0,8},{8,16},{16,24},{24,32},{32,40},{40,48},{48,56},{56,64},{64,7... | collective-permute-start | bytes 196616 | tf_op jit(solution)/shard_map/ppermute | solution.py:431
  105.1 2.6 %collective-permute-start.5 = (bf16[128,256]{1,0:T(8,128)(2,1)S(1)}, bf16[128,256]{1,0:T(8,128)(2,1)S(1)}, u32[]{:S(2)}, u32[]{:S(2)}) collective-permute-start(bf16[128,256]{1,0:T(8,128)(2,1)S(1)} %get-tuple-element.19), channel_id=1, source_target_pairs={{8,0},{16,8},{24,16},{32,24},{40,32},{48,40},{56,48},{64,56},{72,6... | collective-permute-start | bytes 196616 | tf_op jit(solution)/shard_map/ppermute | solution.py:432
  107.8 4.8 %collective-permute-done.5.high_ref = bf16[128,256]{1,0:T(8,128)(2,1)S(1)} collective-permute-done((bf16[128,256]{1,0:T(8,128)(2,1)S(1)}, bf16[128,256]{1,0:T(8,128)(2,1)S(1)}, u32[]{:S(2)}, u32[]{:S(2)}) %collective-permute-start.5) | collective-permute-done | bytes 65568 | tf_op jit(solution)/shard_map/ppermute | solution.py:432
  112.6 4.5 %attention.1 = bf16[768,256]{1,0:T(8,128)(2,1)} custom-call(s32[4]{0:T(128)S(1)} %pad_add_fusion.place_ref, f32[2]{0:T(128)S(1)} %copy-done.3, bf16[768,256]{1,0:T(8,128)(2,1)S(1)} %get-tuple-element.16.q_ref, bf16[128,256]{1,0:T(8,128)(2,1)S(1)} %collective-permute-done.4.low_ref, bf16[768,256]{1,0:T(8,128)(2,1)S(1)} %get-tuple-element.18.kv_ref, ...), custom_call_target="tpu_custom_call" | custom-call | tf_op jit(solution)/shard_map/attention/pallas_call | solution.py:434
  117.1 3.5 %all-to-all-start.4 = ((bf16[4,192,256]{2,1,0:T(8,128)(2,1)}), bf16[4,192,256]{2,1,0:T(8,128)(2,1)S(1)}, u32[]{:S(2)}, u32[]{:S(2)}) async-start(bf16[4,192,256]{2,1,0:T(8,128)(2,1)} %bitcast.13), calls=%async_computation.4 | async-start | bytes 786432 | tf_op jit(solution)/shard_map/all_to_all | solution.py:47
  122.2 4.6 %all-to-all-done.4.attended_ref = bf16[4,192,256]{2,1,0:T(8,128)(2,1)S(1)} async-done(((bf16[4,192,256]{2,1,0:T(8,128)(2,1)}), bf16[4,192,256]{2,1,0:T(8,128)(2,1)S(1)}, u32[]{:S(2)}, u32[]{:S(2)}) %all-to-all-start.4) | async-done | bytes 393248 | tf_op jit(solution)/shard_map/all_to_all | solution.py:47
  126.7 2.8 %project.1 = (bf16[96,2048]{1,0:T(8,128)(2,1)S(1)}, f32[96,2048]{1,0:T(8,128)S(1)}) custom-call(s32[4]{0:T(128)S(1)} %pad_add_fusion.place_ref, bf16[4,192,256]{2,1,0:T(8,128)(2,1)S(1)} %all-to-all-done.4.attended_ref, bf16[2,256,2048]{2,1,0:T(8,128)(2,1)S(1)} %load.1.early_ref, bf16[256,2048]{1,0:T(8,128)(2,1)} %collective-permute-done.7.w2_ref, ...), custom_call_target="tpu_custom_call" | custom-call | tf_op jit(solution)/shard_map/project/pallas_call | solution.py:457
  129.5 8.0 %collective-permute-start.9 = (bf16[96,2048]{1,0:T(8,128)(2,1)S(1)}, bf16[96,2048]{1,0:T(8,128)(2,1)S(1)}, u32[]{:S(2)}, u32[]{:S(2)}) collective-permute-start(bf16[96,2048]{1,0:T(8,128)(2,1)S(1)} %get-tuple-element.22), channel_id=1, source_target_pairs={{0,1},{1,0},{2,3},{3,2},{4,5},{5,4},{6,7},{7,6},{8,9},{9,8},{10,11... | collective-permute-start | bytes 1179656 | tf_op jit(solution)/shard_map/ppermute | solution.py:316
  (31 shorter events, 9.4 us)
Async XLA Ops:
  0.0 13.3 %collective-permute-start = (bf16[96,2048]{1,0:T(8,128)(2,1)}, bf16[96,2048]{1,0:T(8,128)(2,1)S(1)}, u32[]{:S(2)}, u32[]{:S(2)}) collective-permute-start(bf16[96,2048]{1,0:T(8,128)(2,1)} %latent_ref.1), channel_id=1, source_target_pairs={{0,2},{2,4},{4,6},{6,0},{1,3},{3,5},{5,7},{7,1},{8,10},{10,12},{12... | collective-permute-start | bytes 1179656 | tf_op jit(solution)/shard_map/ppermute | solution.py:311
  3.1 11.8 %collective-permute-start.1 = (bf16[96,2048]{1,0:T(8,128)(2,1)}, bf16[96,2048]{1,0:T(8,128)(2,1)S(1)}, u32[]{:S(2)}, u32[]{:S(2)}) collective-permute-start(bf16[96,2048]{1,0:T(8,128)(2,1)} %latent_ref.1), channel_id=1, source_target_pairs={{0,6},{2,0},{4,2},{6,4},{1,7},{3,1},{5,3},{7,5},{8,14},{10,8},{12,... | collective-permute-start | bytes 1179656 | tf_op jit(solution)/shard_map/ppermute | solution.py:311
  6.5 16.2 %collective-permute-start.2 = (bf16[96,2048]{1,0:T(8,128)(2,1)}, bf16[96,2048]{1,0:T(8,128)(2,1)S(1)}, u32[]{:S(2)}, u32[]{:S(2)}) collective-permute-start(bf16[96,2048]{1,0:T(8,128)(2,1)} %latent_ref.1), channel_id=1, source_target_pairs={{0,4},{2,6},{4,0},{6,2},{1,5},{3,7},{5,1},{7,3},{8,12},{10,14},{12... | collective-permute-start | bytes 1179656 | tf_op jit(solution)/shard_map/ppermute | solution.py:311
  22.7 52.1 %copy-start = (bf16[2048,128]{1,0:T(8,128)(2,1)S(1)}, bf16[2048,128]{1,0:T(8,128)(2,1)}, u32[]{:S(2)}) copy-start(bf16[2048,128]{1,0:T(8,128)(2,1)} %wk_ref.3) | copy-start | bytes 1572868
  22.7 52.1 %copy-start.1 = (bf16[2048,128]{1,0:T(8,128)(2,1)S(1)}, bf16[2048,128]{1,0:T(8,128)(2,1)}, u32[]{:S(2)}) copy-start(bf16[2048,128]{1,0:T(8,128)(2,1)} %wv_ref.3) | copy-start | bytes 1572868
  24.0 72.6 %collective-permute-start.3 = (bf16[4,96,2048]{2,1,0:T(8,128)(2,1)S(1)}, bf16[4,96,2048]{2,1,0:T(8,128)(2,1)}, u32[]{:S(2)}, u32[]{:S(2)}) collective-permute-start(bf16[4,96,2048]{2,1,0:T(8,128)(2,1)S(1)} %pad_maximum_fusion.own_ref), channel_id=1, source_target_pairs={{0,1},{1,0},{2,3},{3,2},{4,5},{5,4},{6,7},{7,6},{8,9},{9,8},{10,11... | collective-permute-start | bytes 4718600 | tf_op jit(solution)/shard_map/ppermute | solution.py:316
  55.8 19.0 %all-to-all-start.1 = ((f32[32,1,1280]{2,1,0:T(1,128)}), f32[32,1,1280]{2,1,0:T(1,128)S(1)}, u32[]{:S(2)}, u32[]{:S(2)}) async-start(f32[32,1,1280]{2,1,0:T(1,128)} %sums.1), calls=%async_computation.1 | async-start | bytes 327680 | tf_op jit(solution)/shard_map/all_to_all | solution.py:47
  64.9 55.7 %collective-permute-start.6 = (bf16[256,2048]{1,0:T(8,128)(2,1)}, bf16[256,2048]{1,0:T(8,128)(2,1)}, u32[]{:S(2)}, u32[]{:S(2)}) collective-permute-start(bf16[256,2048]{1,0:T(8,128)(2,1)} %w0_ref.1), channel_id=1, source_target_pairs={{0,2},{2,4},{4,6},{6,0},{1,3},{3,5},{5,7},{7,1},{8,10},{10,12},{12... | collective-permute-start | bytes 3145736 | tf_op jit(solution)/shard_map/ppermute | solution.py:311
  68.0 54.1 %collective-permute-start.7 = (bf16[256,2048]{1,0:T(8,128)(2,1)}, bf16[256,2048]{1,0:T(8,128)(2,1)}, u32[]{:S(2)}, u32[]{:S(2)}) collective-permute-start(bf16[256,2048]{1,0:T(8,128)(2,1)} %w0_ref.1), channel_id=1, source_target_pairs={{0,6},{2,0},{4,2},{6,4},{1,7},{3,1},{5,3},{7,5},{8,14},{10,8},{12,... | collective-permute-start | bytes 3145736 | tf_op jit(solution)/shard_map/ppermute | solution.py:311
  71.4 50.7 %collective-permute-start.8 = (bf16[256,2048]{1,0:T(8,128)(2,1)}, bf16[256,2048]{1,0:T(8,128)(2,1)}, u32[]{:S(2)}, u32[]{:S(2)}) collective-permute-start(bf16[256,2048]{1,0:T(8,128)(2,1)} %w0_ref.1), channel_id=1, source_target_pairs={{0,4},{2,6},{4,0},{6,2},{1,5},{3,7},{5,1},{7,3},{8,12},{10,14},{12... | collective-permute-start | bytes 3145736 | tf_op jit(solution)/shard_map/ppermute | solution.py:311
  75.9 15.4 %all-to-all-start.2 = ((bf16[16,16,256]{2,1,0:T(8,128)(2,1)}), bf16[16,16,256]{2,1,0:T(8,128)(2,1)S(1)}, u32[]{:S(2)}, u32[]{:S(2)}) async-start(bf16[16,16,256]{2,1,0:T(8,128)(2,1)} %context_pairs.1), calls=%async_computation.2 | async-start | bytes 262144 | tf_op jit(solution)/shard_map/all_to_all | solution.py:47
  92.1 15.6 %all-to-all-start.3 = ((bf16[4,256,256]{2,1,0:T(8,128)(2,1)}), bf16[4,256,256]{2,1,0:T(8,128)(2,1)S(1)}, u32[]{:S(2)}, u32[]{:S(2)}) async-start(bf16[4,256,256]{2,1,0:T(8,128)(2,1)} %spread.1), calls=%async_computation.3 | async-start | bytes 1048576 | tf_op jit(solution)/shard_map/all_to_all | solution.py:47
  96.6 16.0 %copy-start.3 = (f32[2]{0:T(128)S(1)}, f32[2]{0:T(128)}, u32[]{:S(2)}) copy-start(f32[2]{0:T(128)} %sink_ref.1) | copy-start | bytes 28
  102.4 5.4 %collective-permute-start.4 = (bf16[128,256]{1,0:T(8,128)(2,1)S(1)}, bf16[128,256]{1,0:T(8,128)(2,1)S(1)}, u32[]{:S(2)}, u32[]{:S(2)}) collective-permute-start(bf16[128,256]{1,0:T(8,128)(2,1)S(1)} %get-tuple-element.17), channel_id=1, source_target_pairs={{0,8},{8,16},{16,24},{24,32},{32,40},{40,48},{48,56},{56,64},{64,7... | collective-permute-start | bytes 196616 | tf_op jit(solution)/shard_map/ppermute | solution.py:431
  105.1 7.5 %collective-permute-start.5 = (bf16[128,256]{1,0:T(8,128)(2,1)S(1)}, bf16[128,256]{1,0:T(8,128)(2,1)S(1)}, u32[]{:S(2)}, u32[]{:S(2)}) collective-permute-start(bf16[128,256]{1,0:T(8,128)(2,1)S(1)} %get-tuple-element.19), channel_id=1, source_target_pairs={{8,0},{16,8},{24,16},{32,24},{40,32},{48,40},{56,48},{64,56},{72,6... | collective-permute-start | bytes 196616 | tf_op jit(solution)/shard_map/ppermute | solution.py:432
  117.1 9.7 %all-to-all-start.4 = ((bf16[4,192,256]{2,1,0:T(8,128)(2,1)}), bf16[4,192,256]{2,1,0:T(8,128)(2,1)S(1)}, u32[]{:S(2)}, u32[]{:S(2)}) async-start(bf16[4,192,256]{2,1,0:T(8,128)(2,1)} %bitcast.13), calls=%async_computation.4 | async-start | bytes 786432 | tf_op jit(solution)/shard_map/all_to_all | solution.py:47
  122.1 16.7 %copy-start.2 = (bf16[96,2048]{1,0:T(8,128)(2,1)S(1)}, bf16[96,2048]{1,0:T(8,128)(2,1)}, u32[]{:S(2)}) copy-start(bf16[96,2048]{1,0:T(8,128)(2,1)} %latent_ref.1) | copy-start | bytes 1179652
  129.5 9.3 %collective-permute-start.9 = (bf16[96,2048]{1,0:T(8,128)(2,1)S(1)}, bf16[96,2048]{1,0:T(8,128)(2,1)S(1)}, u32[]{:S(2)}, u32[]{:S(2)}) collective-permute-start(bf16[96,2048]{1,0:T(8,128)(2,1)S(1)} %get-tuple-element.22), channel_id=1, source_target_pairs={{0,1},{1,0},{2,3},{3,2},{4,5},{5,4},{6,7},{7,6},{8,9},{9,8},{10,11... | collective-permute-start | bytes 1179656 | tf_op jit(solution)/shard_map/ppermute | solution.py:316
